TPU v7x, 32 devices: a whole 2x2x4 slice. The times are simulated.
32 devices in a mesh: grp: 2 (over y), ep: 8 (over z, x), tp: 2 (over core).
Axes of the slice: x: 2, y: 2, z: 4, core: 2. Of those that a mesh axis runs over, the one named last changes fastest.
Arguments:
- tokens: bfloat16 [2048, 2048], P(('grp', 'ep')), parts along dimension 0, may hold values from -6 to 6
- in_gain: float32 [2048], replicated, may hold values from 0.1 to 1.9
- routing: int32 [2048, 4], P(('grp', 'ep')), parts along dimension 0, may hold values from 0 to 15, as said below
- gate_prob: float32 [2048, 4], P(('grp', 'ep')), parts along dimension 0, may hold values from 0.05 to 1
- w_gate: bfloat16 [16, 2048, 512], P('ep', None, 'tp'), may hold values from -0.125 to 0.125
- w_up: bfloat16 [16, 2048, 512], P('ep', None, 'tp'), may hold values from -0.125 to 0.125
- w_down: bfloat16 [16, 512, 2048], P('ep', 'tp')
- out_gain: float32 [2048], P('tp'), may hold values from 0.1 to 1.9
Outputs:
- output: bfloat16 [2048, 2048], P(('grp', 'ep'), 'tp'), parts along dimension 0
There are 2 independent parts, one for each index of `grp`. A program takes and returns all parts, laid end to end along the dimension named above; an argument that names none is the same for every part. Nothing has to cross between parts.
Inputs may be any that keep to these rules, and one draw needn't show every extreme that they name: `routing`: each row names 4 different experts, all of one group (the same value of expert // 4). In the rows of one device no expert is named more than 64 times, and in every device's rows some expert is named exactly 64 times.
All inputs are finite; a program needn't handle non-finite values.
Results may differ from a plain program's by a relative error of at most 0.0077.
Values may be sent and summed in bfloat16 or wider, within the bound.
No kernel may reach another device: no remote copies, remote signals or barrier semaphores. Data moves between devices by JAX's collectives and lax.ppermute only.
A program may use at most 64 MiB of HBM per device.

v0:
```python
import jax
import jax.numpy as jnp
from jax import lax
from jax.sharding import PartitionSpec as P

GROUPS = 4


EPS = 1e-06


def slot_ranks(flat_routes, expert_count):
    matches = (flat_routes[:, None] == jnp.arange(expert_count, dtype=jnp.int32)[None, :]).astype(
        jnp.int32
    )
    earlier = jnp.cumsum(matches, axis=0) - matches
    return jnp.sum(earlier * matches, axis=1)


def fill_rows(source, entries):
    filled = entries > 0
    return jnp.where(
        filled[:, None], source[jnp.maximum(entries - 1, 0)], jnp.zeros((), source.dtype)
    )


def body(tokens, in_gain, routing, gate_prob, w_gate, w_up, w_down, out_gain):
    ep_count = lax.axis_size("ep")
    local_experts = w_gate.shape[0]
    expert_count = local_experts * ep_count
    tok_dev, top_count = routing.shape
    model_width = tokens.shape[1]
    half_width = out_gain.shape[0]
    group_width = expert_count // GROUPS
    row_cap = max(2, tok_dev * top_count // (2 * group_width))
    floats = tokens.astype(jnp.float32)
    normed = (
        floats * lax.rsqrt(jnp.mean(floats * floats, axis=-1, keepdims=True) + EPS) * in_gain
    ).astype(jnp.bfloat16)
    flat_routes = routing.reshape(-1)
    slot_rank = slot_ranks(flat_routes, expert_count)
    slot_ids = flat_routes * row_cap + slot_rank
    token_ids = jnp.arange(tok_dev * top_count, dtype=jnp.int32) // top_count
    slot_table = jnp.zeros((expert_count * row_cap,), jnp.int32).at[slot_ids].set(token_ids + 1)
    own_columns = lax.dynamic_slice_in_dim(normed, lax.axis_index("tp") * half_width, half_width, 1)
    sendbuf = fill_rows(own_columns, slot_table).reshape(
        ep_count, local_experts, row_cap, half_width
    )
    arrived = lax.all_to_all(sendbuf, "ep", split_axis=0, concat_axis=0, tiled=True)
    arrived = lax.all_gather(arrived, "tp", axis=3, tiled=True)
    gate_act = jnp.einsum("secd,edf->secf", arrived, w_gate, preferred_element_type=jnp.float32)
    up_act = jnp.einsum("secd,edf->secf", arrived, w_up, preferred_element_type=jnp.float32)
    hidden = (jax.nn.silu(gate_act) * up_act).astype(jnp.bfloat16)
    partial_out = jnp.einsum("secf,efd->secd", hidden, w_down, preferred_element_type=jnp.float32)
    results = lax.psum_scatter(
        partial_out.astype(jnp.bfloat16), "tp", scatter_dimension=3, tiled=True
    )
    returned = lax.all_to_all(results, "ep", split_axis=0, concat_axis=0, tiled=True).reshape(
        expert_count * row_cap, half_width
    )
    picked = returned[slot_ids].astype(jnp.float32).reshape(tok_dev, top_count, half_width)
    mixed_rows = jnp.sum(picked * gate_prob[:, :, None], axis=1)
    squares = jnp.sum(mixed_rows * mixed_rows, axis=1)
    total_squares = lax.psum(squares, "tp")
    inv_rms = lax.rsqrt(total_squares / model_width + EPS)
    return (mixed_rows * inv_rms[:, None] * out_gain).astype(jnp.bfloat16)


def solution(mesh):
    placed = (
        P(("grp", "ep"), None),
        P(),
        P(("grp", "ep"), None),
        P(("grp", "ep"), None),
        P("ep", None, "tp"),
        P("ep", None, "tp"),
        P("ep", "tp", None),
        P("tp"),
    )
    return jax.shard_map(
        body, mesh=mesh, in_specs=placed, out_specs=P(("grp", "ep"), "tp"), check_vma=False
    )
```

profile of v0, /device:TPU:0, one launch (start us, length us, event | category | flops | bytes accessed | tf_op | source)
XLA Modules:
  0.0 192.8 jit_solution(13421549271625434358)
XLA Ops:
  6.5 0.0 copy-start
  6.5 0.0 copy-start.1
  6.5 0.0 copy-start.4
  6.5 0.0 all-gather.2.cloned.1.call-start
  6.6 1.3 convert_element_type.34
  7.8 1.2 multiply_reduce_fusion.1
  9.1 0.0 copy-done.1
  9.1 0.1 copy.19
  9.2 0.1 eq.29
  9.3 0.1 eq.25
  9.4 1.2 reduce-window.6
  10.6 0.2 slice_reduce_fusion
  10.9 0.1 copy.18
  11.0 0.1 mul.77
  11.1 0.1 fusion.24
  11.2 2.4 %scatter_custom_fusion = s32[1024]{0:T(1024)S(1)} fusion(s32[512]{0:T(512)S(1)} %bitcast.63, s32[512]{0:T(512)S(1)} %fusion.26, s32[]{:T(128)} %constant.19.clone.1), kind=kCustom, calls=%fused_computation.42 | custom fusion | bytes 4100 | tf_op jit(solution)/shard_map/scatter | solution.py:44
  13.7 0.1 broadcast_in_dim.16
  13.8 0.0 copy-done.4
  13.8 0.1 fusion.20
  13.9 5.4 %gather_fusion = bf16[1024,1024]{1,0:T(8,128)(2,1)} fusion(bf16[128,1024]{1,0:T(8,128)(2,1)S(1)} %fusion.20, s32[1024]{0:T(1024)S(1)} %maximum_clamp_fusion), kind=kCustom, calls=%fused_computation | custom fusion | bytes 4198400 | tf_op jit(solution)/shard_map/gather | solution.py:23
  19.3 1.8 broadcast_select_fusion
  21.1 55.3 %all_to_all.10 = bf16[8,2,64,1024]{3,2,1,0:T(8,128)(2,1)S(1)} all-to-all(bf16[8,2,64,1024]{3,2,1,0:T(8,128)(2,1)S(1)} %broadcast_select_fusion), channel_id=1, replica_groups=mesh['grp'=2,'ep'=8,'tp'=2] {'ep'}, dimensions={0} | all-to-all | bytes 4194304 | tf_op jit(solution)/shard_map/all_to_all | solution.py:49
  76.4 1.5 copy.22
  77.9 0.0 all-gather.2.cloned.1.call-update
  78.0 0.0 reduce-scatter.2.cloned.1.call-start
  78.0 12.8 %all-gather.2.cloned.1.call-done = bf16[8,2,64,2048]{3,2,0,1:T(8,128)(2,1)} async-done(((bf16[8,2,64,1024]{3,2,0,1:T(8,128)(2,1)}), bf16[8,2,64,2048]{3,2,0,1:T(8,128)(2,1)}) %all-gather.2.cloned.1.call-update) | async-done | bytes 4194320 | tf_op jit(solution)/shard_map/all_gather | solution.py:50
  90.8 4.1 %fusion.5 = f32[8,2,64,256]{3,2,0,1:T(8,128)S(1)} fusion(bf16[8,2,64,2048]{3,2,0,1:T(8,128)(2,1)} %all-gather.2.cloned.1.call-done, bf16[2,2048,256]{2,1,0:T(8,128)(2,1)} %param.12), kind=kOutput, calls=%fused_computation.11 | convolution fusion | flops 1073741824 | bytes 7340032 | tf_op jit(solution)/shard_map/secd,edf->secf/dot_general | solution.py:51
  94.9 0.0 copy-done
  94.9 7.3 %convert_bitcast_fusion = bf16[8,2,64,2048]{3,2,0,1:T(8,128)(2,1)} fusion(bf16[2,256,2048]{2,1,0:T(8,128)(2,1)S(1)} %copy-done, bf16[8,2,64,2048]{3,2,0,1:T(8,128)(2,1)} %all-gather.2.cloned.1.call-done, bf16[2,2048,256]{2,1,0:T(8,128)(2,1)} %param.13, f32[8,2,64,256]{3,2,0,1:T(8,128)S(1)} %fusion.5), kind=kOutput, calls=%fused_computation.3 | convolution fusion | flops 2151153664 | bytes 13631488 | tf_op jit(solution)/shard_map/secf,efd->secd/dot_general | solution.py:54
  102.2 0.0 reduce-scatter.2.cloned.1.call-update
  102.3 13.2 %reduce-scatter.2.cloned.1.call-done = bf16[8,2,64,1024]{3,2,0,1:T(8,128)(2,1)} async-done(((bf16[8,2,64,2048]{3,2,0,1:T(8,128)(2,1)}), bf16[8,2,64,1024]{3,2,0,1:T(8,128)(2,1)}) %reduce-scatter.2.cloned.1.call-update) | async-done | bytes 2097168 | tf_op jit(solution)/shard_map/reduce_scatter | solution.py:55
  115.5 3.1 %copy.23 = bf16[8,2,64,1024]{3,2,1,0:T(8,128)(2,1)} copy(bf16[8,2,64,1024]{3,2,0,1:T(8,128)(2,1)} %reduce-scatter.2.cloned.1.call-done) | data formatting | bytes 4194304 | tf_op jit(solution)/shard_map/reduce_scatter | solution.py:55
  118.6 0.0 copy-start.3
  118.6 6.0 %all-to-all-start.1 = ((bf16[8,2,64,1024]{3,2,1,0:T(8,128)(2,1)}), bf16[8,2,64,1024]{3,2,1,0:T(8,128)(2,1)}, u32[]{:S(2)}, u32[]{:S(2)}) async-start(bf16[8,2,64,1024]{3,2,1,0:T(8,128)(2,1)} %copy.23), calls=%async_computation.2 | async-start | bytes 4194304 | tf_op jit(solution)/shard_map/all_to_all | solution.py:58
  124.6 0.0 copy-done.3
  124.6 0.1 copy.24
  124.7 48.5 %all-to-all-done.1 = bf16[8,2,64,1024]{3,2,1,0:T(8,128)(2,1)} async-done(((bf16[8,2,64,1024]{3,2,1,0:T(8,128)(2,1)}), bf16[8,2,64,1024]{3,2,1,0:T(8,128)(2,1)}, u32[]{:S(2)}, u32[]{:S(2)}) %all-to-all-start.1) | async-done | bytes 2097184 | tf_op jit(solution)/shard_map/all_to_all | solution.py:58
  173.3 4.6 %gather_fusion.1 = bf16[512,1024]{1,0:T(8,128)(2,1)S(1)} fusion(bf16[1024,1024]{1,0:T(8,128)(2,1)} %bitcast.13, s32[1024]{0:T(1024)S(1)} %pad_clamp_fusion), kind=kCustom, calls=%fused_computation.1 | custom fusion | bytes 2099200 | tf_op jit(solution)/shard_map/gather | solution.py:61
  177.9 1.7 reshape.75
  179.6 0.0 copy-start.2
  179.6 3.0 %multiply_reduce_fusion = f32[128,1024]{1,0:T(8,128)S(1)} fusion(f32[128,4,1024]{2,1,0:T(4,128)} %reshape.75, f32[128,4]{1,0:T(8,128)S(1)} %copy.24), kind=kLoop, calls=%fused_computation.9 | loop fusion | flops 917504 | bytes 2623488 | tf_op jit(solution)/shard_map/reduce_sum | solution.py:62
  182.6 0.1 multiply_reduce_fusion.2
  182.7 2.5 %psum.7 = f32[128]{0:T(128)S(1)} all-reduce(f32[128]{0:T(128)S(1)} %multiply_reduce_fusion.2), channel_id=1, replica_groups=mesh['grp'=2,'ep'=8,'tp'=2] {'tp'}, use_global_device_ids=true, to_apply=%region_8.9 | all-reduce | flops 128 | bytes 1024 | tf_op jit(solution)/shard_map/psum | solution.py:64
  185.2 0.0 copy-done.2
  185.2 0.8 multiply_convert_fusion
  (12 shorter events, 0.1 us)
Async XLA Ops:
  6.5 88.4 %copy-start = (bf16[2,256,2048]{2,1,0:T(8,128)(2,1)S(1)}, bf16[2,256,2048]{2,1,0:T(8,128)(2,1)}, u32[]{:S(2)}) copy-start(bf16[2,256,2048]{2,1,0:T(8,128)(2,1)} %param.14) | copy-start | bytes 6291460
  6.5 2.5 %copy-start.1 = (s32[128,4]{0,1:T(4,128)S(1)}, s32[128,4]{0,1:T(4,128)}, u32[]{:S(2)}) copy-start(s32[128,4]{0,1:T(4,128)} %param.10) | copy-start | bytes 6148
  6.5 7.2 %copy-start.4 = (f32[2048]{0:T(1024)S(1)}, f32[2048]{0:T(1024)}, u32[]{:S(2)}) copy-start(f32[2048]{0:T(1024)} %param.9) | copy-start | bytes 24580
  6.5 84.3 %all-gather.2.cloned.1.call-start = ((), (), s32[]{:S(2)}) async-start(), calls=%async_computation.3 | async-start | bytes 6291456 | tf_op jit(solution)/shard_map/all_gather | solution.py:50
  78.0 37.5 %reduce-scatter.2.cloned.1.call-start = ((), (), s32[]{:S(2)}) async-start(), calls=%async_computation.4 | async-start | bytes 6291456 | tf_op jit(solution)/shard_map/reduce_scatter | solution.py:55
  118.6 6.0 %copy-start.3 = (f32[128,4]{0,1:T(4,128)S(1)}, f32[128,4]{0,1:T(4,128)}, u32[]{:S(2)}) copy-start(f32[128,4]{0,1:T(4,128)} %param.11) | copy-start | bytes 6148
  118.6 54.7 %all-to-all-start.1 = ((bf16[8,2,64,1024]{3,2,1,0:T(8,128)(2,1)}), bf16[8,2,64,1024]{3,2,1,0:T(8,128)(2,1)}, u32[]{:S(2)}, u32[]{:S(2)}) async-start(bf16[8,2,64,1024]{3,2,1,0:T(8,128)(2,1)} %copy.23), calls=%async_computation.2 | async-start | bytes 4194304 | tf_op jit(solution)/shard_map/all_to_all | solution.py:58
  179.6 5.6 %copy-start.2 = (f32[1024]{0:T(1024)S(1)}, f32[1024]{0:T(1024)}, u32[]{:S(2)}) copy-start(f32[1024]{0:T(1024)} %param.15) | copy-start | bytes 12292
Sparse Core Ops, SparseCore 0:
  78.1 12.6 all-gather.1
  102.4 13.0 reduce-scatter.1
where the time goes:
time: 193 us
  waiting for transfers between devices  74.6 us (39%)
  blocking collectives  57.8 us (30%)
  local copies, waits for them, and re-layouts  19.8 us (10%)
  between operations  13.6 us (7%)
  matrix products  11.4 us (6%)
  other arithmetic  9.68 us (5%)
  starting transfers between devices  6.06 us (3%)
    all_to_all x1, blocking collectives, body(): lax.all_to_all(sendbuf, 'ep', split_axis=0, concat_axis=0, tiled=True)  55.3 us
    all_to_all x1, waiting for transfers between devices, body(): lax.all_to_all(results, 'ep', split_axis=0, concat_axis=0, tiled=True)  48.5 us
    reduce_scatter x1, waiting for transfers between devices, body(): lax.psum_scatter(partial_out.astype(jnp.bfloat16), 'tp', scatter_dimensio...  13.2 us
    all_gather x1, waiting for transfers between devices, body(): arrived = lax.all_gather(arrived, 'tp', axis=3, tiled=True)  12.8 us
    dot_general x1, matrix products, body(): jnp.einsum('secf,efd->secd', hidden, w_down, preferred_element_type=jnp.f...  7.3 us
    all_to_all x1, starting transfers between devices, body(): lax.all_to_all(results, 'ep', split_axis=0, concat_axis=0, tiled=True)  6.02 us
    gather x1, local copies, waits for them, and re-layouts, fill_rows(): source[jnp.maximum(entries - 1, 0)]  5.36 us
    gather x1, local copies, waits for them, and re-layouts, body(): returned[slot_ids].astype(jnp.float32)  4.59 us
  transfers between devices with their start and end apart: 3, of which 3 were waited for; matrix products, arithmetic and copies ran while one was open for 0% of the time, Pallas kernels for 0%

commit v1 on v0

--- a/solution.py
+++ b/solution.py
@@ -1,12 +1,19 @@
+import functools
+
 import jax
 import jax.numpy as jnp
 from jax import lax
+from jax.experimental import pallas as pl
+from jax.experimental.pallas import tpu as pltpu
 from jax.sharding import PartitionSpec as P
 
 GROUPS = 4
 
 
 EPS = 1e-06
+LANES = 128
+TERMS = 3
+MIB = 1 << 20
 
 
 def slot_ranks(flat_routes, expert_count):
@@ -24,7 +31,7 @@
     )
 
 
-def body(tokens, in_gain, routing, gate_prob, w_gate, w_up, w_down, out_gain):
+def sparse_body(tokens, in_gain, routing, gate_prob, w_gate, w_up, w_down, out_gain):
     ep_count = lax.axis_size("ep")
     local_experts = w_gate.shape[0]
     expert_count = local_experts * ep_count
@@ -66,6 +73,236 @@
     return (mixed_rows * inv_rms[:, None] * out_gain).astype(jnp.bfloat16)
 
 
+def dot(a, b):
+    return jnp.dot(a, b, preferred_element_type=jnp.float32)
+
+
+def pack_kernel(members, width, cap, tok_ref, gain_ref, route_ref, prob_ref, *outs):
+    half = cap // 2
+    my_group = lax.axis_index("ep") // members
+    my_half = lax.axis_index("tp")
+    floats = tok_ref[...].astype(jnp.float32)
+    tok_dev, model_width = floats.shape
+    inv = lax.rsqrt(jnp.sum(floats * floats, axis=-1, keepdims=True) / model_width + EPS)
+    normed = (floats * inv * gain_ref[...]).astype(jnp.bfloat16)
+    routes = route_ref[...]
+    probs = prob_ref[...]
+    first = routes[:, 0:1]
+    group = jnp.zeros_like(first)
+    for g in range(1, GROUPS):
+        group += (first >= g * width).astype(jnp.int32)
+    lane = lax.broadcasted_iota(jnp.int32, (tok_dev, LANES), 1)
+    member = (group == lane).astype(jnp.float32)
+    row = lax.broadcasted_iota(jnp.int32, (tok_dev, tok_dev), 0)
+    col = lax.broadcasted_iota(jnp.int32, (tok_dev, tok_dev), 1)
+    earlier = dot((col < row).astype(jnp.bfloat16), member.astype(jnp.bfloat16))
+    rank = jnp.sum(earlier * member, axis=1, keepdims=True).astype(jnp.int32)
+    relative = group ^ my_group
+    send_slot = lax.broadcasted_iota(jnp.int32, (tok_dev, GROUPS * half), 1)
+    pick = (
+        (relative == send_slot // half) & (rank == send_slot % half + my_half * half)
+    ).astype(jnp.bfloat16)
+    lane_expert = lane % width
+    weight = jnp.zeros((tok_dev, LANES), jnp.float32)
+    for k in range(routes.shape[1]):
+        weight += jnp.where(routes[:, k : k + 1] - group * width == lane_expert, probs[:, k : k + 1], 0.0)
+    high = weight.astype(jnp.bfloat16)
+    rest = weight - high.astype(jnp.float32)
+    middle = rest.astype(jnp.bfloat16)
+    low = (rest - middle.astype(jnp.float32)).astype(jnp.bfloat16)
+    zero = jnp.zeros_like(high)
+    terms = jnp.where(
+        lane < width,
+        high,
+        jnp.where(lane < 2 * width, middle, jnp.where(lane < TERMS * width, low, zero)),
+    )
+    contract = (((0,), (0,)), ((), ()))
+    rows = lax.dot_general(pick, normed, contract, preferred_element_type=jnp.float32)
+    extra = lax.dot_general(pick, terms, contract, preferred_element_type=jnp.float32)
+    for k in range(GROUPS):
+        outs[k][:, :model_width] = rows[k * half : (k + 1) * half].astype(jnp.bfloat16)
+        outs[k][:, model_width:] = extra[k * half : (k + 1) * half].astype(jnp.bfloat16)
+    slot = lax.broadcasted_iota(jnp.int32, (tok_dev, GROUPS * cap), 1)
+    outs[GROUPS][...] = (relative * cap + rank == slot).astype(jnp.bfloat16)
+
+
+def expert_kernel(chunks, members, width, half, *refs):
+    pieces = refs[: 4 * chunks]
+    wg_ref, wu_ref, wd_ref, keep_ref, send_ref, rows_ref = refs[4 * chunks :]
+    my_half = lax.axis_index("tp")
+    me = lax.axis_index("ep") % members
+    local_experts, model_width, hidden_width = wg_ref.shape
+    half_width = keep_ref.shape[1]
+    mine = pl.multiple_of(my_half * half, half)
+    other = pl.multiple_of((1 - my_half) * half, half)
+    for c in range(chunks):
+        own, own_tp, far, far_tp = pieces[4 * c : 4 * c + 4]
+        near_base = c * 4 * half
+        far_base = near_base + 2 * half
+        rows_ref[pl.ds(near_base + mine, half), :] = own[...]
+        rows_ref[pl.ds(near_base + other, half), :] = own_tp[...]
+        rows_ref[pl.ds(far_base + mine, half), :] = far[...]
+        rows_ref[pl.ds(far_base + other, half), :] = far_tp[...]
+    rows = rows_ref[:, :model_width]
+    terms = rows_ref[:, model_width:].astype(jnp.float32)
+    lane = lax.broadcasted_iota(jnp.int32, terms.shape, 1)
+    hidden = []
+    for e in range(local_experts):
+        wanted = (lane % width == me * local_experts + e) & (lane < TERMS * width)
+        weight = jnp.sum(jnp.where(wanted, terms, 0.0), axis=1, keepdims=True)
+        gate_act = dot(rows, wg_ref[e])
+        up_act = dot(rows, wu_ref[e])
+        act = gate_act / (1.0 + jnp.exp(-gate_act)) * up_act
+        hidden.append((act * weight).astype(jnp.bfloat16))
+    send_at = pl.multiple_of((1 - my_half) * half_width, half_width)
+    keep_at = pl.multiple_of(my_half * half_width, half_width)
+    total = dot(hidden[0], wd_ref[0, :, pl.ds(send_at, half_width)])
+    for e in range(1, local_experts):
+        total += dot(hidden[e], wd_ref[e, :, pl.ds(send_at, half_width)])
+    send_ref[...] = total.astype(jnp.bfloat16)
+    total = dot(hidden[0], wd_ref[0, :, pl.ds(keep_at, half_width)])
+    for e in range(1, local_experts):
+        total += dot(hidden[e], wd_ref[e, :, pl.ds(keep_at, half_width)])
+    keep_ref[...] = total
+
+
+def split_kernel(chunks, cap, mine_ref, recv_ref, keep_ref, send_ref):
+    for c in range(chunks):
+        near = pl.ds(2 * c * cap, cap)
+        far = pl.ds((2 * c + 1) * cap, cap)
+        out = pl.ds(c * cap, cap)
+        keep_ref[out, :] = mine_ref[near, :] + recv_ref[near, :].astype(jnp.float32)
+        send_ref[out, :] = (mine_ref[far, :] + recv_ref[far, :].astype(jnp.float32)).astype(
+            jnp.bfloat16
+        )
+
+
+def join_kernel(chunks, cap, keep_ref, recv_ref, *outs):
+    for c in range(chunks):
+        at = pl.ds(c * cap, cap)
+        outs[c][...] = (keep_ref[at, :] + recv_ref[at, :].astype(jnp.float32)).astype(jnp.bfloat16)
+
+
+def place_kernel(cap, map_ref, *refs):
+    parts = refs[:GROUPS]
+    mixed_ref, square_ref = refs[GROUPS:]
+    mixed = dot(map_ref[:, :cap], parts[0][...])
+    for k in range(1, GROUPS):
+        mixed += dot(map_ref[:, k * cap : (k + 1) * cap], parts[k][...])
+    mixed_ref[...] = mixed
+    square_ref[...] = jnp.broadcast_to(
+        jnp.sum(mixed * mixed, axis=1, keepdims=True), square_ref.shape
+    )
+
+
+def close_kernel(model_width, mixed_ref, mine_ref, other_ref, gain_ref, out_ref):
+    squares = (mine_ref[...] + other_ref[...])[:, 0:1]
+    inv = lax.rsqrt(squares / model_width + EPS)
+    out_ref[...] = (mixed_ref[...] * inv * gain_ref[...]).astype(jnp.bfloat16)
+
+
+def call(kernel, outs, args, name, limit, flops, scratch=()):
+    return pl.pallas_call(
+        kernel,
+        out_shape=outs,
+        scratch_shapes=scratch,
+        name=name,
+        compiler_params=pltpu.CompilerParams(vmem_limit_bytes=limit * MIB),
+        cost_estimate=pl.CostEstimate(flops=flops, transcendentals=0, bytes_accessed=0),
+    )(*args)
+
+
+def dense_body(tokens, in_gain, routing, gate_prob, w_gate, w_up, w_down, out_gain):
+    ep_count = lax.axis_size("ep")
+    local_experts, model_width, hidden_width = w_gate.shape
+    tok_dev, top_count = routing.shape
+    half_width = out_gain.shape[0]
+    width = local_experts * ep_count // GROUPS
+    members = width // local_experts
+    cap = tok_dev * top_count // (2 * width)
+    half = cap // 2
+    sds = jax.ShapeDtypeStruct
+    bf16, f32 = jnp.bfloat16, jnp.float32
+    block = sds((half, model_width + LANES), bf16)
+
+    def hop(value, k):
+        pairs = [(i, ((i // members) ^ k) * members + i % members) for i in range(ep_count)]
+        return lax.ppermute(value, "ep", pairs)
+
+    def cross(value):
+        pairs = [(i, i ^ 1) for i in range(ep_count)]
+        return lax.ppermute(value, "ep", pairs)
+
+    def swap(value):
+        return lax.ppermute(value, "tp", [(0, 1), (1, 0)])
+
+    packed = call(
+        functools.partial(pack_kernel, members, width, cap),
+        [block] * GROUPS + [sds((tok_dev, GROUPS * cap), bf16)],
+        (tokens, in_gain.reshape(1, -1), routing, gate_prob),
+        "pack",
+        12,
+        2 * tok_dev * tok_dev * model_width,
+    )
+    token_map = packed[GROUPS]
+    arrived = [packed[0]] + [hop(packed[k], k) for k in range(1, GROUPS)]
+
+    def experts(ks):
+        pieces = []
+        for k in ks:
+            far = cross(arrived[k])
+            pieces += [arrived[k], swap(arrived[k]), far, swap(far)]
+        n = len(ks)
+        rows = n * 2 * cap
+        mine, other = call(
+            functools.partial(expert_kernel, n, members, width, half),
+            [sds((rows, half_width), f32), sds((rows, half_width), bf16)],
+            (*pieces, w_gate, w_up, w_down),
+            "experts",
+            24,
+            6 * rows * model_width * hidden_width * local_experts,
+            (pltpu.VMEM((rows, model_width + LANES), bf16),),
+        )
+        keep, send = call(
+            functools.partial(split_kernel, n, cap),
+            [sds((n * cap, half_width), f32), sds((n * cap, half_width), bf16)],
+            (mine, swap(other)),
+            "split",
+            8,
+            rows * half_width,
+        )
+        return call(
+            functools.partial(join_kernel, n, cap),
+            [sds((cap, half_width), bf16)] * n,
+            (keep, cross(send)),
+            "join",
+            8,
+            rows * half_width,
+        )
+
+    step = GROUPS // 2
+    first = experts(range(step))
+    second = experts(range(step, GROUPS))
+    done = list(first) + list(second)
+    back = [done[0]] + [hop(done[k], k) for k in range(1, GROUPS)]
+    mixed, squares = call(
+        functools.partial(place_kernel, cap),
+        [sds((tok_dev, half_width), f32), sds((tok_dev, LANES), f32)],
+        (token_map, *back),
+        "place",
+        8,
+        2 * tok_dev * GROUPS * cap * half_width,
+    )
+    return call(
+        functools.partial(close_kernel, model_width),
+        sds((tok_dev, half_width), bf16),
+        (mixed, squares, swap(squares), out_gain.reshape(1, -1)),
+        "close",
+        8,
+        tok_dev * half_width,
+    )
+
+
 def solution(mesh):
     placed = (
         P(("grp", "ep"), None),
@@ -77,6 +314,13 @@
         P("ep", "tp", None),
         P("tp"),
     )
+
+    def body(*args):
+        routing, w_gate = args[2], args[4]
+        width = w_gate.shape[0] * mesh.shape["ep"] // GROUPS
+        dense = routing.shape[1] == width and width == 2 * w_gate.shape[0] and mesh.shape["tp"] == 2
+        return (dense_body if dense else sparse_body)(*args)
+
     return jax.shard_map(
         body, mesh=mesh, in_specs=placed, out_specs=P(("grp", "ep"), "tp"), check_vma=False
     )

time: 193 us -> 63.9 us (0.33)
  blocking collectives: 57.8 us -> 0 us
  waiting for transfers between devices: 74.6 us -> 26.8 us
  starting transfers between devices: 6.06 us -> 22.1 us
  between operations: 13.6 us -> 0.13 us
  local copies, waits for them, and re-layouts: 19.8 us -> 8.09 us
  matrix products: 11.4 us -> 0 us
  other arithmetic: 9.68 us -> 0 us
  Pallas kernels: 0 us -> 6.39 us
    all_to_all x1 -> x0, blocking collectives: 55.3 us -> none  [body(): lax.all_to_all(sendbuf, 'ep', split_axis=0, concat_axis=0, tiled=True)]
    all_to_all x1 -> x0, waiting for transfers between devices: 48.5 us -> none  [body(): lax.all_to_all(results, 'ep', split_axis=0, concat_axis=0, tiled=True)]
    ppermute x0 -> x23, waiting for transfers between devices: none -> 26.8 us  [the longest x6 14 us: hop(): return lax.ppermute(value, 'ep', pairs)]
    ppermute x0 -> x23, starting transfers between devices: none -> 22.1 us  [the longest x6 11.7 us: hop(): return lax.ppermute(value, 'ep', pairs)]
    reduce_scatter x1 -> x0, waiting for transfers between devices: 13.2 us -> none  [body(): lax.psum_scatter(partial_out.astype(jnp.bfloat16), 'tp', scatter_dimensio...]
    all_gather x1 -> x0, waiting for transfers between devices: 12.8 us -> none  [body(): arrived = lax.all_gather(arrived, 'tp', axis=3, tiled=True)]
    dot_general x2 -> x0, matrix products: 11.4 us -> none  [the longest x1 7.3 us: body(): jnp.einsum('secf,efd->secd', hidden, w_down, preferred_element_type=jnp.f...]
    gather x2 -> x0, local copies, waits for them, and re-layouts: 9.95 us -> none  [the longest x1 5.36 us: fill_rows(): source[jnp.maximum(entries - 1, 0)]]
  transfers between devices with their start and end apart: 3 -> 23, of which waited for: 3 -> 9; matrix products, arithmetic and copies ran while one was open for 0% -> 0% of each run, Pallas kernels for 0% -> 7%
where the time goes in v1:
time: 63.9 us; the launch traced here: 63.5 us
  waiting for transfers between devices  26.8 us (42%)
  starting transfers between devices  22.1 us (35%)
  local copies, waits for them, and re-layouts  8.09 us (13%)
  Pallas kernels  6.39 us (10%)
    ppermute x6, waiting for transfers between devices, hop(): return lax.ppermute(value, 'ep', pairs)  14 us
    ppermute x6, starting transfers between devices, hop(): return lax.ppermute(value, 'ep', pairs)  11.7 us
    ppermute x6, waiting for transfers between devices, cross(): return lax.ppermute(value, 'ep', pairs)  11.5 us
    ppermute x6, starting transfers between devices, cross(): return lax.ppermute(value, 'ep', pairs)  8.15 us
    unnamed x16, local copies, waits for them, and re-layouts  8.09 us
    pallas_call x9, Pallas kernels, call(): pl.pallas_call(kernel, out_shape=outs, scratch_shapes=scratch, name=name,...  6.39 us
    ppermute x11, starting transfers between devices, swap(): return lax.ppermute(value, 'tp', [(0, 1), (1, 0)])  2.29 us
  transfers between devices with their start and end apart: 23, of which 9 were waited for; matrix products, arithmetic and copies ran while one was open for 0% of the time, Pallas kernels for 7%

profile of v1, /device:TPU:0, one launch (start us, length us, event | category | flops | bytes accessed | tf_op | source)
XLA Modules:
  0.0 63.5 jit_solution(15991315242156345888)
XLA Ops:
  0.0 0.8 %copy.10.prob_ref = f32[128,4]{1,0:T(8,128)S(1)} copy(f32[128,4]{0,1:T(4,128)} %param.11) | data formatting | bytes 4096 | tf_op args[3]
  0.8 0.8 %copy.9.route_ref = s32[128,4]{1,0:T(8,128)S(1)} copy(s32[128,4]{0,1:T(4,128)} %param.10) | data formatting | bytes 4096 | tf_op args[2]
  1.6 1.0 %copy-done.4 = bf16[128,2048]{1,0:T(8,128)(2,1)S(1)} copy-done((bf16[128,2048]{1,0:T(8,128)(2,1)S(1)}, bf16[128,2048]{1,0:T(8,128)(2,1)}, u32[]{:S(2)}) %copy-start.4) | copy-done | bytes 524312
  2.6 0.7 %copy-done.5 = f32[2048]{0:T(1024)S(1)} copy-done((f32[2048]{0:T(1024)S(1)}, f32[2048]{0:T(1024)}, u32[]{:S(2)}) %copy-start.5) | copy-done | bytes 8216
  3.3 0.9 %pack.1 = (bf16[32,2176]{1,0:T(8,128)(2,1)S(1)}, bf16[32,2176]{1,0:T(8,128)(2,1)S(1)}, bf16[32,2176]{1,0:T(8,128)(2,1)S(1)}, bf16[32,2176]{1,0:T(8,128)(2,1)S(1)}, bf16[128,256]{1,0:T(8,128)(2,1)S(1)}) custom-call(bf16[128,2048]{1,0:T(8,128)(2,1)S(1)} %copy-done.4, f32[1,2048]{1,0:T(1,128)S(1)} %bitcast.2, s32[128,4]{1,0:T(8,128)S(1)} %copy.9.route_ref, ...), custom_call_target="tpu_custom_call" | custom-call | flops 67108864 | tf_op jit(solution)/shard_map/pack/pallas_call | solution.py:205
  4.2 4.1 %collective-permute-start.10 = (bf16[32,2176]{1,0:T(8,128)(2,1)S(1)}, bf16[32,2176]{1,0:T(8,128)(2,1)S(1)}, u32[]{:S(2)}, u32[]{:S(2)}) collective-permute-start(bf16[32,2176]{1,0:T(8,128)(2,1)S(1)} %get-tuple-element.33), channel_id=1, source_target_pairs={{0,8},{2,10},{4,12},{6,14},{8,0},{10,2},{12,4},{14,6},{1,9},{3,11}... | collective-permute-start | bytes 417800 | tf_op jit(solution)/shard_map/ppermute | solution.py:230
  8.3 1.3 %collective-permute-start.14 = (bf16[32,2176]{1,0:T(8,128)(2,1)S(1)}, bf16[32,2176]{1,0:T(8,128)(2,1)S(1)}, u32[]{:S(2)}, u32[]{:S(2)}) collective-permute-start(bf16[32,2176]{1,0:T(8,128)(2,1)S(1)} %get-tuple-element.34), channel_id=1, source_target_pairs={{0,12},{2,14},{4,8},{6,10},{8,4},{10,6},{12,0},{14,2},{1,13},{3,15... | collective-permute-start | bytes 417800 | tf_op jit(solution)/shard_map/ppermute | solution.py:230
  9.6 0.2 collective-permute-start.3
  9.9 1.5 %collective-permute-start.1 = (bf16[32,2176]{1,0:T(8,128)(2,1)S(1)}, bf16[32,2176]{1,0:T(8,128)(2,1)S(1)}, u32[]{:S(2)}, u32[]{:S(2)}) collective-permute-start(bf16[32,2176]{1,0:T(8,128)(2,1)S(1)} %get-tuple-element.25.refs_0_), channel_id=1, source_target_pairs={{0,2},{2,0},{4,6},{6,4},{8,10},{10,8},{12,14},{14,12},{1,3},{3,1},... | collective-permute-start | bytes 417800 | tf_op jit(solution)/shard_map/ppermute | solution.py:234
  11.4 7.5 %collective-permute-done.10.refs_0_ = bf16[32,2176]{1,0:T(8,128)(2,1)S(1)} collective-permute-done((bf16[32,2176]{1,0:T(8,128)(2,1)S(1)}, bf16[32,2176]{1,0:T(8,128)(2,1)S(1)}, u32[]{:S(2)}, u32[]{:S(2)}) %collective-permute-start.10) | collective-permute-done | bytes 139296 | tf_op jit(solution)/shard_map/ppermute | solution.py:230
  18.8 1.8 %collective-permute-start.12 = (bf16[32,2176]{1,0:T(8,128)(2,1)S(1)}, bf16[32,2176]{1,0:T(8,128)(2,1)S(1)}, u32[]{:S(2)}, u32[]{:S(2)}) collective-permute-start(bf16[32,2176]{1,0:T(8,128)(2,1)S(1)} %collective-permute-done.10.refs_0_), channel_id=1, source_target_pairs={{0,2},{2,0},{4,6},{6,4},{8,10},{10,8},{12,14},{14,12},{1,3},{3,1},... | collective-permute-start | bytes 417800 | tf_op jit(solution)/shard_map/ppermute | solution.py:234
  20.6 0.2 collective-permute-start.16
  20.9 0.0 collective-permute-start.11
  20.9 0.0 collective-permute-done.3.refs_4_
  20.9 0.5 collective-permute-start.15
  21.4 0.0 collective-permute-done.1.refs_2_
  21.4 1.8 %collective-permute-start.5 = (bf16[32,2176]{1,0:T(8,128)(2,1)S(1)}, bf16[32,2176]{1,0:T(8,128)(2,1)S(1)}, u32[]{:S(2)}, u32[]{:S(2)}) collective-permute-start(bf16[32,2176]{1,0:T(8,128)(2,1)S(1)} %collective-permute-done.3.refs_4_), channel_id=1, source_target_pairs={{0,2},{2,0},{4,6},{6,4},{8,10},{10,8},{12,14},{14,12},{1,3},{3,1},... | collective-permute-start | bytes 417800 | tf_op jit(solution)/shard_map/ppermute | solution.py:234
  23.2 1.4 %collective-permute-done.12.refs_2_ = bf16[32,2176]{1,0:T(8,128)(2,1)S(1)} collective-permute-done((bf16[32,2176]{1,0:T(8,128)(2,1)S(1)}, bf16[32,2176]{1,0:T(8,128)(2,1)S(1)}, u32[]{:S(2)}, u32[]{:S(2)}) %collective-permute-start.12) | collective-permute-done | bytes 139296 | tf_op jit(solution)/shard_map/ppermute | solution.py:234
  24.5 0.0 collective-permute-start.13
  24.5 2.8 %collective-permute-done.16.refs_6_ = bf16[32,2176]{1,0:T(8,128)(2,1)S(1)} collective-permute-done((bf16[32,2176]{1,0:T(8,128)(2,1)S(1)}, bf16[32,2176]{1,0:T(8,128)(2,1)S(1)}, u32[]{:S(2)}, u32[]{:S(2)}) %collective-permute-start.16) | collective-permute-done | bytes 139296 | tf_op jit(solution)/shard_map/ppermute | solution.py:234
  27.3 0.5 collective-permute-start
  27.8 0.1 collective-permute-start.4
  27.9 0.9 %collective-permute-done.5.refs_6_ = bf16[32,2176]{1,0:T(8,128)(2,1)S(1)} collective-permute-done((bf16[32,2176]{1,0:T(8,128)(2,1)S(1)}, bf16[32,2176]{1,0:T(8,128)(2,1)S(1)}, u32[]{:S(2)}, u32[]{:S(2)}) %collective-permute-start.5) | collective-permute-done | bytes 139296 | tf_op jit(solution)/shard_map/ppermute | solution.py:234
  28.8 0.5 collective-permute-start.6
  29.3 1.6 %copy-done = bf16[2,2048,256]{2,1,0:T(8,128)(2,1)S(1)} copy-done((bf16[2,2048,256]{2,1,0:T(8,128)(2,1)S(1)}, bf16[2,2048,256]{2,1,0:T(8,128)(2,1)}, u32[]{:S(2)}) %copy-start) | copy-done | bytes 2097176
  30.9 1.6 %copy-done.2 = bf16[2,2048,256]{2,1,0:T(8,128)(2,1)S(1)} copy-done((bf16[2,2048,256]{2,1,0:T(8,128)(2,1)S(1)}, bf16[2,2048,256]{2,1,0:T(8,128)(2,1)}, u32[]{:S(2)}) %copy-start.2) | copy-done | bytes 2097176
  32.5 1.6 %copy-done.3 = bf16[2,256,2048]{2,1,0:T(8,128)(2,1)S(1)} copy-done((bf16[2,256,2048]{2,1,0:T(8,128)(2,1)S(1)}, bf16[2,256,2048]{2,1,0:T(8,128)(2,1)}, u32[]{:S(2)}) %copy-start.3) | copy-done | bytes 2097176
  34.1 2.0 %experts.3 = (f32[256,1024]{1,0:T(8,128)S(1)}, bf16[256,1024]{1,0:T(8,128)(2,1)S(1)}) custom-call(bf16[32,2176]{1,0:T(8,128)(2,1)S(1)} %collective-permute-done.10.refs_0_, bf16[32,2176]{1,0:T(8,128)(2,1)S(1)} %collective-permute-done.11.refs_1_, bf16[32,2176]{1,0:T(8,128)(2,1)S(1)} %collective-permute-done.12.refs_2_, ...), custom_call_target="tpu_custom_call" | custom-call | flops 1610612736 | tf_op jit(solution)/shard_map/experts/pallas_call | solution.py:205
  36.0 0.1 collective-permute-start.18
  36.2 2.0 %experts.2 = (f32[256,1024]{1,0:T(8,128)S(1)}, bf16[256,1024]{1,0:T(8,128)(2,1)S(1)}) custom-call(bf16[32,2176]{1,0:T(8,128)(2,1)S(1)} %get-tuple-element.25.refs_0_, bf16[32,2176]{1,0:T(8,128)(2,1)S(1)} %collective-permute-done.refs_1_, bf16[32,2176]{1,0:T(8,128)(2,1)S(1)} %collective-permute-done.1.refs_2_, ...), custom_call_target="tpu_custom_call" | custom-call | flops 1610612736 | tf_op jit(solution)/shard_map/experts/pallas_call | solution.py:205
  38.1 0.5 collective-permute-start.7
  38.7 0.1 split.3
  38.8 0.0 copy-start.6
  38.8 1.4 %collective-permute-start.19 = (bf16[128,1024]{1,0:T(8,128)(2,1)S(1)}, bf16[128,1024]{1,0:T(8,128)(2,1)S(1)}, u32[]{:S(2)}, u32[]{:S(2)}) collective-permute-start(bf16[128,1024]{1,0:T(8,128)(2,1)S(1)} %get-tuple-element.38), channel_id=1, source_target_pairs={{0,2},{2,0},{4,6},{6,4},{8,10},{10,8},{12,14},{14,12},{1,3},{3,1},... | collective-permute-start | bytes 786440 | tf_op jit(solution)/shard_map/ppermute | solution.py:234
  40.2 0.0 collective-permute-done.7.recv_ref
  40.2 0.1 split.2
  40.3 1.4 %collective-permute-start.8 = (bf16[128,1024]{1,0:T(8,128)(2,1)S(1)}, bf16[128,1024]{1,0:T(8,128)(2,1)S(1)}, u32[]{:S(2)}, u32[]{:S(2)}) collective-permute-start(bf16[128,1024]{1,0:T(8,128)(2,1)S(1)} %get-tuple-element.30), channel_id=1, source_target_pairs={{0,2},{2,0},{4,6},{6,4},{8,10},{10,8},{12,14},{14,12},{1,3},{3,1},... | collective-permute-start | bytes 786440 | tf_op jit(solution)/shard_map/ppermute | solution.py:234
  41.7 6.3 %collective-permute-done.19.recv_ref = bf16[128,1024]{1,0:T(8,128)(2,1)S(1)} collective-permute-done((bf16[128,1024]{1,0:T(8,128)(2,1)S(1)}, bf16[128,1024]{1,0:T(8,128)(2,1)S(1)}, u32[]{:S(2)}, u32[]{:S(2)}) %collective-permute-start.19) | collective-permute-done | bytes 262176 | tf_op jit(solution)/shard_map/ppermute | solution.py:234
  48.1 3.5 %collective-permute-start.20 = (bf16[64,1024]{1,0:T(8,128)(2,1)S(1)}, bf16[64,1024]{1,0:T(8,128)(2,1)S(1)}, u32[]{:S(2)}, u32[]{:S(2)}) collective-permute-start(bf16[64,1024]{1,0:T(8,128)(2,1)S(1)} %get-tuple-element.39), channel_id=1, source_target_pairs={{0,8},{2,10},{4,12},{6,14},{8,0},{10,2},{12,4},{14,6},{1,9},{3,11}... | collective-permute-start | bytes 393224 | tf_op jit(solution)/shard_map/ppermute | solution.py:230
  51.5 1.0 %collective-permute-start.21 = (bf16[64,1024]{1,0:T(8,128)(2,1)S(1)}, bf16[64,1024]{1,0:T(8,128)(2,1)S(1)}, u32[]{:S(2)}, u32[]{:S(2)}) collective-permute-start(bf16[64,1024]{1,0:T(8,128)(2,1)S(1)} %get-tuple-element.40), channel_id=1, source_target_pairs={{0,12},{2,14},{4,8},{6,10},{8,4},{10,6},{12,0},{14,2},{1,13},{3,15... | collective-permute-start | bytes 393224 | tf_op jit(solution)/shard_map/ppermute | solution.py:230
  52.5 0.2 collective-permute-done.8.recv_ref
  52.8 1.5 %collective-permute-start.9 = (bf16[64,1024]{1,0:T(8,128)(2,1)S(1)}, bf16[64,1024]{1,0:T(8,128)(2,1)S(1)}, u32[]{:S(2)}, u32[]{:S(2)}) collective-permute-start(bf16[64,1024]{1,0:T(8,128)(2,1)S(1)} %get-tuple-element.32), channel_id=1, source_target_pairs={{0,4},{2,6},{4,0},{6,2},{8,12},{10,14},{12,8},{14,10},{1,5},{3,7},... | collective-permute-start | bytes 393224 | tf_op jit(solution)/shard_map/ppermute | solution.py:230
  54.3 5.8 %collective-permute-done.20.refs_2_ = bf16[64,1024]{1,0:T(8,128)(2,1)S(1)} collective-permute-done((bf16[64,1024]{1,0:T(8,128)(2,1)S(1)}, bf16[64,1024]{1,0:T(8,128)(2,1)S(1)}, u32[]{:S(2)}, u32[]{:S(2)}) %collective-permute-start.20) | collective-permute-done | bytes 131104 | tf_op jit(solution)/shard_map/ppermute | solution.py:230
  60.1 0.7 %collective-permute-done.9.refs_1_ = bf16[64,1024]{1,0:T(8,128)(2,1)S(1)} collective-permute-done((bf16[64,1024]{1,0:T(8,128)(2,1)S(1)}, bf16[64,1024]{1,0:T(8,128)(2,1)S(1)}, u32[]{:S(2)}, u32[]{:S(2)}) %collective-permute-start.9) | collective-permute-done | bytes 131104 | tf_op jit(solution)/shard_map/ppermute | solution.py:230
  60.8 0.5 place.1
  61.4 0.1 collective-permute-start.22
  61.4 1.2 %collective-permute-done.22.other_ref = f32[128,128]{1,0:T(8,128)S(1)} collective-permute-done((f32[128,128]{1,0:T(8,128)S(1)}, f32[128,128]{1,0:T(8,128)S(1)}, u32[]{:S(2)}, u32[]{:S(2)}) %collective-permute-start.22) | collective-permute-done | bytes 65568 | tf_op jit(solution)/shard_map/ppermute | solution.py:237
  62.7 0.8 %close.1 = bf16[128,1024]{1,0:T(8,128)(2,1)} custom-call(f32[128,1024]{1,0:T(8,128)S(1)} %get-tuple-element.41.mixed_ref, f32[128,128]{1,0:T(8,128)S(1)} %get-tuple-element.42.mine_ref, f32[128,128]{1,0:T(8,128)S(1)} %collective-permute-done.22.other_ref, f32[1,1024]{1,0:T(1,128)S(1)} %bitcast.3), custom_call_target="tpu_custom_call" | custom-call | flops 131072 | tf_op jit(solution)/shard_map/close/pallas_call | solution.py:205
  (23 shorter events, 0.1 us)
Async XLA Ops:
  1.6 1.0 %copy-start.4 = (bf16[128,2048]{1,0:T(8,128)(2,1)S(1)}, bf16[128,2048]{1,0:T(8,128)(2,1)}, u32[]{:S(2)}) copy-start(bf16[128,2048]{1,0:T(8,128)(2,1)} %tok_ref.1) | copy-start | bytes 1572868
  2.6 0.7 %copy-start.5 = (f32[2048]{0:T(1024)S(1)}, f32[2048]{0:T(1024)}, u32[]{:S(2)}) copy-start(f32[2048]{0:T(1024)} %param.9) | copy-start | bytes 24580
  4.2 14.7 %collective-permute-start.10 = (bf16[32,2176]{1,0:T(8,128)(2,1)S(1)}, bf16[32,2176]{1,0:T(8,128)(2,1)S(1)}, u32[]{:S(2)}, u32[]{:S(2)}) collective-permute-start(bf16[32,2176]{1,0:T(8,128)(2,1)S(1)} %get-tuple-element.33), channel_id=1, source_target_pairs={{0,8},{2,10},{4,12},{6,14},{8,0},{10,2},{12,4},{14,6},{1,9},{3,11}... | collective-permute-start | bytes 417800 | tf_op jit(solution)/shard_map/ppermute | solution.py:230
  8.3 12.3 %collective-permute-start.14 = (bf16[32,2176]{1,0:T(8,128)(2,1)S(1)}, bf16[32,2176]{1,0:T(8,128)(2,1)S(1)}, u32[]{:S(2)}, u32[]{:S(2)}) collective-permute-start(bf16[32,2176]{1,0:T(8,128)(2,1)S(1)} %get-tuple-element.34), channel_id=1, source_target_pairs={{0,12},{2,14},{4,8},{6,10},{8,4},{10,6},{12,0},{14,2},{1,13},{3,15... | collective-permute-start | bytes 417800 | tf_op jit(solution)/shard_map/ppermute | solution.py:230
  9.6 11.2 %collective-permute-start.3 = (bf16[32,2176]{1,0:T(8,128)(2,1)S(1)}, bf16[32,2176]{1,0:T(8,128)(2,1)S(1)}, u32[]{:S(2)}, u32[]{:S(2)}) collective-permute-start(bf16[32,2176]{1,0:T(8,128)(2,1)S(1)} %get-tuple-element.26), channel_id=1, source_target_pairs={{0,4},{2,6},{4,0},{6,2},{8,12},{10,14},{12,8},{14,10},{1,5},{3,7},... | collective-permute-start | bytes 417800 | tf_op jit(solution)/shard_map/ppermute | solution.py:230
  9.9 11.5 %collective-permute-start.1 = (bf16[32,2176]{1,0:T(8,128)(2,1)S(1)}, bf16[32,2176]{1,0:T(8,128)(2,1)S(1)}, u32[]{:S(2)}, u32[]{:S(2)}) collective-permute-start(bf16[32,2176]{1,0:T(8,128)(2,1)S(1)} %get-tuple-element.25.refs_0_), channel_id=1, source_target_pairs={{0,2},{2,0},{4,6},{6,4},{8,10},{10,8},{12,14},{14,12},{1,3},{3,1},... | collective-permute-start | bytes 417800 | tf_op jit(solution)/shard_map/ppermute | solution.py:234
  18.8 5.7 %collective-permute-start.12 = (bf16[32,2176]{1,0:T(8,128)(2,1)S(1)}, bf16[32,2176]{1,0:T(8,128)(2,1)S(1)}, u32[]{:S(2)}, u32[]{:S(2)}) collective-permute-start(bf16[32,2176]{1,0:T(8,128)(2,1)S(1)} %collective-permute-done.10.refs_0_), channel_id=1, source_target_pairs={{0,2},{2,0},{4,6},{6,4},{8,10},{10,8},{12,14},{14,12},{1,3},{3,1},... | collective-permute-start | bytes 417800 | tf_op jit(solution)/shard_map/ppermute | solution.py:234
  20.6 6.7 %collective-permute-start.16 = (bf16[32,2176]{1,0:T(8,128)(2,1)S(1)}, bf16[32,2176]{1,0:T(8,128)(2,1)S(1)}, u32[]{:S(2)}, u32[]{:S(2)}) collective-permute-start(bf16[32,2176]{1,0:T(8,128)(2,1)S(1)} %collective-permute-done.14.refs_4_), channel_id=1, source_target_pairs={{0,2},{2,0},{4,6},{6,4},{8,10},{10,8},{12,14},{14,12},{1,3},{3,1},... | collective-permute-start | bytes 417800 | tf_op jit(solution)/shard_map/ppermute | solution.py:234
  20.9 6.4 %collective-permute-start.11 = (bf16[32,2176]{1,0:T(8,128)(2,1)S(1)}, bf16[32,2176]{1,0:T(8,128)(2,1)S(1)}, u32[]{:S(2)}, u32[]{:S(2)}) collective-permute-start(bf16[32,2176]{1,0:T(8,128)(2,1)S(1)} %collective-permute-done.10.refs_0_), channel_id=1, source_target_pairs={{0,1},{1,0},{2,3},{3,2},{4,5},{5,4},{6,7},{7,6},{8,9},{9,8},{10,11... | collective-permute-start | bytes 417800 | tf_op jit(solution)/shard_map/ppermute | solution.py:237
  20.9 6.9 %collective-permute-start.15 = (bf16[32,2176]{1,0:T(8,128)(2,1)S(1)}, bf16[32,2176]{1,0:T(8,128)(2,1)S(1)}, u32[]{:S(2)}, u32[]{:S(2)}) collective-permute-start(bf16[32,2176]{1,0:T(8,128)(2,1)S(1)} %collective-permute-done.14.refs_4_), channel_id=1, source_target_pairs={{0,1},{1,0},{2,3},{3,2},{4,5},{5,4},{6,7},{7,6},{8,9},{9,8},{10,11... | collective-permute-start | bytes 417800 | tf_op jit(solution)/shard_map/ppermute | solution.py:237
  21.4 7.4 %collective-permute-start.5 = (bf16[32,2176]{1,0:T(8,128)(2,1)S(1)}, bf16[32,2176]{1,0:T(8,128)(2,1)S(1)}, u32[]{:S(2)}, u32[]{:S(2)}) collective-permute-start(bf16[32,2176]{1,0:T(8,128)(2,1)S(1)} %collective-permute-done.3.refs_4_), channel_id=1, source_target_pairs={{0,2},{2,0},{4,6},{6,4},{8,10},{10,8},{12,14},{14,12},{1,3},{3,1},... | collective-permute-start | bytes 417800 | tf_op jit(solution)/shard_map/ppermute | solution.py:234
  24.5 4.3 %collective-permute-start.13 = (bf16[32,2176]{1,0:T(8,128)(2,1)S(1)}, bf16[32,2176]{1,0:T(8,128)(2,1)S(1)}, u32[]{:S(2)}, u32[]{:S(2)}) collective-permute-start(bf16[32,2176]{1,0:T(8,128)(2,1)S(1)} %collective-permute-done.12.refs_2_), channel_id=1, source_target_pairs={{0,1},{1,0},{2,3},{3,2},{4,5},{5,4},{6,7},{7,6},{8,9},{9,8},{10,11... | collective-permute-start | bytes 417800 | tf_op jit(solution)/shard_map/ppermute | solution.py:237
  27.3 2.0 %collective-permute-start.17 = (bf16[32,2176]{1,0:T(8,128)(2,1)S(1)}, bf16[32,2176]{1,0:T(8,128)(2,1)S(1)}, u32[]{:S(2)}, u32[]{:S(2)}) collective-permute-start(bf16[32,2176]{1,0:T(8,128)(2,1)S(1)} %collective-permute-done.16.refs_6_), channel_id=1, source_target_pairs={{0,1},{1,0},{2,3},{3,2},{4,5},{5,4},{6,7},{7,6},{8,9},{9,8},{10,11... | collective-permute-start | bytes 417800 | tf_op jit(solution)/shard_map/ppermute | solution.py:237
  27.3 8.8 %collective-permute-start = (bf16[32,2176]{1,0:T(8,128)(2,1)S(1)}, bf16[32,2176]{1,0:T(8,128)(2,1)S(1)}, u32[]{:S(2)}, u32[]{:S(2)}) collective-permute-start(bf16[32,2176]{1,0:T(8,128)(2,1)S(1)} %get-tuple-element.25.refs_0_), channel_id=1, source_target_pairs={{0,1},{1,0},{2,3},{3,2},{4,5},{5,4},{6,7},{7,6},{8,9},{9,8},{10,11... | collective-permute-start | bytes 417800 | tf_op jit(solution)/shard_map/ppermute | solution.py:237
  27.8 8.3 %collective-permute-start.4 = (bf16[32,2176]{1,0:T(8,128)(2,1)S(1)}, bf16[32,2176]{1,0:T(8,128)(2,1)S(1)}, u32[]{:S(2)}, u32[]{:S(2)}) collective-permute-start(bf16[32,2176]{1,0:T(8,128)(2,1)S(1)} %collective-permute-done.3.refs_4_), channel_id=1, source_target_pairs={{0,1},{1,0},{2,3},{3,2},{4,5},{5,4},{6,7},{7,6},{8,9},{9,8},{10,11... | collective-permute-start | bytes 417800 | tf_op jit(solution)/shard_map/ppermute | solution.py:237
  28.8 7.3 %collective-permute-start.2 = (bf16[32,2176]{1,0:T(8,128)(2,1)S(1)}, bf16[32,2176]{1,0:T(8,128)(2,1)S(1)}, u32[]{:S(2)}, u32[]{:S(2)}) collective-permute-start(bf16[32,2176]{1,0:T(8,128)(2,1)S(1)} %collective-permute-done.1.refs_2_), channel_id=1, source_target_pairs={{0,1},{1,0},{2,3},{3,2},{4,5},{5,4},{6,7},{7,6},{8,9},{9,8},{10,11... | collective-permute-start | bytes 417800 | tf_op jit(solution)/shard_map/ppermute | solution.py:237
  28.8 7.4 %collective-permute-start.6 = (bf16[32,2176]{1,0:T(8,128)(2,1)S(1)}, bf16[32,2176]{1,0:T(8,128)(2,1)S(1)}, u32[]{:S(2)}, u32[]{:S(2)}) collective-permute-start(bf16[32,2176]{1,0:T(8,128)(2,1)S(1)} %collective-permute-done.5.refs_6_), channel_id=1, source_target_pairs={{0,1},{1,0},{2,3},{3,2},{4,5},{5,4},{6,7},{7,6},{8,9},{9,8},{10,11... | collective-permute-start | bytes 417800 | tf_op jit(solution)/shard_map/ppermute | solution.py:237
  29.3 1.6 %copy-start = (bf16[2,2048,256]{2,1,0:T(8,128)(2,1)S(1)}, bf16[2,2048,256]{2,1,0:T(8,128)(2,1)}, u32[]{:S(2)}) copy-start(bf16[2,2048,256]{2,1,0:T(8,128)(2,1)} %refs_8_.3) | copy-start | bytes 6291460
  30.9 1.6 %copy-start.2 = (bf16[2,2048,256]{2,1,0:T(8,128)(2,1)S(1)}, bf16[2,2048,256]{2,1,0:T(8,128)(2,1)}, u32[]{:S(2)}) copy-start(bf16[2,2048,256]{2,1,0:T(8,128)(2,1)} %refs_9_.3) | copy-start | bytes 6291460
  32.5 1.6 %copy-start.3 = (bf16[2,256,2048]{2,1,0:T(8,128)(2,1)S(1)}, bf16[2,256,2048]{2,1,0:T(8,128)(2,1)}, u32[]{:S(2)}) copy-start(bf16[2,256,2048]{2,1,0:T(8,128)(2,1)} %refs_10_.3) | copy-start | bytes 6291460
  34.1 2.1 %copy-start.1 = (bf16[2,2048,256]{2,1,0:T(8,128)(2,1)S(1)}, bf16[2,2048,256]{2,1,0:T(8,128)(2,1)}, u32[]{:S(2)}) copy-start(bf16[2,2048,256]{2,1,0:T(8,128)(2,1)} %refs_8_.3) | copy-start | bytes 6291460
  36.0 2.6 %collective-permute-start.18 = (bf16[256,1024]{1,0:T(8,128)(2,1)S(1)}, bf16[256,1024]{1,0:T(8,128)(2,1)S(1)}, u32[]{:S(2)}, u32[]{:S(2)}) collective-permute-start(bf16[256,1024]{1,0:T(8,128)(2,1)S(1)} %get-tuple-element.36), channel_id=1, source_target_pairs={{0,1},{1,0},{2,3},{3,2},{4,5},{5,4},{6,7},{7,6},{8,9},{9,8},{10,11... | collective-permute-start | bytes 1572872 | tf_op jit(solution)/shard_map/ppermute | solution.py:237
  38.1 2.1 %collective-permute-start.7 = (bf16[256,1024]{1,0:T(8,128)(2,1)S(1)}, bf16[256,1024]{1,0:T(8,128)(2,1)S(1)}, u32[]{:S(2)}, u32[]{:S(2)}) collective-permute-start(bf16[256,1024]{1,0:T(8,128)(2,1)S(1)} %get-tuple-element.28), channel_id=1, source_target_pairs={{0,1},{1,0},{2,3},{3,2},{4,5},{5,4},{6,7},{7,6},{8,9},{9,8},{10,11... | collective-permute-start | bytes 1572872 | tf_op jit(solution)/shard_map/ppermute | solution.py:237
  38.8 23.9 %copy-start.6 = (f32[1024]{0:T(1024)S(1)}, f32[1024]{0:T(1024)}, u32[]{:S(2)}) copy-start(f32[1024]{0:T(1024)} %param.15) | copy-start | bytes 12292
  38.8 9.2 %collective-permute-start.19 = (bf16[128,1024]{1,0:T(8,128)(2,1)S(1)}, bf16[128,1024]{1,0:T(8,128)(2,1)S(1)}, u32[]{:S(2)}, u32[]{:S(2)}) collective-permute-start(bf16[128,1024]{1,0:T(8,128)(2,1)S(1)} %get-tuple-element.38), channel_id=1, source_target_pairs={{0,2},{2,0},{4,6},{6,4},{8,10},{10,8},{12,14},{14,12},{1,3},{3,1},... | collective-permute-start | bytes 786440 | tf_op jit(solution)/shard_map/ppermute | solution.py:234
  40.3 12.4 %collective-permute-start.8 = (bf16[128,1024]{1,0:T(8,128)(2,1)S(1)}, bf16[128,1024]{1,0:T(8,128)(2,1)S(1)}, u32[]{:S(2)}, u32[]{:S(2)}) collective-permute-start(bf16[128,1024]{1,0:T(8,128)(2,1)S(1)} %get-tuple-element.30), channel_id=1, source_target_pairs={{0,2},{2,0},{4,6},{6,4},{8,10},{10,8},{12,14},{14,12},{1,3},{3,1},... | collective-permute-start | bytes 786440 | tf_op jit(solution)/shard_map/ppermute | solution.py:234
  48.1 12.0 %collective-permute-start.20 = (bf16[64,1024]{1,0:T(8,128)(2,1)S(1)}, bf16[64,1024]{1,0:T(8,128)(2,1)S(1)}, u32[]{:S(2)}, u32[]{:S(2)}) collective-permute-start(bf16[64,1024]{1,0:T(8,128)(2,1)S(1)} %get-tuple-element.39), channel_id=1, source_target_pairs={{0,8},{2,10},{4,12},{6,14},{8,0},{10,2},{12,4},{14,6},{1,9},{3,11}... | collective-permute-start | bytes 393224 | tf_op jit(solution)/shard_map/ppermute | solution.py:230
  51.5 8.6 %collective-permute-start.21 = (bf16[64,1024]{1,0:T(8,128)(2,1)S(1)}, bf16[64,1024]{1,0:T(8,128)(2,1)S(1)}, u32[]{:S(2)}, u32[]{:S(2)}) collective-permute-start(bf16[64,1024]{1,0:T(8,128)(2,1)S(1)} %get-tuple-element.40), channel_id=1, source_target_pairs={{0,12},{2,14},{4,8},{6,10},{8,4},{10,6},{12,0},{14,2},{1,13},{3,15... | collective-permute-start | bytes 393224 | tf_op jit(solution)/shard_map/ppermute | solution.py:230
  52.8 8.1 %collective-permute-start.9 = (bf16[64,1024]{1,0:T(8,128)(2,1)S(1)}, bf16[64,1024]{1,0:T(8,128)(2,1)S(1)}, u32[]{:S(2)}, u32[]{:S(2)}) collective-permute-start(bf16[64,1024]{1,0:T(8,128)(2,1)S(1)} %get-tuple-element.32), channel_id=1, source_target_pairs={{0,4},{2,6},{4,0},{6,2},{8,12},{10,14},{12,8},{14,10},{1,5},{3,7},... | collective-permute-start | bytes 393224 | tf_op jit(solution)/shard_map/ppermute | solution.py:230
  61.4 1.3 %collective-permute-start.22 = (f32[128,128]{1,0:T(8,128)S(1)}, f32[128,128]{1,0:T(8,128)S(1)}, u32[]{:S(2)}, u32[]{:S(2)}) collective-permute-start(f32[128,128]{1,0:T(8,128)S(1)} %get-tuple-element.42.mine_ref), channel_id=1, source_target_pairs={{0,1},{1,0},{2,3},{3,2},{4,5},{5,4},{6,7},{7,6},{8,9},{9,8},{10,11... | collective-permute-start | bytes 196616 | tf_op jit(solution)/shard_map/ppermute | solution.py:237

commit v2 on v1

v2 whole, which is shorter than its diff:
```python
import functools

import jax
import jax.numpy as jnp
from jax import lax
from jax.experimental import pallas as pl
from jax.experimental.pallas import tpu as pltpu
from jax.sharding import PartitionSpec as P

GROUPS = 4


EPS = 1e-06
LANES = 128
TERMS = 3
MIB = 1 << 20


def slot_ranks(flat_routes, expert_count):
    matches = (flat_routes[:, None] == jnp.arange(expert_count, dtype=jnp.int32)[None, :]).astype(
        jnp.int32
    )
    earlier = jnp.cumsum(matches, axis=0) - matches
    return jnp.sum(earlier * matches, axis=1)


def fill_rows(source, entries):
    filled = entries > 0
    return jnp.where(
        filled[:, None], source[jnp.maximum(entries - 1, 0)], jnp.zeros((), source.dtype)
    )


def sparse_body(tokens, in_gain, routing, gate_prob, w_gate, w_up, w_down, out_gain):
    ep_count = lax.axis_size("ep")
    local_experts = w_gate.shape[0]
    expert_count = local_experts * ep_count
    tok_dev, top_count = routing.shape
    model_width = tokens.shape[1]
    half_width = out_gain.shape[0]
    group_width = expert_count // GROUPS
    row_cap = max(2, tok_dev * top_count // (2 * group_width))
    floats = tokens.astype(jnp.float32)
    normed = (
        floats * lax.rsqrt(jnp.mean(floats * floats, axis=-1, keepdims=True) + EPS) * in_gain
    ).astype(jnp.bfloat16)
    flat_routes = routing.reshape(-1)
    slot_rank = slot_ranks(flat_routes, expert_count)
    slot_ids = flat_routes * row_cap + slot_rank
    token_ids = jnp.arange(tok_dev * top_count, dtype=jnp.int32) // top_count
    slot_table = jnp.zeros((expert_count * row_cap,), jnp.int32).at[slot_ids].set(token_ids + 1)
    own_columns = lax.dynamic_slice_in_dim(normed, lax.axis_index("tp") * half_width, half_width, 1)
    sendbuf = fill_rows(own_columns, slot_table).reshape(
        ep_count, local_experts, row_cap, half_width
    )
    arrived = lax.all_to_all(sendbuf, "ep", split_axis=0, concat_axis=0, tiled=True)
    arrived = lax.all_gather(arrived, "tp", axis=3, tiled=True)
    gate_act = jnp.einsum("secd,edf->secf", arrived, w_gate, preferred_element_type=jnp.float32)
    up_act = jnp.einsum("secd,edf->secf", arrived, w_up, preferred_element_type=jnp.float32)
    hidden = (jax.nn.silu(gate_act) * up_act).astype(jnp.bfloat16)
    partial_out = jnp.einsum("secf,efd->secd", hidden, w_down, preferred_element_type=jnp.float32)
    results = lax.psum_scatter(
        partial_out.astype(jnp.bfloat16), "tp", scatter_dimension=3, tiled=True
    )
    returned = lax.all_to_all(results, "ep", split_axis=0, concat_axis=0, tiled=True).reshape(
        expert_count * row_cap, half_width
    )
    picked = returned[slot_ids].astype(jnp.float32).reshape(tok_dev, top_count, half_width)
    mixed_rows = jnp.sum(picked * gate_prob[:, :, None], axis=1)
    squares = jnp.sum(mixed_rows * mixed_rows, axis=1)
    total_squares = lax.psum(squares, "tp")
    inv_rms = lax.rsqrt(total_squares / model_width + EPS)
    return (mixed_rows * inv_rms[:, None] * out_gain).astype(jnp.bfloat16)


def dot(a, b):
    return jnp.dot(a, b, preferred_element_type=jnp.float32)


def iota(shape, dim):
    return lax.broadcasted_iota(jnp.int32, shape, dim)


def pack_kernel(members, width, cap, *refs):
    sources, refs = refs[:4], refs[4:]
    outs, map_ref, refs = refs[:GROUPS], refs[GROUPS], refs[GROUPS + 1 :]
    copies = [
        pltpu.make_async_copy(source, target, refs[4].at[i])
        for i, (source, target) in enumerate(zip(sources, refs[:4]))
    ]
    for copy in copies:
        copy.start()
    tok_ref, gain_ref, route_ref, prob_ref = refs[:4]
    half = cap // 2
    my_group = lax.axis_index("ep") // members
    my_half = lax.axis_index("tp")
    tok_dev, model_width = tok_ref.shape
    copies[2].wait()
    copies[3].wait()
    routes = route_ref[...]
    probs = prob_ref[...]
    first = routes[0:1]
    group = jnp.zeros_like(first)
    for g in range(1, GROUPS):
        group += (first >= g * width).astype(jnp.int32)
    member = (group == iota((8, tok_dev), 0)).astype(jnp.float32)
    before = (iota((tok_dev, tok_dev), 0) < iota((tok_dev, tok_dev), 1)).astype(jnp.bfloat16)
    earlier = dot(member.astype(jnp.bfloat16), before)
    rank = jnp.sum(earlier * member, axis=0, keepdims=True).astype(jnp.int32)
    relative = group ^ my_group
    send_slot = iota((GROUPS * half, tok_dev), 0)
    pick = (
        (relative == send_slot // half) & (rank == send_slot % half + my_half * half)
    ).astype(jnp.bfloat16)
    lane = iota((LANES, tok_dev), 0)
    weight = jnp.zeros((LANES, tok_dev), jnp.float32)
    for k in range(routes.shape[0]):
        weight += jnp.where(
            routes[k : k + 1] - group * width == lane % width, probs[k : k + 1], 0.0
        )
    high = weight.astype(jnp.bfloat16).astype(jnp.float32)
    rest = weight - high
    middle = rest.astype(jnp.bfloat16).astype(jnp.float32)
    low = rest - middle
    terms = jnp.where(
        lane < width,
        high,
        jnp.where(lane < 2 * width, middle, jnp.where(lane < TERMS * width, low, 0.0)),
    ).astype(jnp.bfloat16)
    extra = lax.dot_general(
        pick, terms, (((1,), (1,)), ((), ())), preferred_element_type=jnp.float32
    ).astype(jnp.bfloat16)
    map_ref[...] = (relative * cap + rank == iota((GROUPS * cap, tok_dev), 0)).astype(jnp.bfloat16)
    copies[0].wait()
    copies[1].wait()
    floats = tok_ref[...].astype(jnp.float32)
    inv = lax.rsqrt(jnp.sum(floats * floats, axis=-1, keepdims=True) / model_width + EPS)
    normed = (floats * inv * gain_ref[...]).astype(jnp.bfloat16)
    rows = dot(pick, normed).astype(jnp.bfloat16)
    for k in range(GROUPS):
        outs[k][:, :model_width] = rows[k * half : (k + 1) * half]
        outs[k][:, model_width:] = extra[k * half : (k + 1) * half]


def load_kernel(wg_ref, wu_ref, wd_ref, map_ref, wg_out, wu_out, wd_out, map_out, sems):
    copies = [
        pltpu.make_async_copy(source.at[e], target.at[e], sems.at[i, e])
        for i, (source, target) in enumerate(
            ((wg_ref, wg_out), (wu_ref, wu_out), (wd_ref, wd_out))
        )
        for e in range(wg_ref.shape[0])
    ]
    for copy in copies:
        copy.start()
    map_out[...] = map_ref[...].astype(jnp.float32).T.astype(jnp.bfloat16)
    for copy in copies:
        copy.wait()


def expert_kernel(chunks, members, width, half, *refs):
    pieces = refs[: 4 * chunks]
    wg_ref, wu_ref, wd_ref, keep_ref, send_ref, rows_ref = refs[4 * chunks :]
    my_half = lax.axis_index("tp")
    me = lax.axis_index("ep") % members
    local_experts, model_width, _ = wg_ref.shape
    half_width = keep_ref.shape[1]
    mine = pl.multiple_of(my_half * half, half)
    other = pl.multiple_of((1 - my_half) * half, half)
    for c in range(chunks):
        own, own_tp, far, far_tp = pieces[4 * c : 4 * c + 4]
        near_base = c * 4 * half
        far_base = near_base + 2 * half
        rows_ref[pl.ds(near_base + mine, half), :] = own[...]
        rows_ref[pl.ds(near_base + other, half), :] = own_tp[...]
        rows_ref[pl.ds(far_base + mine, half), :] = far[...]
        rows_ref[pl.ds(far_base + other, half), :] = far_tp[...]
    rows = rows_ref[:, :model_width]
    terms = rows_ref[:, model_width:].astype(jnp.float32)
    lane = lax.broadcasted_iota(jnp.int32, terms.shape, 1)
    hidden = []
    for e in range(local_experts):
        wanted = (lane % width == me * local_experts + e) & (lane < TERMS * width)
        weight = jnp.sum(jnp.where(wanted, terms, 0.0), axis=1, keepdims=True)
        gate_act = dot(rows, wg_ref[e])
        up_act = dot(rows, wu_ref[e])
        act = gate_act / (1.0 + jnp.exp(-gate_act)) * up_act
        hidden.append((act * weight).astype(jnp.bfloat16))
    send_at = pl.multiple_of((1 - my_half) * half_width, half_width)
    keep_at = pl.multiple_of(my_half * half_width, half_width)
    total = dot(hidden[0], wd_ref[0, :, pl.ds(send_at, half_width)])
    for e in range(1, local_experts):
        total += dot(hidden[e], wd_ref[e, :, pl.ds(send_at, half_width)])
    send_ref[...] = total.astype(jnp.bfloat16)
    total = dot(hidden[0], wd_ref[0, :, pl.ds(keep_at, half_width)])
    for e in range(1, local_experts):
        total += dot(hidden[e], wd_ref[e, :, pl.ds(keep_at, half_width)])
    keep_ref[...] = total


def split_kernel(chunks, cap, mine_ref, recv_ref, *outs):
    for c in range(chunks):
        near = pl.ds(2 * c * cap, cap)
        far = pl.ds((2 * c + 1) * cap, cap)
        keep_ref, send_ref = outs[2 * c : 2 * c + 2]
        keep_ref[...] = mine_ref[near, :] + recv_ref[near, :].astype(jnp.float32)
        send_ref[...] = (mine_ref[far, :] + recv_ref[far, :].astype(jnp.float32)).astype(
            jnp.bfloat16
        )


def join_kernel(keep_ref, recv_ref, row_ref, square_ref):
    rows = keep_ref[...] + recv_ref[...].astype(jnp.float32)
    row_ref[...] = rows.astype(jnp.bfloat16)
    squares = jnp.sum(rows * rows, axis=1, keepdims=True)
    square_ref[...] = jnp.broadcast_to(squares, (rows.shape[0], LANES)).T[:8]


def close_kernel(cap, model_width, map_ref, gain_ref, *refs):
    parts, squares = refs[:GROUPS], refs[GROUPS : 2 * GROUPS]
    out_ref, rows_ref = refs[2 * GROUPS :]
    for k in range(GROUPS):
        rows_ref[k * cap : (k + 1) * cap, :] = parts[k][...]
    placing = map_ref[...]
    mixed = dot(placing, rows_ref[...])
    far = jnp.concatenate([square[0:1, :] for square in squares], axis=1)
    total = jnp.sum(mixed * mixed, axis=1, keepdims=True) + jnp.sum(
        placing.astype(jnp.float32) * far, axis=1, keepdims=True
    )
    out_ref[...] = (mixed * lax.rsqrt(total / model_width + EPS) * gain_ref[...]).astype(
        jnp.bfloat16
    )


def call(kernel, outs, args, limit, scratch=(), in_specs=None):
    return pl.pallas_call(
        kernel,
        out_shape=outs,
        in_specs=in_specs or [pl.BlockSpec(memory_space=pltpu.VMEM)] * len(args),
        scratch_shapes=scratch,
        compiler_params=pltpu.CompilerParams(vmem_limit_bytes=limit * MIB),
    )(*args)


def dense_body(tokens, in_gain, routing, gate_prob, w_gate, w_up, w_down, out_gain):
    ep_count = lax.axis_size("ep")
    local_experts, model_width, _ = w_gate.shape
    tok_dev, top_count = routing.shape
    half_width = out_gain.shape[0]
    width = local_experts * ep_count // GROUPS
    members = width // local_experts
    cap = tok_dev * top_count // (2 * width)
    half = cap // 2
    sds = jax.ShapeDtypeStruct
    bf16, f32 = jnp.bfloat16, jnp.float32
    block = sds((half, model_width + LANES), bf16)
    anywhere = pl.BlockSpec(memory_space=pltpu.HBM)
    in_vmem = pl.BlockSpec(memory_space=pltpu.VMEM)

    def far_ep(i, k):
        return ((i // members) ^ k) * members + i % members

    def hop(value, k):
        return lax.ppermute(value, "ep", [(i, far_ep(i, k)) for i in range(ep_count)])

    def hop_swap(value, k):
        pairs = [
            (2 * i + t, 2 * far_ep(i, k) + 1 - t) for i in range(ep_count) for t in range(2)
        ]
        return lax.ppermute(value, ("ep", "tp"), pairs)

    def cross(value):
        return lax.ppermute(value, "ep", [(i, i ^ 1) for i in range(ep_count)])

    def swap(value):
        return lax.ppermute(value, "tp", [(0, 1), (1, 0)])

    def held(value):
        return pltpu.with_memory_space_constraint(value, pltpu.HBM)

    routes_t, probs_t = held(routing.T), held(gate_prob.T)
    tokens, gain_row = held(tokens), held(in_gain.reshape(1, -1))
    w_gate, w_up, w_down = held(w_gate), held(w_up), held(w_down)
    *packed, slot_map = call(
        functools.partial(pack_kernel, members, width, cap),
        [block] * GROUPS + [sds((GROUPS * cap, tok_dev), bf16)],
        (tokens, gain_row, routes_t, probs_t),
        12,
        (
            pltpu.VMEM(tokens.shape, bf16),
            pltpu.VMEM((1, model_width), f32),
            pltpu.VMEM(routes_t.shape, jnp.int32),
            pltpu.VMEM(probs_t.shape, f32),
            pltpu.SemaphoreType.DMA((4,)),
        ),
        [anywhere] * 4,
    )
    *weights, token_map = call(
        load_kernel,
        [sds(w.shape, bf16) for w in (w_gate, w_up, w_down)]
        + [sds((tok_dev, GROUPS * cap), bf16)],
        (w_gate, w_up, w_down, slot_map),
        12,
        (pltpu.SemaphoreType.DMA((3, local_experts)),),
        [anywhere] * 3 + [in_vmem],
    )
    arrived = [packed[0]] + [hop(packed[k], k) for k in range(1, GROUPS)]

    back, squares = [None] * GROUPS, [None] * GROUPS

    def experts(ks):
        pieces = []
        for k in ks:
            far = cross(arrived[k])
            pieces += [arrived[k], swap(arrived[k]), far, swap(far)]
        n = len(ks)
        rows = n * 2 * cap
        mine, other = call(
            functools.partial(expert_kernel, n, members, width, half),
            [sds((rows, half_width), f32), sds((rows, half_width), bf16)],
            (*pieces, *weights),
            24,
            (pltpu.VMEM((rows, model_width + LANES), bf16),),
        )
        split = call(
            functools.partial(split_kernel, n, cap),
            [sds((cap, half_width), f32), sds((cap, half_width), bf16)] * n,
            (mine, swap(other)),
            8,
        )
        for c, k in enumerate(ks):
            keep, send = split[2 * c : 2 * c + 2]
            rows_out, square = call(
                join_kernel,
                [sds((cap, half_width), bf16), sds((8, cap), f32)],
                (keep, cross(send)),
                8,
            )
            if k == 0:
                back[k], squares[k] = rows_out, swap(square)
            else:
                back[k] = hop(rows_out, k)
                squares[k] = hop_swap(square, k)

    for ks in STAGES:
        experts(ks)
    return call(
        functools.partial(close_kernel, cap, model_width),
        sds((tok_dev, half_width), bf16),
        (token_map, out_gain.reshape(1, -1), *back, *squares),
        8,
        (pltpu.VMEM((GROUPS * cap, half_width), bf16),),
    )


STAGES = ((0, 1), (3,), (2,))


def solution(mesh):
    placed = (
        P(("grp", "ep"), None),
        P(),
        P(("grp", "ep"), None),
        P(("grp", "ep"), None),
        P("ep", None, "tp"),
        P("ep", None, "tp"),
        P("ep", "tp", None),
        P("tp"),
    )

    def step(*args):
        routing, w_gate = args[2], args[4]
        width = w_gate.shape[0] // GROUPS
        members = mesh.shape["ep"] // GROUPS
        dense = routing.shape[1] == width and members == 2 and mesh.shape["tp"] == 2

        def body(*shards):
            return (dense_body if dense else sparse_body)(*shards)

        whole = jax.shard_map(
            body, mesh=mesh, in_specs=placed, out_specs=P(("grp", "ep"), "tp"), check_vma=False
        )
        return whole(*args)

    return step
```

time: 63.9 us -> 54.4 us (0.85)
  waiting for transfers between devices: 26.8 us -> 12.7 us
  starting transfers between devices: 22.1 us -> 30.4 us
  local copies, waits for them, and re-layouts: 8.09 us -> 0.01 us
  Pallas kernels: 6.39 us -> 10.8 us
    ppermute x12 -> x17, waiting for transfers between devices: 25.5 us -> 12.1 us  [the longest x8 4.61 us: cross(): return lax.ppermute(value, 'ep', [(i, i ^ 1) for i in range(ep_count)])]
    ppermute x12 -> x17, starting transfers between devices: 19.8 us -> 28.1 us  [the longest x6 14 us: hop(): lax.ppermute(value, 'ep', [(i, far_ep(i, k)) for i in range(ep_count)])]
    unnamed x16 -> x2, local copies, waits for them, and re-layouts: 8.09 us -> 0.01 us
    pallas_call x9 -> x13, Pallas kernels: 6.39 us -> 10.8 us  [call(): pl.pallas_call(kernel, out_shape=outs, in_specs=in_specs or [pl.BlockSpec...]
    ppermute x11 -> x12, waiting for transfers between devices: 1.27 us -> 0.61 us  [swap(): return lax.ppermute(value, 'tp', [(0, 1), (1, 0)])]
    ppermute x11 -> x12, starting transfers between devices: 2.29 us -> 2.33 us  [swap(): return lax.ppermute(value, 'tp', [(0, 1), (1, 0)])]
  transfers between devices with their start and end apart: 23 -> 29, of which waited for: 9 -> 11; matrix products, arithmetic and copies ran while one was open for 0% -> 0% of each run, Pallas kernels for 7% -> 15%
where the time goes in v2:
time: 54.4 us; the launch traced here: 54.1 us
  starting transfers between devices  30.4 us (56%)
  waiting for transfers between devices  12.7 us (23%)
  Pallas kernels  10.8 us (20%)
    ppermute x6, starting transfers between devices, hop(): lax.ppermute(value, 'ep', [(i, far_ep(i, k)) for i in range(ep_count)])  14 us
    ppermute x8, starting transfers between devices, cross(): return lax.ppermute(value, 'ep', [(i, i ^ 1) for i in range(ep_count)])  11.1 us
    pallas_call x13, Pallas kernels, call(): pl.pallas_call(kernel, out_shape=outs, in_specs=in_specs or [pl.BlockSpec...  10.8 us
    ppermute x8, waiting for transfers between devices, cross(): return lax.ppermute(value, 'ep', [(i, i ^ 1) for i in range(ep_count)])  4.61 us
    ppermute x3, waiting for transfers between devices, hop_swap(): return lax.ppermute(value, ('ep', 'tp'), pairs)  4.13 us
    ppermute x6, waiting for transfers between devices, hop(): lax.ppermute(value, 'ep', [(i, far_ep(i, k)) for i in range(ep_count)])  3.4 us
    ppermute x3, starting transfers between devices, hop_swap(): return lax.ppermute(value, ('ep', 'tp'), pairs)  2.96 us
    ppermute x12, starting transfers between devices, swap(): return lax.ppermute(value, 'tp', [(0, 1), (1, 0)])  2.33 us
  transfers between devices with their start and end apart: 29, of which 11 were waited for; matrix products, arithmetic and copies ran while one was open for 0% of the time, Pallas kernels for 15%

profile of v2, /device:TPU:0, one launch (start us, length us, event | category | flops | bytes accessed | tf_op | source)
XLA Modules:
  0.0 54.1 jit_solution(5093400040343501051)
XLA Ops:
  0.0 1.7 %shard_map.82 = (bf16[32,2176]{1,0:T(8,128)(2,1)S(1)}, bf16[32,2176]{1,0:T(8,128)(2,1)S(1)}, bf16[32,2176]{1,0:T(8,128)(2,1)S(1)}, bf16[32,2176]{1,0:T(8,128)(2,1)S(1)}, bf16[256,128]{1,0:T(8,128)(2,1)S(1)}) custom-call(bf16[128,2048]{1,0:T(8,128)(2,1)} %refs_0_.1, f32[1,2048]{1,0:T(1,128)} %bitcast.5, s32[4,128]{1,0:T(4,128)} %bitcast.6, f32[4,128]{1,0:T(4,128)} %bitcast.7), custom_call_target="tpu_custom_call" | custom-call | tf_op jit(solution)/shard_map/pallas_call | solution.py:235
  1.7 3.1 %collective-permute-start.3 = (bf16[32,2176]{1,0:T(8,128)(2,1)S(1)}, bf16[32,2176]{1,0:T(8,128)(2,1)S(1)}, u32[]{:S(2)}, u32[]{:S(2)}) collective-permute-start(bf16[32,2176]{1,0:T(8,128)(2,1)S(1)} %get-tuple-element.39), channel_id=1, source_target_pairs={{0,4},{2,6},{4,0},{6,2},{8,12},{10,14},{12,8},{14,10},{1,5},{3,7},... | collective-permute-start | bytes 417800 | tf_op jit(solution)/shard_map/ppermute | solution.py:263
  4.8 2.5 %collective-permute-start.18 = (bf16[32,2176]{1,0:T(8,128)(2,1)S(1)}, bf16[32,2176]{1,0:T(8,128)(2,1)S(1)}, u32[]{:S(2)}, u32[]{:S(2)}) collective-permute-start(bf16[32,2176]{1,0:T(8,128)(2,1)S(1)} %get-tuple-element.57), channel_id=1, source_target_pairs={{0,12},{2,14},{4,8},{6,10},{8,4},{10,6},{12,0},{14,2},{1,13},{3,15... | collective-permute-start | bytes 417800 | tf_op jit(solution)/shard_map/ppermute | solution.py:263
  7.3 1.5 %collective-permute-start.1 = (bf16[32,2176]{1,0:T(8,128)(2,1)S(1)}, bf16[32,2176]{1,0:T(8,128)(2,1)S(1)}, u32[]{:S(2)}, u32[]{:S(2)}) collective-permute-start(bf16[32,2176]{1,0:T(8,128)(2,1)S(1)} %get-tuple-element.38.refs_0_), channel_id=1, source_target_pairs={{0,2},{2,0},{4,6},{6,4},{8,10},{10,8},{12,14},{14,12},{1,3},{3,1},... | collective-permute-start | bytes 417800 | tf_op jit(solution)/shard_map/ppermute | solution.py:272
  8.8 1.4 %collective-permute-start.5 = (bf16[32,2176]{1,0:T(8,128)(2,1)S(1)}, bf16[32,2176]{1,0:T(8,128)(2,1)S(1)}, u32[]{:S(2)}, u32[]{:S(2)}) collective-permute-start(bf16[32,2176]{1,0:T(8,128)(2,1)S(1)} %collective-permute-done.3.refs_4_), channel_id=1, source_target_pairs={{0,2},{2,0},{4,6},{6,4},{8,10},{10,8},{12,14},{14,12},{1,3},{3,1},... | collective-permute-start | bytes 417800 | tf_op jit(solution)/shard_map/ppermute | solution.py:272
  10.1 3.7 %collective-permute-start.11 = (bf16[32,2176]{1,0:T(8,128)(2,1)S(1)}, bf16[32,2176]{1,0:T(8,128)(2,1)S(1)}, u32[]{:S(2)}, u32[]{:S(2)}) collective-permute-start(bf16[32,2176]{1,0:T(8,128)(2,1)S(1)} %get-tuple-element.51), channel_id=1, source_target_pairs={{0,8},{2,10},{4,12},{6,14},{8,0},{10,2},{12,4},{14,6},{1,9},{3,11}... | collective-permute-start | bytes 417800 | tf_op jit(solution)/shard_map/ppermute | solution.py:263
  13.8 0.3 collective-permute-done.18.refs_0_
  14.1 0.3 collective-permute-start.4
  14.4 0.3 collective-permute-start.2
  14.6 0.5 collective-permute-done.5.refs_6_
  15.1 3.1 %collective-permute-done.11.refs_0_ = bf16[32,2176]{1,0:T(8,128)(2,1)S(1)} collective-permute-done((bf16[32,2176]{1,0:T(8,128)(2,1)S(1)}, bf16[32,2176]{1,0:T(8,128)(2,1)S(1)}, u32[]{:S(2)}, u32[]{:S(2)}) %collective-permute-start.11) | collective-permute-done | bytes 139296 | tf_op jit(solution)/shard_map/ppermute | solution.py:263
  18.2 3.0 %collective-permute-start.20 = (bf16[32,2176]{1,0:T(8,128)(2,1)S(1)}, bf16[32,2176]{1,0:T(8,128)(2,1)S(1)}, u32[]{:S(2)}, u32[]{:S(2)}) collective-permute-start(bf16[32,2176]{1,0:T(8,128)(2,1)S(1)} %collective-permute-done.18.refs_0_), channel_id=1, source_target_pairs={{0,2},{2,0},{4,6},{6,4},{8,10},{10,8},{12,14},{14,12},{1,3},{3,1},... | collective-permute-start | bytes 417800 | tf_op jit(solution)/shard_map/ppermute | solution.py:272
  21.2 0.0 collective-permute-start.13
  21.2 2.9 %shard_map.83 = (bf16[2,2048,256]{2,1,0:T(8,128)(2,1)S(1)}, bf16[2,2048,256]{2,1,0:T(8,128)(2,1)S(1)}, bf16[2,256,2048]{2,1,0:T(8,128)(2,1)S(1)}, bf16[128,256]{1,0:T(8,128)(2,1)S(1)}) custom-call(bf16[2,2048,256]{2,1,0:T(8,128)(2,1)} %wg_ref.1, bf16[2,2048,256]{2,1,0:T(8,128)(2,1)} %wu_ref.1, bf16[2,256,2048]{2,1,0:T(8,128)(2,1)} %wd_ref.1, ...), custom_call_target="tpu_custom_call" | custom-call | tf_op jit(solution)/shard_map/pallas_call | solution.py:235
  24.1 2.0 %shard_map.84 = (f32[256,1024]{1,0:T(8,128)S(1)}, bf16[256,1024]{1,0:T(8,128)(2,1)S(1)}) custom-call(bf16[32,2176]{1,0:T(8,128)(2,1)S(1)} %get-tuple-element.38.refs_0_, bf16[32,2176]{1,0:T(8,128)(2,1)S(1)} %collective-permute-done.refs_1_, bf16[32,2176]{1,0:T(8,128)(2,1)S(1)} %collective-permute-done.1.refs_2_, ...), custom_call_target="tpu_custom_call" | custom-call | tf_op jit(solution)/shard_map/pallas_call | solution.py:235
  26.1 0.1 collective-permute-start.7
  26.2 0.5 collective-permute-start.19
  26.7 0.1 collective-permute-start.21
  26.8 0.4 collective-permute-start.12
  27.2 0.7 %collective-permute-done.13.refs_2_ = bf16[32,2176]{1,0:T(8,128)(2,1)S(1)} collective-permute-done((bf16[32,2176]{1,0:T(8,128)(2,1)S(1)}, bf16[32,2176]{1,0:T(8,128)(2,1)S(1)}, u32[]{:S(2)}, u32[]{:S(2)}) %collective-permute-start.13) | collective-permute-done | bytes 139296 | tf_op jit(solution)/shard_map/ppermute | solution.py:272
  27.9 0.4 collective-permute-done.19.refs_1_
  28.3 0.2 collective-permute-done.21.refs_3_
  28.5 1.2 %shard_map.91 = (f32[128,1024]{1,0:T(8,128)S(1)}, bf16[128,1024]{1,0:T(8,128)(2,1)S(1)}) custom-call(bf16[32,2176]{1,0:T(8,128)(2,1)S(1)} %collective-permute-done.18.refs_0_, bf16[32,2176]{1,0:T(8,128)(2,1)S(1)} %collective-permute-done.19.refs_1_, bf16[32,2176]{1,0:T(8,128)(2,1)S(1)} %collective-permute-done.20.refs_2_, ...), custom_call_target="tpu_custom_call" | custom-call | tf_op jit(solution)/shard_map/pallas_call | solution.py:235
  29.6 0.2 collective-permute-start.22
  29.9 1.2 %shard_map.88 = (f32[128,1024]{1,0:T(8,128)S(1)}, bf16[128,1024]{1,0:T(8,128)(2,1)S(1)}) custom-call(bf16[32,2176]{1,0:T(8,128)(2,1)S(1)} %collective-permute-done.11.refs_0_, bf16[32,2176]{1,0:T(8,128)(2,1)S(1)} %collective-permute-done.12.refs_1_, bf16[32,2176]{1,0:T(8,128)(2,1)S(1)} %collective-permute-done.13.refs_2_, ...), custom_call_target="tpu_custom_call" | custom-call | tf_op jit(solution)/shard_map/pallas_call | solution.py:235
  31.0 0.4 collective-permute-start.15
  31.5 0.0 copy-start
  31.6 2.1 %collective-permute-start.23 = (bf16[64,1024]{1,0:T(8,128)(2,1)S(1)}, bf16[64,1024]{1,0:T(8,128)(2,1)S(1)}, u32[]{:S(2)}, u32[]{:S(2)}) collective-permute-start(bf16[64,1024]{1,0:T(8,128)(2,1)S(1)} %get-tuple-element.61), channel_id=1, source_target_pairs={{0,2},{2,0},{4,6},{6,4},{8,10},{10,8},{12,14},{14,12},{1,3},{3,1},... | collective-permute-start | bytes 393224 | tf_op jit(solution)/shard_map/ppermute | solution.py:272
  33.7 1.1 %collective-permute-start.16 = (bf16[64,1024]{1,0:T(8,128)(2,1)S(1)}, bf16[64,1024]{1,0:T(8,128)(2,1)S(1)}, u32[]{:S(2)}, u32[]{:S(2)}) collective-permute-start(bf16[64,1024]{1,0:T(8,128)(2,1)S(1)} %get-tuple-element.55), channel_id=1, source_target_pairs={{0,2},{2,0},{4,6},{6,4},{8,10},{10,8},{12,14},{14,12},{1,3},{3,1},... | collective-permute-start | bytes 393224 | tf_op jit(solution)/shard_map/ppermute | solution.py:272
  34.8 0.1 shard_map.85
  34.9 1.1 %collective-permute-start.9 = (bf16[64,1024]{1,0:T(8,128)(2,1)S(1)}, bf16[64,1024]{1,0:T(8,128)(2,1)S(1)}, u32[]{:S(2)}, u32[]{:S(2)}) collective-permute-start(bf16[64,1024]{1,0:T(8,128)(2,1)S(1)} %get-tuple-element.49), channel_id=1, source_target_pairs={{0,2},{2,0},{4,6},{6,4},{8,10},{10,8},{12,14},{14,12},{1,3},{3,1},... | collective-permute-start | bytes 393224 | tf_op jit(solution)/shard_map/ppermute | solution.py:272
  36.0 1.0 %collective-permute-start.8 = (bf16[64,1024]{1,0:T(8,128)(2,1)S(1)}, bf16[64,1024]{1,0:T(8,128)(2,1)S(1)}, u32[]{:S(2)}, u32[]{:S(2)}) collective-permute-start(bf16[64,1024]{1,0:T(8,128)(2,1)S(1)} %get-tuple-element.46), channel_id=1, source_target_pairs={{0,2},{2,0},{4,6},{6,4},{8,10},{10,8},{12,14},{14,12},{1,3},{3,1},... | collective-permute-start | bytes 393224 | tf_op jit(solution)/shard_map/ppermute | solution.py:272
  37.0 1.0 %collective-permute-done.23.recv_ref = bf16[64,1024]{1,0:T(8,128)(2,1)S(1)} collective-permute-done((bf16[64,1024]{1,0:T(8,128)(2,1)S(1)}, bf16[64,1024]{1,0:T(8,128)(2,1)S(1)}, u32[]{:S(2)}, u32[]{:S(2)}) %collective-permute-start.23) | collective-permute-done | bytes 131104 | tf_op jit(solution)/shard_map/ppermute | solution.py:272
  38.0 0.2 shard_map.93
  38.2 3.4 %collective-permute-start.24 = (bf16[64,1024]{1,0:T(8,128)(2,1)S(1)}, bf16[64,1024]{1,0:T(8,128)(2,1)S(1)}, u32[]{:S(2)}, u32[]{:S(2)}) collective-permute-start(bf16[64,1024]{1,0:T(8,128)(2,1)S(1)} %get-tuple-element.62), channel_id=1, source_target_pairs={{0,12},{2,14},{4,8},{6,10},{8,4},{10,6},{12,0},{14,2},{1,13},{3,15... | collective-permute-start | bytes 393224 | tf_op jit(solution)/shard_map/ppermute | solution.py:263
  41.6 0.2 shard_map.90
  41.7 1.9 %collective-permute-done.9.recv_ref = bf16[64,1024]{1,0:T(8,128)(2,1)S(1)} collective-permute-done((bf16[64,1024]{1,0:T(8,128)(2,1)S(1)}, bf16[64,1024]{1,0:T(8,128)(2,1)S(1)}, u32[]{:S(2)}, u32[]{:S(2)}) %collective-permute-start.9) | collective-permute-done | bytes 131104 | tf_op jit(solution)/shard_map/ppermute | solution.py:272
  43.6 0.2 shard_map.87
  43.8 1.3 %collective-permute-start.10 = (bf16[64,1024]{1,0:T(8,128)(2,1)S(1)}, bf16[64,1024]{1,0:T(8,128)(2,1)S(1)}, u32[]{:S(2)}, u32[]{:S(2)}) collective-permute-start(bf16[64,1024]{1,0:T(8,128)(2,1)S(1)} %get-tuple-element.50), channel_id=1, source_target_pairs={{0,4},{2,6},{4,0},{6,2},{8,12},{10,14},{12,8},{14,10},{1,5},{3,7},... | collective-permute-start | bytes 393224 | tf_op jit(solution)/shard_map/ppermute | solution.py:263
  45.1 0.2 collective-permute-start.28
  45.3 0.6 %collective-permute-done.8.recv_ref = bf16[64,1024]{1,0:T(8,128)(2,1)S(1)} collective-permute-done((bf16[64,1024]{1,0:T(8,128)(2,1)S(1)}, bf16[64,1024]{1,0:T(8,128)(2,1)S(1)}, u32[]{:S(2)}, u32[]{:S(2)}) %collective-permute-start.8) | collective-permute-done | bytes 131104 | tf_op jit(solution)/shard_map/ppermute | solution.py:272
  45.9 1.1 %collective-permute-start.27 = (f32[8,64]{1,0:T(8,128)S(1)}, f32[8,64]{1,0:T(8,128)S(1)}, u32[]{:S(2)}, u32[]{:S(2)}) collective-permute-start(f32[8,64]{1,0:T(8,128)S(1)} %get-tuple-element.65), channel_id=1, source_target_pairs={{0,9},{1,8},{2,11},{3,10},{4,13},{5,12},{6,15},{7,14},{8,1},{9,0},... | collective-permute-start | bytes 6152 | tf_op jit(solution)/shard_map/ppermute | solution.py:269
  47.0 0.2 shard_map.86
  47.2 2.8 %collective-permute-done.28.refs_7_ = f32[8,64]{1,0:T(8,128)S(1)} collective-permute-done((f32[8,64]{1,0:T(8,128)S(1)}, f32[8,64]{1,0:T(8,128)S(1)}, u32[]{:S(2)}, u32[]{:S(2)}) %collective-permute-start.28) | collective-permute-done | bytes 2080 | tf_op jit(solution)/shard_map/ppermute | solution.py:269
  50.0 1.6 %collective-permute-start.26 = (f32[8,64]{1,0:T(8,128)S(1)}, f32[8,64]{1,0:T(8,128)S(1)}, u32[]{:S(2)}, u32[]{:S(2)}) collective-permute-start(f32[8,64]{1,0:T(8,128)S(1)} %get-tuple-element.64), channel_id=1, source_target_pairs={{0,5},{1,4},{2,7},{3,6},{4,1},{5,0},{6,3},{7,2},{8,13},{9,12},{10,... | collective-permute-start | bytes 6152 | tf_op jit(solution)/shard_map/ppermute | solution.py:269
  51.6 0.1 collective-permute-start.25
  51.7 1.3 %collective-permute-done.26.refs_5_ = f32[8,64]{1,0:T(8,128)S(1)} collective-permute-done((f32[8,64]{1,0:T(8,128)S(1)}, f32[8,64]{1,0:T(8,128)S(1)}, u32[]{:S(2)}, u32[]{:S(2)}) %collective-permute-start.26) | collective-permute-done | bytes 2080 | tf_op jit(solution)/shard_map/ppermute | solution.py:269
  53.0 1.1 %shard_map.94 = bf16[128,1024]{1,0:T(8,128)(2,1)} custom-call(bf16[128,256]{1,0:T(8,128)(2,1)S(1)} %get-tuple-element.37.map_ref, f32[1,1024]{1,0:T(1,128)S(1)} %bitcast.4, bf16[64,1024]{1,0:T(8,128)(2,1)S(1)} %get-tuple-element.47.refs_0_, bf16[64,1024]{1,0:T(8,128)(2,1)S(1)} %collective-permute-done.10.refs_1_, ...), custom_call_target="tpu_custom_call" | custom-call | tf_op jit(solution)/shard_map/pallas_call | solution.py:235
  (25 shorter events, 0.2 us)
Async XLA Ops:
  1.7 7.1 %collective-permute-start.3 = (bf16[32,2176]{1,0:T(8,128)(2,1)S(1)}, bf16[32,2176]{1,0:T(8,128)(2,1)S(1)}, u32[]{:S(2)}, u32[]{:S(2)}) collective-permute-start(bf16[32,2176]{1,0:T(8,128)(2,1)S(1)} %get-tuple-element.39), channel_id=1, source_target_pairs={{0,4},{2,6},{4,0},{6,2},{8,12},{10,14},{12,8},{14,10},{1,5},{3,7},... | collective-permute-start | bytes 417800 | tf_op jit(solution)/shard_map/ppermute | solution.py:263
  4.8 9.3 %collective-permute-start.18 = (bf16[32,2176]{1,0:T(8,128)(2,1)S(1)}, bf16[32,2176]{1,0:T(8,128)(2,1)S(1)}, u32[]{:S(2)}, u32[]{:S(2)}) collective-permute-start(bf16[32,2176]{1,0:T(8,128)(2,1)S(1)} %get-tuple-element.57), channel_id=1, source_target_pairs={{0,12},{2,14},{4,8},{6,10},{8,4},{10,6},{12,0},{14,2},{1,13},{3,15... | collective-permute-start | bytes 417800 | tf_op jit(solution)/shard_map/ppermute | solution.py:263
  7.3 7.1 %collective-permute-start.1 = (bf16[32,2176]{1,0:T(8,128)(2,1)S(1)}, bf16[32,2176]{1,0:T(8,128)(2,1)S(1)}, u32[]{:S(2)}, u32[]{:S(2)}) collective-permute-start(bf16[32,2176]{1,0:T(8,128)(2,1)S(1)} %get-tuple-element.38.refs_0_), channel_id=1, source_target_pairs={{0,2},{2,0},{4,6},{6,4},{8,10},{10,8},{12,14},{14,12},{1,3},{3,1},... | collective-permute-start | bytes 417800 | tf_op jit(solution)/shard_map/ppermute | solution.py:272
  8.8 6.3 %collective-permute-start.5 = (bf16[32,2176]{1,0:T(8,128)(2,1)S(1)}, bf16[32,2176]{1,0:T(8,128)(2,1)S(1)}, u32[]{:S(2)}, u32[]{:S(2)}) collective-permute-start(bf16[32,2176]{1,0:T(8,128)(2,1)S(1)} %collective-permute-done.3.refs_4_), channel_id=1, source_target_pairs={{0,2},{2,0},{4,6},{6,4},{8,10},{10,8},{12,14},{14,12},{1,3},{3,1},... | collective-permute-start | bytes 417800 | tf_op jit(solution)/shard_map/ppermute | solution.py:272
  10.1 8.1 %collective-permute-start.11 = (bf16[32,2176]{1,0:T(8,128)(2,1)S(1)}, bf16[32,2176]{1,0:T(8,128)(2,1)S(1)}, u32[]{:S(2)}, u32[]{:S(2)}) collective-permute-start(bf16[32,2176]{1,0:T(8,128)(2,1)S(1)} %get-tuple-element.51), channel_id=1, source_target_pairs={{0,8},{2,10},{4,12},{6,14},{8,0},{10,2},{12,4},{14,6},{1,9},{3,11}... | collective-permute-start | bytes 417800 | tf_op jit(solution)/shard_map/ppermute | solution.py:263
  13.8 7.4 %collective-permute-start = (bf16[32,2176]{1,0:T(8,128)(2,1)S(1)}, bf16[32,2176]{1,0:T(8,128)(2,1)S(1)}, u32[]{:S(2)}, u32[]{:S(2)}) collective-permute-start(bf16[32,2176]{1,0:T(8,128)(2,1)S(1)} %get-tuple-element.38.refs_0_), channel_id=1, source_target_pairs={{0,1},{1,0},{2,3},{3,2},{4,5},{5,4},{6,7},{7,6},{8,9},{9,8},{10,11... | collective-permute-start | bytes 417800 | tf_op jit(solution)/shard_map/ppermute | solution.py:275
  14.1 10.0 %collective-permute-start.4 = (bf16[32,2176]{1,0:T(8,128)(2,1)S(1)}, bf16[32,2176]{1,0:T(8,128)(2,1)S(1)}, u32[]{:S(2)}, u32[]{:S(2)}) collective-permute-start(bf16[32,2176]{1,0:T(8,128)(2,1)S(1)} %collective-permute-done.3.refs_4_), channel_id=1, source_target_pairs={{0,1},{1,0},{2,3},{3,2},{4,5},{5,4},{6,7},{7,6},{8,9},{9,8},{10,11... | collective-permute-start | bytes 417800 | tf_op jit(solution)/shard_map/ppermute | solution.py:275
  14.4 9.7 %collective-permute-start.2 = (bf16[32,2176]{1,0:T(8,128)(2,1)S(1)}, bf16[32,2176]{1,0:T(8,128)(2,1)S(1)}, u32[]{:S(2)}, u32[]{:S(2)}) collective-permute-start(bf16[32,2176]{1,0:T(8,128)(2,1)S(1)} %collective-permute-done.1.refs_2_), channel_id=1, source_target_pairs={{0,1},{1,0},{2,3},{3,2},{4,5},{5,4},{6,7},{7,6},{8,9},{9,8},{10,11... | collective-permute-start | bytes 417800 | tf_op jit(solution)/shard_map/ppermute | solution.py:275
  15.1 9.0 %collective-permute-start.6 = (bf16[32,2176]{1,0:T(8,128)(2,1)S(1)}, bf16[32,2176]{1,0:T(8,128)(2,1)S(1)}, u32[]{:S(2)}, u32[]{:S(2)}) collective-permute-start(bf16[32,2176]{1,0:T(8,128)(2,1)S(1)} %collective-permute-done.5.refs_6_), channel_id=1, source_target_pairs={{0,1},{1,0},{2,3},{3,2},{4,5},{5,4},{6,7},{7,6},{8,9},{9,8},{10,11... | collective-permute-start | bytes 417800 | tf_op jit(solution)/shard_map/ppermute | solution.py:275
  18.2 8.4 %collective-permute-start.20 = (bf16[32,2176]{1,0:T(8,128)(2,1)S(1)}, bf16[32,2176]{1,0:T(8,128)(2,1)S(1)}, u32[]{:S(2)}, u32[]{:S(2)}) collective-permute-start(bf16[32,2176]{1,0:T(8,128)(2,1)S(1)} %collective-permute-done.18.refs_0_), channel_id=1, source_target_pairs={{0,2},{2,0},{4,6},{6,4},{8,10},{10,8},{12,14},{14,12},{1,3},{3,1},... | collective-permute-start | bytes 417800 | tf_op jit(solution)/shard_map/ppermute | solution.py:272
  21.2 6.7 %collective-permute-start.13 = (bf16[32,2176]{1,0:T(8,128)(2,1)S(1)}, bf16[32,2176]{1,0:T(8,128)(2,1)S(1)}, u32[]{:S(2)}, u32[]{:S(2)}) collective-permute-start(bf16[32,2176]{1,0:T(8,128)(2,1)S(1)} %collective-permute-done.11.refs_0_), channel_id=1, source_target_pairs={{0,2},{2,0},{4,6},{6,4},{8,10},{10,8},{12,14},{14,12},{1,3},{3,1},... | collective-permute-start | bytes 417800 | tf_op jit(solution)/shard_map/ppermute | solution.py:272
  26.1 8.7 %collective-permute-start.7 = (bf16[256,1024]{1,0:T(8,128)(2,1)S(1)}, bf16[256,1024]{1,0:T(8,128)(2,1)S(1)}, u32[]{:S(2)}, u32[]{:S(2)}) collective-permute-start(bf16[256,1024]{1,0:T(8,128)(2,1)S(1)} %get-tuple-element.44), channel_id=1, source_target_pairs={{0,1},{1,0},{2,3},{3,2},{4,5},{5,4},{6,7},{7,6},{8,9},{9,8},{10,11... | collective-permute-start | bytes 1572872 | tf_op jit(solution)/shard_map/ppermute | solution.py:275
  26.2 2.1 %collective-permute-start.19 = (bf16[32,2176]{1,0:T(8,128)(2,1)S(1)}, bf16[32,2176]{1,0:T(8,128)(2,1)S(1)}, u32[]{:S(2)}, u32[]{:S(2)}) collective-permute-start(bf16[32,2176]{1,0:T(8,128)(2,1)S(1)} %collective-permute-done.18.refs_0_), channel_id=1, source_target_pairs={{0,1},{1,0},{2,3},{3,2},{4,5},{5,4},{6,7},{7,6},{8,9},{9,8},{10,11... | collective-permute-start | bytes 417800 | tf_op jit(solution)/shard_map/ppermute | solution.py:275
  26.7 1.8 %collective-permute-start.21 = (bf16[32,2176]{1,0:T(8,128)(2,1)S(1)}, bf16[32,2176]{1,0:T(8,128)(2,1)S(1)}, u32[]{:S(2)}, u32[]{:S(2)}) collective-permute-start(bf16[32,2176]{1,0:T(8,128)(2,1)S(1)} %collective-permute-done.20.refs_2_), channel_id=1, source_target_pairs={{0,1},{1,0},{2,3},{3,2},{4,5},{5,4},{6,7},{7,6},{8,9},{9,8},{10,11... | collective-permute-start | bytes 417800 | tf_op jit(solution)/shard_map/ppermute | solution.py:275
  26.8 3.1 %collective-permute-start.12 = (bf16[32,2176]{1,0:T(8,128)(2,1)S(1)}, bf16[32,2176]{1,0:T(8,128)(2,1)S(1)}, u32[]{:S(2)}, u32[]{:S(2)}) collective-permute-start(bf16[32,2176]{1,0:T(8,128)(2,1)S(1)} %collective-permute-done.11.refs_0_), channel_id=1, source_target_pairs={{0,1},{1,0},{2,3},{3,2},{4,5},{5,4},{6,7},{7,6},{8,9},{9,8},{10,11... | collective-permute-start | bytes 417800 | tf_op jit(solution)/shard_map/ppermute | solution.py:275
  27.9 2.0 %collective-permute-start.14 = (bf16[32,2176]{1,0:T(8,128)(2,1)S(1)}, bf16[32,2176]{1,0:T(8,128)(2,1)S(1)}, u32[]{:S(2)}, u32[]{:S(2)}) collective-permute-start(bf16[32,2176]{1,0:T(8,128)(2,1)S(1)} %collective-permute-done.13.refs_2_), channel_id=1, source_target_pairs={{0,1},{1,0},{2,3},{3,2},{4,5},{5,4},{6,7},{7,6},{8,9},{9,8},{10,11... | collective-permute-start | bytes 417800 | tf_op jit(solution)/shard_map/ppermute | solution.py:275
  29.6 1.8 %collective-permute-start.22 = (bf16[128,1024]{1,0:T(8,128)(2,1)S(1)}, bf16[128,1024]{1,0:T(8,128)(2,1)S(1)}, u32[]{:S(2)}, u32[]{:S(2)}) collective-permute-start(bf16[128,1024]{1,0:T(8,128)(2,1)S(1)} %get-tuple-element.59), channel_id=1, source_target_pairs={{0,1},{1,0},{2,3},{3,2},{4,5},{5,4},{6,7},{7,6},{8,9},{9,8},{10,11... | collective-permute-start | bytes 786440 | tf_op jit(solution)/shard_map/ppermute | solution.py:275
  31.0 2.6 %collective-permute-start.15 = (bf16[128,1024]{1,0:T(8,128)(2,1)S(1)}, bf16[128,1024]{1,0:T(8,128)(2,1)S(1)}, u32[]{:S(2)}, u32[]{:S(2)}) collective-permute-start(bf16[128,1024]{1,0:T(8,128)(2,1)S(1)} %get-tuple-element.53), channel_id=1, source_target_pairs={{0,1},{1,0},{2,3},{3,2},{4,5},{5,4},{6,7},{7,6},{8,9},{9,8},{10,11... | collective-permute-start | bytes 786440 | tf_op jit(solution)/shard_map/ppermute | solution.py:275
  31.5 21.5 %copy-start = (f32[1024]{0:T(1024)S(1)}, f32[1024]{0:T(1024)}, u32[]{:S(2)}) copy-start(f32[1024]{0:T(1024)} %param.15) | copy-start | bytes 12292
  31.6 6.4 %collective-permute-start.23 = (bf16[64,1024]{1,0:T(8,128)(2,1)S(1)}, bf16[64,1024]{1,0:T(8,128)(2,1)S(1)}, u32[]{:S(2)}, u32[]{:S(2)}) collective-permute-start(bf16[64,1024]{1,0:T(8,128)(2,1)S(1)} %get-tuple-element.61), channel_id=1, source_target_pairs={{0,2},{2,0},{4,6},{6,4},{8,10},{10,8},{12,14},{14,12},{1,3},{3,1},... | collective-permute-start | bytes 393224 | tf_op jit(solution)/shard_map/ppermute | solution.py:272
  33.7 7.9 %collective-permute-start.16 = (bf16[64,1024]{1,0:T(8,128)(2,1)S(1)}, bf16[64,1024]{1,0:T(8,128)(2,1)S(1)}, u32[]{:S(2)}, u32[]{:S(2)}) collective-permute-start(bf16[64,1024]{1,0:T(8,128)(2,1)S(1)} %get-tuple-element.55), channel_id=1, source_target_pairs={{0,2},{2,0},{4,6},{6,4},{8,10},{10,8},{12,14},{14,12},{1,3},{3,1},... | collective-permute-start | bytes 393224 | tf_op jit(solution)/shard_map/ppermute | solution.py:272
  34.9 8.7 %collective-permute-start.9 = (bf16[64,1024]{1,0:T(8,128)(2,1)S(1)}, bf16[64,1024]{1,0:T(8,128)(2,1)S(1)}, u32[]{:S(2)}, u32[]{:S(2)}) collective-permute-start(bf16[64,1024]{1,0:T(8,128)(2,1)S(1)} %get-tuple-element.49), channel_id=1, source_target_pairs={{0,2},{2,0},{4,6},{6,4},{8,10},{10,8},{12,14},{14,12},{1,3},{3,1},... | collective-permute-start | bytes 393224 | tf_op jit(solution)/shard_map/ppermute | solution.py:272
  36.0 9.9 %collective-permute-start.8 = (bf16[64,1024]{1,0:T(8,128)(2,1)S(1)}, bf16[64,1024]{1,0:T(8,128)(2,1)S(1)}, u32[]{:S(2)}, u32[]{:S(2)}) collective-permute-start(bf16[64,1024]{1,0:T(8,128)(2,1)S(1)} %get-tuple-element.46), channel_id=1, source_target_pairs={{0,2},{2,0},{4,6},{6,4},{8,10},{10,8},{12,14},{14,12},{1,3},{3,1},... | collective-permute-start | bytes 393224 | tf_op jit(solution)/shard_map/ppermute | solution.py:272
  38.2 13.5 %collective-permute-start.24 = (bf16[64,1024]{1,0:T(8,128)(2,1)S(1)}, bf16[64,1024]{1,0:T(8,128)(2,1)S(1)}, u32[]{:S(2)}, u32[]{:S(2)}) collective-permute-start(bf16[64,1024]{1,0:T(8,128)(2,1)S(1)} %get-tuple-element.62), channel_id=1, source_target_pairs={{0,12},{2,14},{4,8},{6,10},{8,4},{10,6},{12,0},{14,2},{1,13},{3,15... | collective-permute-start | bytes 393224 | tf_op jit(solution)/shard_map/ppermute | solution.py:263
  41.7 10.0 %collective-permute-start.17 = (bf16[64,1024]{1,0:T(8,128)(2,1)S(1)}, bf16[64,1024]{1,0:T(8,128)(2,1)S(1)}, u32[]{:S(2)}, u32[]{:S(2)}) collective-permute-start(bf16[64,1024]{1,0:T(8,128)(2,1)S(1)} %get-tuple-element.56), channel_id=1, source_target_pairs={{0,8},{2,10},{4,12},{6,14},{8,0},{10,2},{12,4},{14,6},{1,9},{3,11}... | collective-permute-start | bytes 393224 | tf_op jit(solution)/shard_map/ppermute | solution.py:263
  43.8 9.2 %collective-permute-start.10 = (bf16[64,1024]{1,0:T(8,128)(2,1)S(1)}, bf16[64,1024]{1,0:T(8,128)(2,1)S(1)}, u32[]{:S(2)}, u32[]{:S(2)}) collective-permute-start(bf16[64,1024]{1,0:T(8,128)(2,1)S(1)} %get-tuple-element.50), channel_id=1, source_target_pairs={{0,4},{2,6},{4,0},{6,2},{8,12},{10,14},{12,8},{14,10},{1,5},{3,7},... | collective-permute-start | bytes 393224 | tf_op jit(solution)/shard_map/ppermute | solution.py:263
  45.1 4.9 %collective-permute-start.28 = (f32[8,64]{1,0:T(8,128)S(1)}, f32[8,64]{1,0:T(8,128)S(1)}, u32[]{:S(2)}, u32[]{:S(2)}) collective-permute-start(f32[8,64]{1,0:T(8,128)S(1)} %get-tuple-element.66), channel_id=1, source_target_pairs={{0,13},{1,12},{2,15},{3,14},{4,9},{5,8},{6,11},{7,10},{8,5},{9,4},... | collective-permute-start | bytes 6152 | tf_op jit(solution)/shard_map/ppermute | solution.py:269
  45.9 5.8 %collective-permute-start.27 = (f32[8,64]{1,0:T(8,128)S(1)}, f32[8,64]{1,0:T(8,128)S(1)}, u32[]{:S(2)}, u32[]{:S(2)}) collective-permute-start(f32[8,64]{1,0:T(8,128)S(1)} %get-tuple-element.65), channel_id=1, source_target_pairs={{0,9},{1,8},{2,11},{3,10},{4,13},{5,12},{6,15},{7,14},{8,1},{9,0},... | collective-permute-start | bytes 6152 | tf_op jit(solution)/shard_map/ppermute | solution.py:269
  50.0 3.0 %collective-permute-start.26 = (f32[8,64]{1,0:T(8,128)S(1)}, f32[8,64]{1,0:T(8,128)S(1)}, u32[]{:S(2)}, u32[]{:S(2)}) collective-permute-start(f32[8,64]{1,0:T(8,128)S(1)} %get-tuple-element.64), channel_id=1, source_target_pairs={{0,5},{1,4},{2,7},{3,6},{4,1},{5,0},{6,3},{7,2},{8,13},{9,12},{10,... | collective-permute-start | bytes 6152 | tf_op jit(solution)/shard_map/ppermute | solution.py:269
  51.6 1.4 %collective-permute-start.25 = (f32[8,64]{1,0:T(8,128)S(1)}, f32[8,64]{1,0:T(8,128)S(1)}, u32[]{:S(2)}, u32[]{:S(2)}) collective-permute-start(f32[8,64]{1,0:T(8,128)S(1)} %get-tuple-element.63), channel_id=1, source_target_pairs={{0,1},{1,0},{2,3},{3,2},{4,5},{5,4},{6,7},{7,6},{8,9},{9,8},{10,11... | collective-permute-start | bytes 6152 | tf_op jit(solution)/shard_map/ppermute | solution.py:275

commit v3 on v2

--- a/solution.py
+++ b/solution.py
@@ -157,78 +157,60 @@
         copy.wait()
 
 
-def expert_kernel(chunks, members, width, half, *refs):
-    pieces = refs[: 4 * chunks]
-    wg_ref, wu_ref, wd_ref, keep_ref, send_ref, rows_ref = refs[4 * chunks :]
-    my_half = lax.axis_index("tp")
+def expert_kernel(chunks, members, width, *refs):
+    pieces, refs = refs[: 2 * chunks], refs[2 * chunks :]
+    weights, outs, rows_ref = refs[:6], refs[6:-1], refs[-1]
     me = lax.axis_index("ep") % members
-    local_experts, model_width, _ = wg_ref.shape
-    half_width = keep_ref.shape[1]
-    mine = pl.multiple_of(my_half * half, half)
-    other = pl.multiple_of((1 - my_half) * half, half)
-    for c in range(chunks):
-        own, own_tp, far, far_tp = pieces[4 * c : 4 * c + 4]
-        near_base = c * 4 * half
-        far_base = near_base + 2 * half
-        rows_ref[pl.ds(near_base + mine, half), :] = own[...]
-        rows_ref[pl.ds(near_base + other, half), :] = own_tp[...]
-        rows_ref[pl.ds(far_base + mine, half), :] = far[...]
-        rows_ref[pl.ds(far_base + other, half), :] = far_tp[...]
+    local_experts, model_width, _ = weights[0].shape
+    half = pieces[0].shape[0]
+    for i, piece in enumerate(pieces):
+        rows_ref[i * half : (i + 1) * half, :] = piece[...]
+    used = len(pieces) * half
+    if used < rows_ref.shape[0]:
+        rows_ref[used:, :] = jnp.zeros((rows_ref.shape[0] - used, rows_ref.shape[1]), rows_ref.dtype)
     rows = rows_ref[:, :model_width]
     terms = rows_ref[:, model_width:].astype(jnp.float32)
-    lane = lax.broadcasted_iota(jnp.int32, terms.shape, 1)
+    lane = iota(terms.shape, 1)
     hidden = []
     for e in range(local_experts):
         wanted = (lane % width == me * local_experts + e) & (lane < TERMS * width)
         weight = jnp.sum(jnp.where(wanted, terms, 0.0), axis=1, keepdims=True)
-        gate_act = dot(rows, wg_ref[e])
-        up_act = dot(rows, wu_ref[e])
-        act = gate_act / (1.0 + jnp.exp(-gate_act)) * up_act
-        hidden.append((act * weight).astype(jnp.bfloat16))
-    send_at = pl.multiple_of((1 - my_half) * half_width, half_width)
-    keep_at = pl.multiple_of(my_half * half_width, half_width)
-    total = dot(hidden[0], wd_ref[0, :, pl.ds(send_at, half_width)])
-    for e in range(1, local_experts):
-        total += dot(hidden[e], wd_ref[e, :, pl.ds(send_at, half_width)])
-    send_ref[...] = total.astype(jnp.bfloat16)
-    total = dot(hidden[0], wd_ref[0, :, pl.ds(keep_at, half_width)])
-    for e in range(1, local_experts):
-        total += dot(hidden[e], wd_ref[e, :, pl.ds(keep_at, half_width)])
-    keep_ref[...] = total
-
-
-def split_kernel(chunks, cap, mine_ref, recv_ref, *outs):
+        for wg_ref, wu_ref in (weights[:2], weights[3:5]):
+            gate_act = dot(rows, wg_ref[e])
+            up_act = dot(rows, wu_ref[e])
+            act = gate_act / (1.0 + jnp.exp(-gate_act)) * up_act
+            hidden.append((act * weight).astype(jnp.bfloat16))
+    hidden = jnp.concatenate(hidden, axis=1)
+    down = [ref[e] for e in range(local_experts) for ref in (weights[2], weights[5])]
+    total = dot(hidden, jnp.concatenate(down, axis=0))
     for c in range(chunks):
-        near = pl.ds(2 * c * cap, cap)
-        far = pl.ds((2 * c + 1) * cap, cap)
-        keep_ref, send_ref = outs[2 * c : 2 * c + 2]
-        keep_ref[...] = mine_ref[near, :] + recv_ref[near, :].astype(jnp.float32)
-        send_ref[...] = (mine_ref[far, :] + recv_ref[far, :].astype(jnp.float32)).astype(
-            jnp.bfloat16
-        )
-
-
-def join_kernel(keep_ref, recv_ref, row_ref, square_ref):
+        outs[2 * c][...] = total[2 * c * half : (2 * c + 1) * half]
+        outs[2 * c + 1][...] = total[(2 * c + 1) * half : (2 * c + 2) * half].astype(jnp.bfloat16)
+
+
+def join_kernel(keep_ref, recv_ref, same_ref, other_ref, rows_ref):
     rows = keep_ref[...] + recv_ref[...].astype(jnp.float32)
-    row_ref[...] = rows.astype(jnp.bfloat16)
-    squares = jnp.sum(rows * rows, axis=1, keepdims=True)
-    square_ref[...] = jnp.broadcast_to(squares, (rows.shape[0], LANES)).T[:8]
-
-
-def close_kernel(cap, model_width, map_ref, gain_ref, *refs):
-    parts, squares = refs[:GROUPS], refs[GROUPS : 2 * GROUPS]
-    out_ref, rows_ref = refs[2 * GROUPS :]
+    model_width = rows.shape[1]
+    mean = jnp.sum(rows * rows, axis=1, keepdims=True) / model_width
+    rows_ref[...] = (rows * lax.rsqrt(mean + EPS)).astype(jnp.bfloat16)
+    half_width = same_ref.shape[1]
+    my_half = lax.axis_index("tp")
+    same_ref[...] = rows_ref[:, pl.ds(pl.multiple_of(my_half * half_width, half_width), half_width)]
+    other_ref[...] = rows_ref[
+        :, pl.ds(pl.multiple_of((1 - my_half) * half_width, half_width), half_width)
+    ]
+
+
+def close_kernel(cap, map_ref, gain_ref, *refs):
+    parts, out_ref, rows_ref = refs[: 2 * GROUPS], refs[-2], refs[-1]
+    half = cap // 2
+    my_half = lax.axis_index("tp")
     for k in range(GROUPS):
-        rows_ref[k * cap : (k + 1) * cap, :] = parts[k][...]
-    placing = map_ref[...]
-    mixed = dot(placing, rows_ref[...])
-    far = jnp.concatenate([square[0:1, :] for square in squares], axis=1)
-    total = jnp.sum(mixed * mixed, axis=1, keepdims=True) + jnp.sum(
-        placing.astype(jnp.float32) * far, axis=1, keepdims=True
-    )
-    out_ref[...] = (mixed * lax.rsqrt(total / model_width + EPS) * gain_ref[...]).astype(
-        jnp.bfloat16
-    )
+        same = pl.multiple_of(k * cap + my_half * half, half)
+        other = pl.multiple_of(k * cap + (1 - my_half) * half, half)
+        rows_ref[pl.ds(same, half), :] = parts[2 * k][...]
+        rows_ref[pl.ds(other, half), :] = parts[2 * k + 1][...]
+    out_ref[...] = (dot(map_ref[...], rows_ref[...]) * gain_ref[...]).astype(jnp.bfloat16)
 
 
 def call(kernel, outs, args, limit, scratch=(), in_specs=None):
@@ -239,6 +221,9 @@
         scratch_shapes=scratch,
         compiler_params=pltpu.CompilerParams(vmem_limit_bytes=limit * MIB),
     )(*args)
+
+
+STAGES = ((0, 1), (3,), (2,))
 
 
 def dense_body(tokens, in_gain, routing, gate_prob, w_gate, w_up, w_down, out_gain):
@@ -304,55 +289,46 @@
         [anywhere] * 3 + [in_vmem],
     )
     arrived = [packed[0]] + [hop(packed[k], k) for k in range(1, GROUPS)]
-
-    back, squares = [None] * GROUPS, [None] * GROUPS
+    weights += [swap(w) for w in (w_gate, w_up, w_down)]
+    weights = [pltpu.with_memory_space_constraint(w, pltpu.VMEM) for w in weights]
+
+    back = [None] * (2 * GROUPS)
 
     def experts(ks):
         pieces = []
         for k in ks:
-            far = cross(arrived[k])
-            pieces += [arrived[k], swap(arrived[k]), far, swap(far)]
+            pieces += [arrived[k], cross(arrived[k])]
         n = len(ks)
-        rows = n * 2 * cap
-        mine, other = call(
-            functools.partial(expert_kernel, n, members, width, half),
-            [sds((rows, half_width), f32), sds((rows, half_width), bf16)],
+        sums = call(
+            functools.partial(expert_kernel, n, members, width),
+            [sds((half, model_width), f32), sds((half, model_width), bf16)] * n,
             (*pieces, *weights),
-            24,
-            (pltpu.VMEM((rows, model_width + LANES), bf16),),
-        )
-        split = call(
-            functools.partial(split_kernel, n, cap),
-            [sds((cap, half_width), f32), sds((cap, half_width), bf16)] * n,
-            (mine, swap(other)),
-            8,
+            20,
+            (pltpu.VMEM((max(n * cap, LANES), model_width + LANES), bf16),),
         )
         for c, k in enumerate(ks):
-            keep, send = split[2 * c : 2 * c + 2]
-            rows_out, square = call(
+            same, other = call(
                 join_kernel,
-                [sds((cap, half_width), bf16), sds((8, cap), f32)],
-                (keep, cross(send)),
+                [sds((half, half_width), bf16)] * 2,
+                (sums[2 * c], cross(sums[2 * c + 1])),
                 8,
+                (pltpu.VMEM((half, model_width), bf16),),
             )
             if k == 0:
-                back[k], squares[k] = rows_out, swap(square)
+                back[:2] = same, swap(other)
             else:
-                back[k] = hop(rows_out, k)
-                squares[k] = hop_swap(square, k)
+                back[2 * k] = hop(same, k)
+                back[2 * k + 1] = hop_swap(other, k)
 
     for ks in STAGES:
         experts(ks)
     return call(
-        functools.partial(close_kernel, cap, model_width),
+        functools.partial(close_kernel, cap),
         sds((tok_dev, half_width), bf16),
-        (token_map, out_gain.reshape(1, -1), *back, *squares),
+        (token_map, out_gain.reshape(1, -1), *back),
         8,
         (pltpu.VMEM((GROUPS * cap, half_width), bf16),),
     )
-
-
-STAGES = ((0, 1), (3,), (2,))
 
 
 def solution(mesh):

time: 54.4 us -> 55.3 us (1.017)
  waiting for transfers between devices: 12.7 us -> 16.4 us
  starting transfers between devices: 30.4 us -> 27.1 us
  Pallas kernels: 10.8 us -> 11.6 us
    ppermute x6, waiting for transfers between devices: 3.4 us -> 11.7 us  [hop(): lax.ppermute(value, 'ep', [(i, far_ep(i, k)) for i in range(ep_count)])]
    ppermute x8, waiting for transfers between devices: 4.61 us -> 2.28 us  [cross(): return lax.ppermute(value, 'ep', [(i, i ^ 1) for i in range(ep_count)])]
    ppermute x8, starting transfers between devices: 11.1 us -> 9.25 us  [cross(): return lax.ppermute(value, 'ep', [(i, i ^ 1) for i in range(ep_count)])]
    ppermute x3, waiting for transfers between devices: 4.13 us -> 2.36 us  [hop_swap(): return lax.ppermute(value, ('ep', 'tp'), pairs)]
    ppermute x12 -> x4, starting transfers between devices: 2.33 us -> 1.44 us  [swap(): return lax.ppermute(value, 'tp', [(0, 1), (1, 0)])]
    pallas_call x13 -> x10, Pallas kernels: 10.8 us -> 11.6 us  [call(): pl.pallas_call(kernel, out_shape=outs, in_specs=in_specs or [pl.BlockSpec...]
    ppermute x12 -> x4, waiting for transfers between devices: 0.61 us -> 0.01 us  [swap(): return lax.ppermute(value, 'tp', [(0, 1), (1, 0)])]
  transfers between devices with their start and end apart: 29 -> 21, of which waited for: 11 -> 10; matrix products, arithmetic and copies ran while one was open for 0% -> 0% of each run, Pallas kernels for 15% -> 19%
where the time goes in v3:
time: 55.3 us; the launch traced here: 55.2 us
  starting transfers between devices  27.1 us (49%)
  waiting for transfers between devices  16.4 us (30%)
  Pallas kernels  11.6 us (21%)
    ppermute x6, starting transfers between devices, hop(): lax.ppermute(value, 'ep', [(i, far_ep(i, k)) for i in range(ep_count)])  13.6 us
    ppermute x6, waiting for transfers between devices, hop(): lax.ppermute(value, 'ep', [(i, far_ep(i, k)) for i in range(ep_count)])  11.7 us
    pallas_call x10, Pallas kernels, call(): pl.pallas_call(kernel, out_shape=outs, in_specs=in_specs or [pl.BlockSpec...  11.6 us
    ppermute x8, starting transfers between devices, cross(): return lax.ppermute(value, 'ep', [(i, i ^ 1) for i in range(ep_count)])  9.25 us
    ppermute x3, starting transfers between devices, hop_swap(): return lax.ppermute(value, ('ep', 'tp'), pairs)  2.83 us
    ppermute x3, waiting for transfers between devices, hop_swap(): return lax.ppermute(value, ('ep', 'tp'), pairs)  2.36 us
    ppermute x8, waiting for transfers between devices, cross(): return lax.ppermute(value, 'ep', [(i, i ^ 1) for i in range(ep_count)])  2.28 us
    ppermute x4, starting transfers between devices, swap(): return lax.ppermute(value, 'tp', [(0, 1), (1, 0)])  1.44 us
  transfers between devices with their start and end apart: 21, of which 10 were waited for; matrix products, arithmetic and copies ran while one was open for 0% of the time, Pallas kernels for 19%

profile of v3, /device:TPU:0, one launch (start us, length us, event | category | flops | bytes accessed | tf_op | source)
XLA Modules:
  0.0 55.2 jit_solution(10820880397436258949)
XLA Ops:
  0.0 0.5 collective-permute-start.3
  0.5 0.0 collective-permute-start.4
  0.5 0.5 collective-permute-start.5
  1.0 1.7 %shard_map.82 = (bf16[32,2176]{1,0:T(8,128)(2,1)S(1)}, bf16[32,2176]{1,0:T(8,128)(2,1)S(1)}, bf16[32,2176]{1,0:T(8,128)(2,1)S(1)}, bf16[32,2176]{1,0:T(8,128)(2,1)S(1)}, bf16[256,128]{1,0:T(8,128)(2,1)S(1)}) custom-call(bf16[128,2048]{1,0:T(8,128)(2,1)} %refs_0_.1, f32[1,2048]{1,0:T(1,128)} %bitcast.5, s32[4,128]{1,0:T(4,128)} %bitcast.6, f32[4,128]{1,0:T(4,128)} %bitcast.7), custom_call_target="tpu_custom_call" | custom-call | tf_op jit(solution)/shard_map/pallas_call | solution.py:217
  2.7 4.7 %collective-permute-start.16 = (bf16[32,2176]{1,0:T(8,128)(2,1)S(1)}, bf16[32,2176]{1,0:T(8,128)(2,1)S(1)}, u32[]{:S(2)}, u32[]{:S(2)}) collective-permute-start(bf16[32,2176]{1,0:T(8,128)(2,1)S(1)} %get-tuple-element.50), channel_id=1, source_target_pairs={{0,12},{2,14},{4,8},{6,10},{8,4},{10,6},{12,0},{14,2},{1,13},{3,15... | collective-permute-start | bytes 417800 | tf_op jit(solution)/shard_map/ppermute | solution.py:248
  7.3 0.0 collective-permute-start.11
  7.3 4.6 %collective-permute-done.16.refs_0_ = bf16[32,2176]{1,0:T(8,128)(2,1)S(1)} collective-permute-done((bf16[32,2176]{1,0:T(8,128)(2,1)S(1)}, bf16[32,2176]{1,0:T(8,128)(2,1)S(1)}, u32[]{:S(2)}, u32[]{:S(2)}) %collective-permute-start.16) | collective-permute-done | bytes 139296 | tf_op jit(solution)/shard_map/ppermute | solution.py:248
  12.0 5.9 %collective-permute-start.1 = (bf16[32,2176]{1,0:T(8,128)(2,1)S(1)}, bf16[32,2176]{1,0:T(8,128)(2,1)S(1)}, u32[]{:S(2)}, u32[]{:S(2)}) collective-permute-start(bf16[32,2176]{1,0:T(8,128)(2,1)S(1)} %get-tuple-element.33), channel_id=1, source_target_pairs={{0,4},{2,6},{4,0},{6,2},{8,12},{10,14},{12,8},{14,10},{1,5},{3,7},... | collective-permute-start | bytes 417800 | tf_op jit(solution)/shard_map/ppermute | solution.py:248
  17.8 2.1 %collective-permute-done.11.refs_0_ = bf16[32,2176]{1,0:T(8,128)(2,1)S(1)} collective-permute-done((bf16[32,2176]{1,0:T(8,128)(2,1)S(1)}, bf16[32,2176]{1,0:T(8,128)(2,1)S(1)}, u32[]{:S(2)}, u32[]{:S(2)}) %collective-permute-start.11) | collective-permute-done | bytes 139296 | tf_op jit(solution)/shard_map/ppermute | solution.py:248
  19.9 1.5 %collective-permute-start.17 = (bf16[32,2176]{1,0:T(8,128)(2,1)S(1)}, bf16[32,2176]{1,0:T(8,128)(2,1)S(1)}, u32[]{:S(2)}, u32[]{:S(2)}) collective-permute-start(bf16[32,2176]{1,0:T(8,128)(2,1)S(1)} %collective-permute-done.16.refs_0_), channel_id=1, source_target_pairs={{0,2},{2,0},{4,6},{6,4},{8,10},{10,8},{12,14},{14,12},{1,3},{3,1},... | collective-permute-start | bytes 417800 | tf_op jit(solution)/shard_map/ppermute | solution.py:257
  21.4 1.4 %collective-permute-done.1.refs_2_ = bf16[32,2176]{1,0:T(8,128)(2,1)S(1)} collective-permute-done((bf16[32,2176]{1,0:T(8,128)(2,1)S(1)}, bf16[32,2176]{1,0:T(8,128)(2,1)S(1)}, u32[]{:S(2)}, u32[]{:S(2)}) %collective-permute-start.1) | collective-permute-done | bytes 139296 | tf_op jit(solution)/shard_map/ppermute | solution.py:248
  22.8 1.5 %collective-permute-start.12 = (bf16[32,2176]{1,0:T(8,128)(2,1)S(1)}, bf16[32,2176]{1,0:T(8,128)(2,1)S(1)}, u32[]{:S(2)}, u32[]{:S(2)}) collective-permute-start(bf16[32,2176]{1,0:T(8,128)(2,1)S(1)} %collective-permute-done.11.refs_0_), channel_id=1, source_target_pairs={{0,2},{2,0},{4,6},{6,4},{8,10},{10,8},{12,14},{14,12},{1,3},{3,1},... | collective-permute-start | bytes 417800 | tf_op jit(solution)/shard_map/ppermute | solution.py:257
  24.3 0.8 %collective-permute-done.17.refs_1_ = bf16[32,2176]{1,0:T(8,128)(2,1)S(1)} collective-permute-done((bf16[32,2176]{1,0:T(8,128)(2,1)S(1)}, bf16[32,2176]{1,0:T(8,128)(2,1)S(1)}, u32[]{:S(2)}, u32[]{:S(2)}) %collective-permute-start.17) | collective-permute-done | bytes 139296 | tf_op jit(solution)/shard_map/ppermute | solution.py:257
  25.0 1.5 %collective-permute-start = (bf16[32,2176]{1,0:T(8,128)(2,1)S(1)}, bf16[32,2176]{1,0:T(8,128)(2,1)S(1)}, u32[]{:S(2)}, u32[]{:S(2)}) collective-permute-start(bf16[32,2176]{1,0:T(8,128)(2,1)S(1)} %get-tuple-element.32.refs_0_), channel_id=1, source_target_pairs={{0,2},{2,0},{4,6},{6,4},{8,10},{10,8},{12,14},{14,12},{1,3},{3,1},... | collective-permute-start | bytes 417800 | tf_op jit(solution)/shard_map/ppermute | solution.py:257
  26.5 0.5 collective-permute-start.2
  27.0 2.9 %shard_map.83 = (bf16[2,2048,256]{2,1,0:T(8,128)(2,1)S(1)}, bf16[2,2048,256]{2,1,0:T(8,128)(2,1)S(1)}, bf16[2,256,2048]{2,1,0:T(8,128)(2,1)S(1)}, bf16[128,256]{1,0:T(8,128)(2,1)S(1)}) custom-call(bf16[2,2048,256]{2,1,0:T(8,128)(2,1)} %wg_ref.1, bf16[2,2048,256]{2,1,0:T(8,128)(2,1)} %wu_ref.1, bf16[2,256,2048]{2,1,0:T(8,128)(2,1)} %wd_ref.1, ...), custom_call_target="tpu_custom_call" | custom-call | tf_op jit(solution)/shard_map/pallas_call | solution.py:217
  29.9 0.0 collective-permute-done.4.refs_8_.refs_6_
  29.9 1.8 %shard_map.89 = (f32[32,2048]{1,0:T(8,128)S(1)}, bf16[32,2048]{1,0:T(8,128)(2,1)S(1)}) custom-call(bf16[32,2176]{1,0:T(8,128)(2,1)S(1)} %collective-permute-done.16.refs_0_, bf16[32,2176]{1,0:T(8,128)(2,1)S(1)} %collective-permute-done.17.refs_1_, bf16[2,2048,256]{2,1,0:T(8,128)(2,1)S(1)} %get-tuple-element.34.refs_4_.refs_2_, ...), custom_call_target="tpu_custom_call" | custom-call | tf_op jit(solution)/shard_map/pallas_call | solution.py:217
  31.8 1.6 %collective-permute-start.18 = (bf16[32,2048]{1,0:T(8,128)(2,1)S(1)}, bf16[32,2048]{1,0:T(8,128)(2,1)S(1)}, u32[]{:S(2)}, u32[]{:S(2)}) collective-permute-start(bf16[32,2048]{1,0:T(8,128)(2,1)S(1)} %get-tuple-element.52), channel_id=1, source_target_pairs={{0,2},{2,0},{4,6},{6,4},{8,10},{10,8},{12,14},{14,12},{1,3},{3,1},... | collective-permute-start | bytes 393224 | tf_op jit(solution)/shard_map/ppermute | solution.py:257
  33.3 0.0 collective-permute-done.12.refs_1_
  33.3 1.8 %shard_map.87 = (f32[32,2048]{1,0:T(8,128)S(1)}, bf16[32,2048]{1,0:T(8,128)(2,1)S(1)}) custom-call(bf16[32,2176]{1,0:T(8,128)(2,1)S(1)} %collective-permute-done.11.refs_0_, bf16[32,2176]{1,0:T(8,128)(2,1)S(1)} %collective-permute-done.12.refs_1_, bf16[2,2048,256]{2,1,0:T(8,128)(2,1)S(1)} %get-tuple-element.34.refs_4_.refs_2_, ...), custom_call_target="tpu_custom_call" | custom-call | tf_op jit(solution)/shard_map/pallas_call | solution.py:217
  35.2 0.0 copy-start
  35.2 0.6 %collective-permute-start.13 = (bf16[32,2048]{1,0:T(8,128)(2,1)S(1)}, bf16[32,2048]{1,0:T(8,128)(2,1)S(1)}, u32[]{:S(2)}, u32[]{:S(2)}) collective-permute-start(bf16[32,2048]{1,0:T(8,128)(2,1)S(1)} %get-tuple-element.47), channel_id=1, source_target_pairs={{0,2},{2,0},{4,6},{6,4},{8,10},{10,8},{12,14},{14,12},{1,3},{3,1},... | collective-permute-start | bytes 393224 | tf_op jit(solution)/shard_map/ppermute | solution.py:257
  35.8 0.0 collective-permute-done.refs_1_
  35.8 0.0 collective-permute-done.2.refs_3_
  35.8 1.8 %shard_map.84 = (f32[32,2048]{1,0:T(8,128)S(1)}, bf16[32,2048]{1,0:T(8,128)(2,1)S(1)}, f32[32,2048]{1,0:T(8,128)S(1)}, bf16[32,2048]{1,0:T(8,128)(2,1)S(1)}) custom-call(bf16[32,2176]{1,0:T(8,128)(2,1)S(1)} %get-tuple-element.32.refs_0_, bf16[32,2176]{1,0:T(8,128)(2,1)S(1)} %collective-permute-done.refs_1_, ...), custom_call_target="tpu_custom_call" | custom-call | tf_op jit(solution)/shard_map/pallas_call | solution.py:217
  37.6 1.6 %collective-permute-start.8 = (bf16[32,2048]{1,0:T(8,128)(2,1)S(1)}, bf16[32,2048]{1,0:T(8,128)(2,1)S(1)}, u32[]{:S(2)}, u32[]{:S(2)}) collective-permute-start(bf16[32,2048]{1,0:T(8,128)(2,1)S(1)} %get-tuple-element.42), channel_id=1, source_target_pairs={{0,2},{2,0},{4,6},{6,4},{8,10},{10,8},{12,14},{14,12},{1,3},{3,1},... | collective-permute-start | bytes 393224 | tf_op jit(solution)/shard_map/ppermute | solution.py:257
  39.2 0.5 collective-permute-start.6
  39.7 0.1 shard_map.90
  39.9 2.5 %collective-permute-start.19 = (bf16[32,1024]{1,0:T(8,128)(2,1)S(1)}, bf16[32,1024]{1,0:T(8,128)(2,1)S(1)}, u32[]{:S(2)}, u32[]{:S(2)}) collective-permute-start(bf16[32,1024]{1,0:T(8,128)(2,1)S(1)} %get-tuple-element.53), channel_id=1, source_target_pairs={{0,12},{2,14},{4,8},{6,10},{8,4},{10,6},{12,0},{14,2},{1,13},{3,15... | collective-permute-start | bytes 196616 | tf_op jit(solution)/shard_map/ppermute | solution.py:248
  42.4 0.1 shard_map.88
  42.6 0.1 collective-permute-start.14
  42.6 1.5 %collective-permute-done.8.recv_ref = bf16[32,2048]{1,0:T(8,128)(2,1)S(1)} collective-permute-done((bf16[32,2048]{1,0:T(8,128)(2,1)S(1)}, bf16[32,2048]{1,0:T(8,128)(2,1)S(1)}, u32[]{:S(2)}, u32[]{:S(2)}) %collective-permute-start.8) | collective-permute-done | bytes 131104 | tf_op jit(solution)/shard_map/ppermute | solution.py:257
  44.2 2.2 %collective-permute-start.15 = (bf16[32,1024]{1,0:T(8,128)(2,1)S(1)}, bf16[32,1024]{1,0:T(8,128)(2,1)S(1)}, u32[]{:S(2)}, u32[]{:S(2)}) collective-permute-start(bf16[32,1024]{1,0:T(8,128)(2,1)S(1)} %get-tuple-element.49), channel_id=1, source_target_pairs={{0,9},{1,8},{2,11},{3,10},{4,13},{5,12},{6,15},{7,14},{8,1},{9,0},... | collective-permute-start | bytes 196616 | tf_op jit(solution)/shard_map/ppermute | solution.py:254
  46.3 0.1 shard_map.86
  46.5 0.0 collective-permute-done.6.recv_ref
  46.5 0.6 %collective-permute-start.10 = (bf16[32,1024]{1,0:T(8,128)(2,1)S(1)}, bf16[32,1024]{1,0:T(8,128)(2,1)S(1)}, u32[]{:S(2)}, u32[]{:S(2)}) collective-permute-start(bf16[32,1024]{1,0:T(8,128)(2,1)S(1)} %get-tuple-element.44), channel_id=1, source_target_pairs={{0,5},{1,4},{2,7},{3,6},{4,1},{5,0},{6,3},{7,2},{8,13},{9,12},{10,... | collective-permute-start | bytes 196616 | tf_op jit(solution)/shard_map/ppermute | solution.py:254
  47.1 0.1 shard_map.85
  47.3 0.0 collective-permute-done.19.refs_6_
  47.3 0.5 collective-permute-start.9
  47.7 0.5 collective-permute-done.20.refs_7_
  48.2 0.4 collective-permute-start.7
  48.6 3.0 %collective-permute-done.14.refs_4_ = bf16[32,1024]{1,0:T(8,128)(2,1)S(1)} collective-permute-done((bf16[32,1024]{1,0:T(8,128)(2,1)S(1)}, bf16[32,1024]{1,0:T(8,128)(2,1)S(1)}, u32[]{:S(2)}, u32[]{:S(2)}) %collective-permute-start.14) | collective-permute-done | bytes 65568 | tf_op jit(solution)/shard_map/ppermute | solution.py:248
  51.7 1.4 %collective-permute-done.15.refs_5_ = bf16[32,1024]{1,0:T(8,128)(2,1)S(1)} collective-permute-done((bf16[32,1024]{1,0:T(8,128)(2,1)S(1)}, bf16[32,1024]{1,0:T(8,128)(2,1)S(1)}, u32[]{:S(2)}, u32[]{:S(2)}) %collective-permute-start.15) | collective-permute-done | bytes 65568 | tf_op jit(solution)/shard_map/ppermute | solution.py:254
  53.1 0.4 collective-permute-done.10.refs_3_
  53.6 0.6 %collective-permute-done.9.refs_2_ = bf16[32,1024]{1,0:T(8,128)(2,1)S(1)} collective-permute-done((bf16[32,1024]{1,0:T(8,128)(2,1)S(1)}, bf16[32,1024]{1,0:T(8,128)(2,1)S(1)}, u32[]{:S(2)}, u32[]{:S(2)}) %collective-permute-start.9) | collective-permute-done | bytes 65568 | tf_op jit(solution)/shard_map/ppermute | solution.py:248
  54.2 0.0 collective-permute-done.7.refs_1_
  54.2 1.0 %shard_map.91 = bf16[128,1024]{1,0:T(8,128)(2,1)} custom-call(bf16[128,256]{1,0:T(8,128)(2,1)S(1)} %get-tuple-element.31.map_ref, f32[1,1024]{1,0:T(1,128)S(1)} %bitcast.4, bf16[32,1024]{1,0:T(8,128)(2,1)S(1)} %get-tuple-element.39.refs_0_, bf16[32,1024]{1,0:T(8,128)(2,1)S(1)} %collective-permute-done.7.refs_1_, ...), custom_call_target="tpu_custom_call" | custom-call | tf_op jit(solution)/shard_map/pallas_call | solution.py:217
  (6 shorter events, 0.0 us)
Async XLA Ops:
  0.0 26.5 %collective-permute-start.3 = (bf16[2,2048,256]{2,1,0:T(8,128)(2,1)}, bf16[2,2048,256]{2,1,0:T(8,128)(2,1)S(1)}, u32[]{:S(2)}, u32[]{:S(2)}) collective-permute-start(bf16[2,2048,256]{2,1,0:T(8,128)(2,1)} %wg_ref.1), channel_id=1, source_target_pairs={{0,1},{1,0},{2,3},{3,2},{4,5},{5,4},{6,7},{7,6},{8,9},{9,8},{10,11... | collective-permute-start | bytes 6291464 | tf_op jit(solution)/shard_map/ppermute | solution.py:260
  0.5 29.4 %collective-permute-start.4 = (bf16[2,2048,256]{2,1,0:T(8,128)(2,1)}, bf16[2,2048,256]{2,1,0:T(8,128)(2,1)S(1)}, u32[]{:S(2)}, u32[]{:S(2)}) collective-permute-start(bf16[2,2048,256]{2,1,0:T(8,128)(2,1)} %wu_ref.1), channel_id=1, source_target_pairs={{0,1},{1,0},{2,3},{3,2},{4,5},{5,4},{6,7},{7,6},{8,9},{9,8},{10,11... | collective-permute-start | bytes 6291464 | tf_op jit(solution)/shard_map/ppermute | solution.py:260
  0.5 29.4 %collective-permute-start.5 = (bf16[2,256,2048]{2,1,0:T(8,128)(2,1)}, bf16[2,256,2048]{2,1,0:T(8,128)(2,1)S(1)}, u32[]{:S(2)}, u32[]{:S(2)}) collective-permute-start(bf16[2,256,2048]{2,1,0:T(8,128)(2,1)} %wd_ref.1), channel_id=1, source_target_pairs={{0,1},{1,0},{2,3},{3,2},{4,5},{5,4},{6,7},{7,6},{8,9},{9,8},{10,11... | collective-permute-start | bytes 6291464 | tf_op jit(solution)/shard_map/ppermute | solution.py:260
  2.7 9.3 %collective-permute-start.16 = (bf16[32,2176]{1,0:T(8,128)(2,1)S(1)}, bf16[32,2176]{1,0:T(8,128)(2,1)S(1)}, u32[]{:S(2)}, u32[]{:S(2)}) collective-permute-start(bf16[32,2176]{1,0:T(8,128)(2,1)S(1)} %get-tuple-element.50), channel_id=1, source_target_pairs={{0,12},{2,14},{4,8},{6,10},{8,4},{10,6},{12,0},{14,2},{1,13},{3,15... | collective-permute-start | bytes 417800 | tf_op jit(solution)/shard_map/ppermute | solution.py:248
  7.3 12.5 %collective-permute-start.11 = (bf16[32,2176]{1,0:T(8,128)(2,1)S(1)}, bf16[32,2176]{1,0:T(8,128)(2,1)S(1)}, u32[]{:S(2)}, u32[]{:S(2)}) collective-permute-start(bf16[32,2176]{1,0:T(8,128)(2,1)S(1)} %get-tuple-element.45), channel_id=1, source_target_pairs={{0,8},{2,10},{4,12},{6,14},{8,0},{10,2},{12,4},{14,6},{1,9},{3,11}... | collective-permute-start | bytes 417800 | tf_op jit(solution)/shard_map/ppermute | solution.py:248
  12.0 10.8 %collective-permute-start.1 = (bf16[32,2176]{1,0:T(8,128)(2,1)S(1)}, bf16[32,2176]{1,0:T(8,128)(2,1)S(1)}, u32[]{:S(2)}, u32[]{:S(2)}) collective-permute-start(bf16[32,2176]{1,0:T(8,128)(2,1)S(1)} %get-tuple-element.33), channel_id=1, source_target_pairs={{0,4},{2,6},{4,0},{6,2},{8,12},{10,14},{12,8},{14,10},{1,5},{3,7},... | collective-permute-start | bytes 417800 | tf_op jit(solution)/shard_map/ppermute | solution.py:248
  19.9 5.1 %collective-permute-start.17 = (bf16[32,2176]{1,0:T(8,128)(2,1)S(1)}, bf16[32,2176]{1,0:T(8,128)(2,1)S(1)}, u32[]{:S(2)}, u32[]{:S(2)}) collective-permute-start(bf16[32,2176]{1,0:T(8,128)(2,1)S(1)} %collective-permute-done.16.refs_0_), channel_id=1, source_target_pairs={{0,2},{2,0},{4,6},{6,4},{8,10},{10,8},{12,14},{14,12},{1,3},{3,1},... | collective-permute-start | bytes 417800 | tf_op jit(solution)/shard_map/ppermute | solution.py:257
  22.8 10.6 %collective-permute-start.12 = (bf16[32,2176]{1,0:T(8,128)(2,1)S(1)}, bf16[32,2176]{1,0:T(8,128)(2,1)S(1)}, u32[]{:S(2)}, u32[]{:S(2)}) collective-permute-start(bf16[32,2176]{1,0:T(8,128)(2,1)S(1)} %collective-permute-done.11.refs_0_), channel_id=1, source_target_pairs={{0,2},{2,0},{4,6},{6,4},{8,10},{10,8},{12,14},{14,12},{1,3},{3,1},... | collective-permute-start | bytes 417800 | tf_op jit(solution)/shard_map/ppermute | solution.py:257
  25.0 10.8 %collective-permute-start = (bf16[32,2176]{1,0:T(8,128)(2,1)S(1)}, bf16[32,2176]{1,0:T(8,128)(2,1)S(1)}, u32[]{:S(2)}, u32[]{:S(2)}) collective-permute-start(bf16[32,2176]{1,0:T(8,128)(2,1)S(1)} %get-tuple-element.32.refs_0_), channel_id=1, source_target_pairs={{0,2},{2,0},{4,6},{6,4},{8,10},{10,8},{12,14},{14,12},{1,3},{3,1},... | collective-permute-start | bytes 417800 | tf_op jit(solution)/shard_map/ppermute | solution.py:257
  26.5 9.3 %collective-permute-start.2 = (bf16[32,2176]{1,0:T(8,128)(2,1)S(1)}, bf16[32,2176]{1,0:T(8,128)(2,1)S(1)}, u32[]{:S(2)}, u32[]{:S(2)}) collective-permute-start(bf16[32,2176]{1,0:T(8,128)(2,1)S(1)} %collective-permute-done.1.refs_2_), channel_id=1, source_target_pairs={{0,2},{2,0},{4,6},{6,4},{8,10},{10,8},{12,14},{14,12},{1,3},{3,1},... | collective-permute-start | bytes 417800 | tf_op jit(solution)/shard_map/ppermute | solution.py:257
  31.8 8.0 %collective-permute-start.18 = (bf16[32,2048]{1,0:T(8,128)(2,1)S(1)}, bf16[32,2048]{1,0:T(8,128)(2,1)S(1)}, u32[]{:S(2)}, u32[]{:S(2)}) collective-permute-start(bf16[32,2048]{1,0:T(8,128)(2,1)S(1)} %get-tuple-element.52), channel_id=1, source_target_pairs={{0,2},{2,0},{4,6},{6,4},{8,10},{10,8},{12,14},{14,12},{1,3},{3,1},... | collective-permute-start | bytes 393224 | tf_op jit(solution)/shard_map/ppermute | solution.py:257
  35.2 19.0 %copy-start = (f32[1024]{0:T(1024)S(1)}, f32[1024]{0:T(1024)}, u32[]{:S(2)}) copy-start(f32[1024]{0:T(1024)} %param.15) | copy-start | bytes 12292
  35.2 7.2 %collective-permute-start.13 = (bf16[32,2048]{1,0:T(8,128)(2,1)S(1)}, bf16[32,2048]{1,0:T(8,128)(2,1)S(1)}, u32[]{:S(2)}, u32[]{:S(2)}) collective-permute-start(bf16[32,2048]{1,0:T(8,128)(2,1)S(1)} %get-tuple-element.47), channel_id=1, source_target_pairs={{0,2},{2,0},{4,6},{6,4},{8,10},{10,8},{12,14},{14,12},{1,3},{3,1},... | collective-permute-start | bytes 393224 | tf_op jit(solution)/shard_map/ppermute | solution.py:257
  37.6 6.5 %collective-permute-start.8 = (bf16[32,2048]{1,0:T(8,128)(2,1)S(1)}, bf16[32,2048]{1,0:T(8,128)(2,1)S(1)}, u32[]{:S(2)}, u32[]{:S(2)}) collective-permute-start(bf16[32,2048]{1,0:T(8,128)(2,1)S(1)} %get-tuple-element.42), channel_id=1, source_target_pairs={{0,2},{2,0},{4,6},{6,4},{8,10},{10,8},{12,14},{14,12},{1,3},{3,1},... | collective-permute-start | bytes 393224 | tf_op jit(solution)/shard_map/ppermute | solution.py:257
  39.2 7.3 %collective-permute-start.6 = (bf16[32,2048]{1,0:T(8,128)(2,1)S(1)}, bf16[32,2048]{1,0:T(8,128)(2,1)S(1)}, u32[]{:S(2)}, u32[]{:S(2)}) collective-permute-start(bf16[32,2048]{1,0:T(8,128)(2,1)S(1)} %get-tuple-element.38), channel_id=1, source_target_pairs={{0,2},{2,0},{4,6},{6,4},{8,10},{10,8},{12,14},{14,12},{1,3},{3,1},... | collective-permute-start | bytes 393224 | tf_op jit(solution)/shard_map/ppermute | solution.py:257
  39.9 7.4 %collective-permute-start.19 = (bf16[32,1024]{1,0:T(8,128)(2,1)S(1)}, bf16[32,1024]{1,0:T(8,128)(2,1)S(1)}, u32[]{:S(2)}, u32[]{:S(2)}) collective-permute-start(bf16[32,1024]{1,0:T(8,128)(2,1)S(1)} %get-tuple-element.53), channel_id=1, source_target_pairs={{0,12},{2,14},{4,8},{6,10},{8,4},{10,6},{12,0},{14,2},{1,13},{3,15... | collective-permute-start | bytes 196616 | tf_op jit(solution)/shard_map/ppermute | solution.py:248
  42.4 5.8 %collective-permute-start.20 = (bf16[32,1024]{1,0:T(8,128)(2,1)S(1)}, bf16[32,1024]{1,0:T(8,128)(2,1)S(1)}, u32[]{:S(2)}, u32[]{:S(2)}) collective-permute-start(bf16[32,1024]{1,0:T(8,128)(2,1)S(1)} %get-tuple-element.54), channel_id=1, source_target_pairs={{0,13},{1,12},{2,15},{3,14},{4,9},{5,8},{6,11},{7,10},{8,5},{9,4},... | collective-permute-start | bytes 196616 | tf_op jit(solution)/shard_map/ppermute | solution.py:254
  42.6 9.1 %collective-permute-start.14 = (bf16[32,1024]{1,0:T(8,128)(2,1)S(1)}, bf16[32,1024]{1,0:T(8,128)(2,1)S(1)}, u32[]{:S(2)}, u32[]{:S(2)}) collective-permute-start(bf16[32,1024]{1,0:T(8,128)(2,1)S(1)} %get-tuple-element.48), channel_id=1, source_target_pairs={{0,8},{2,10},{4,12},{6,14},{8,0},{10,2},{12,4},{14,6},{1,9},{3,11}... | collective-permute-start | bytes 196616 | tf_op jit(solution)/shard_map/ppermute | solution.py:248
  44.2 9.0 %collective-permute-start.15 = (bf16[32,1024]{1,0:T(8,128)(2,1)S(1)}, bf16[32,1024]{1,0:T(8,128)(2,1)S(1)}, u32[]{:S(2)}, u32[]{:S(2)}) collective-permute-start(bf16[32,1024]{1,0:T(8,128)(2,1)S(1)} %get-tuple-element.49), channel_id=1, source_target_pairs={{0,9},{1,8},{2,11},{3,10},{4,13},{5,12},{6,15},{7,14},{8,1},{9,0},... | collective-permute-start | bytes 196616 | tf_op jit(solution)/shard_map/ppermute | solution.py:254
  46.5 7.1 %collective-permute-start.10 = (bf16[32,1024]{1,0:T(8,128)(2,1)S(1)}, bf16[32,1024]{1,0:T(8,128)(2,1)S(1)}, u32[]{:S(2)}, u32[]{:S(2)}) collective-permute-start(bf16[32,1024]{1,0:T(8,128)(2,1)S(1)} %get-tuple-element.44), channel_id=1, source_target_pairs={{0,5},{1,4},{2,7},{3,6},{4,1},{5,0},{6,3},{7,2},{8,13},{9,12},{10,... | collective-permute-start | bytes 196616 | tf_op jit(solution)/shard_map/ppermute | solution.py:254
  47.3 6.9 %collective-permute-start.9 = (bf16[32,1024]{1,0:T(8,128)(2,1)S(1)}, bf16[32,1024]{1,0:T(8,128)(2,1)S(1)}, u32[]{:S(2)}, u32[]{:S(2)}) collective-permute-start(bf16[32,1024]{1,0:T(8,128)(2,1)S(1)} %get-tuple-element.43), channel_id=1, source_target_pairs={{0,4},{2,6},{4,0},{6,2},{8,12},{10,14},{12,8},{14,10},{1,5},{3,7},... | collective-permute-start | bytes 196616 | tf_op jit(solution)/shard_map/ppermute | solution.py:248
  48.2 6.0 %collective-permute-start.7 = (bf16[32,1024]{1,0:T(8,128)(2,1)S(1)}, bf16[32,1024]{1,0:T(8,128)(2,1)S(1)}, u32[]{:S(2)}, u32[]{:S(2)}) collective-permute-start(bf16[32,1024]{1,0:T(8,128)(2,1)S(1)} %get-tuple-element.40), channel_id=1, source_target_pairs={{0,1},{1,0},{2,3},{3,2},{4,5},{5,4},{6,7},{7,6},{8,9},{9,8},{10,11... | collective-permute-start | bytes 196616 | tf_op jit(solution)/shard_map/ppermute | solution.py:260

commit v4 on v3

--- a/solution.py
+++ b/solution.py
@@ -107,7 +107,8 @@
     before = (iota((tok_dev, tok_dev), 0) < iota((tok_dev, tok_dev), 1)).astype(jnp.bfloat16)
     earlier = dot(member.astype(jnp.bfloat16), before)
     rank = jnp.sum(earlier * member, axis=0, keepdims=True).astype(jnp.int32)
-    relative = group ^ my_group
+    relative = group - my_group
+    relative += jnp.where(relative < 0, GROUPS, 0)
     send_slot = iota((GROUPS * half, tok_dev), 0)
     pick = (
         (relative == send_slot // half) & (rank == send_slot % half + my_half * half)
@@ -201,15 +202,28 @@
     ]
 
 
+def join_whole_kernel(keep_ref, recv_ref, out_ref):
+    rows = keep_ref[...] + recv_ref[...].astype(jnp.float32)
+    mean = jnp.sum(rows * rows, axis=1, keepdims=True) / rows.shape[1]
+    out_ref[...] = (rows * lax.rsqrt(mean + EPS)).astype(jnp.bfloat16)
+
+
 def close_kernel(cap, map_ref, gain_ref, *refs):
     parts, out_ref, rows_ref = refs[: 2 * GROUPS], refs[-2], refs[-1]
     half = cap // 2
+    half_width = out_ref.shape[1]
     my_half = lax.axis_index("tp")
+
+    def features(ref):
+        if ref.shape[1] == half_width:
+            return ref[...]
+        return ref[:, pl.ds(pl.multiple_of(my_half * half_width, half_width), half_width)]
+
     for k in range(GROUPS):
         same = pl.multiple_of(k * cap + my_half * half, half)
         other = pl.multiple_of(k * cap + (1 - my_half) * half, half)
-        rows_ref[pl.ds(same, half), :] = parts[2 * k][...]
-        rows_ref[pl.ds(other, half), :] = parts[2 * k + 1][...]
+        rows_ref[pl.ds(same, half), :] = features(parts[2 * k])
+        rows_ref[pl.ds(other, half), :] = features(parts[2 * k + 1])
     out_ref[...] = (dot(map_ref[...], rows_ref[...]) * gain_ref[...]).astype(jnp.bfloat16)
 
 
@@ -223,7 +237,8 @@
     )(*args)
 
 
-STAGES = ((0, 1), (3,), (2,))
+STAGES = ((0, 1), (2,), (3,))
+SPLIT = (3,)
 
 
 def dense_body(tokens, in_gain, routing, gate_prob, w_gate, w_up, w_down, out_gain):
@@ -242,7 +257,7 @@
     in_vmem = pl.BlockSpec(memory_space=pltpu.VMEM)
 
     def far_ep(i, k):
-        return ((i // members) ^ k) * members + i % members
+        return (i // members + k) % GROUPS * members + i % members
 
     def hop(value, k):
         return lax.ppermute(value, "ep", [(i, far_ep(i, k)) for i in range(ep_count)])
@@ -307,18 +322,21 @@
             (pltpu.VMEM((max(n * cap, LANES), model_width + LANES), bf16),),
         )
         for c, k in enumerate(ks):
-            same, other = call(
-                join_kernel,
-                [sds((half, half_width), bf16)] * 2,
-                (sums[2 * c], cross(sums[2 * c + 1])),
-                8,
-                (pltpu.VMEM((half, model_width), bf16),),
-            )
-            if k == 0:
-                back[:2] = same, swap(other)
+            keep, recv = sums[2 * c], cross(sums[2 * c + 1])
+            if k in SPLIT:
+                same, other = call(
+                    join_kernel,
+                    [sds((half, half_width), bf16)] * 2,
+                    (keep, recv),
+                    8,
+                    (pltpu.VMEM((half, model_width), bf16),),
+                )
+                back[2 * k] = hop(same, -k)
+                back[2 * k + 1] = hop_swap(other, -k)
             else:
-                back[2 * k] = hop(same, k)
-                back[2 * k + 1] = hop_swap(other, k)
+                mixed = call(join_whole_kernel, sds((half, model_width), bf16), (keep, recv), 8)
+                home = hop(mixed, -k) if k else mixed
+                back[2 * k : 2 * k + 2] = home, swap(home)
 
     for ks in STAGES:
         experts(ks)

time: 55.3 us -> 55.1 us (level)
  starting transfers between devices: 27.1 us -> 20.2 us
  waiting for transfers between devices: 16.4 us -> 23 us
    ppermute x8, waiting for transfers between devices: 2.28 us -> 11.2 us  [cross(): return lax.ppermute(value, 'ep', [(i, i ^ 1) for i in range(ep_count)])]
    ppermute x6, starting transfers between devices: 13.6 us -> 8.09 us  [hop(): lax.ppermute(value, 'ep', [(i, far_ep(i, k)) for i in range(ep_count)])]
    ppermute x3 -> x1, starting transfers between devices: 2.83 us -> 0.06 us  [hop_swap(): return lax.ppermute(value, ('ep', 'tp'), pairs)]
    ppermute x3 -> x1, waiting for transfers between devices: 2.36 us -> 0.01 us  [hop_swap(): return lax.ppermute(value, ('ep', 'tp'), pairs)]
    ppermute x8, starting transfers between devices: 9.25 us -> 10.4 us  [cross(): return lax.ppermute(value, 'ep', [(i, i ^ 1) for i in range(ep_count)])]
    ppermute x4 -> x6, starting transfers between devices: 1.44 us -> 1.65 us  [swap(): return lax.ppermute(value, 'tp', [(0, 1), (1, 0)])]
  transfers between devices with their start and end apart: 21 -> 21, of which waited for: 10 -> 7; matrix products, arithmetic and copies ran while one was open for 0% -> 0% of each run, Pallas kernels for 19% -> 19%
where the time goes in v4:
time: 55.1 us; the launch traced here: 54.9 us
  waiting for transfers between devices  23 us (42%)
  starting transfers between devices  20.2 us (37%)
  Pallas kernels  11.6 us (21%)
    ppermute x6, waiting for transfers between devices, hop(): lax.ppermute(value, 'ep', [(i, far_ep(i, k)) for i in range(ep_count)])  11.7 us
    pallas_call x10, Pallas kernels, call(): pl.pallas_call(kernel, out_shape=outs, in_specs=in_specs or [pl.BlockSpec...  11.6 us
    ppermute x8, waiting for transfers between devices, cross(): return lax.ppermute(value, 'ep', [(i, i ^ 1) for i in range(ep_count)])  11.2 us
    ppermute x8, starting transfers between devices, cross(): return lax.ppermute(value, 'ep', [(i, i ^ 1) for i in range(ep_count)])  10.4 us
    ppermute x6, starting transfers between devices, hop(): lax.ppermute(value, 'ep', [(i, far_ep(i, k)) for i in range(ep_count)])  8.09 us
    ppermute x6, starting transfers between devices, swap(): return lax.ppermute(value, 'tp', [(0, 1), (1, 0)])  1.65 us
  transfers between devices with their start and end apart: 21, of which 7 were waited for; matrix products, arithmetic and copies ran while one was open for 0% of the time, Pallas kernels for 19%

profile of v4, /device:TPU:0, one launch (start us, length us, event | category | flops | bytes accessed | tf_op | source)
XLA Modules:
  0.0 54.9 jit_solution(5540400322247809088)
XLA Ops:
  0.0 0.5 collective-permute-start.3
  0.5 0.0 collective-permute-start.4
  0.5 0.5 collective-permute-start.5
  1.0 1.7 %shard_map.82 = (bf16[32,2176]{1,0:T(8,128)(2,1)S(1)}, bf16[32,2176]{1,0:T(8,128)(2,1)S(1)}, bf16[32,2176]{1,0:T(8,128)(2,1)S(1)}, bf16[32,2176]{1,0:T(8,128)(2,1)S(1)}, bf16[256,128]{1,0:T(8,128)(2,1)S(1)}) custom-call(bf16[128,2048]{1,0:T(8,128)(2,1)} %refs_0_.1, f32[1,2048]{1,0:T(1,128)} %bitcast.5, s32[4,128]{1,0:T(4,128)} %bitcast.6, f32[4,128]{1,0:T(4,128)} %bitcast.7), custom_call_target="tpu_custom_call" | custom-call | tf_op jit(solution)/shard_map/pallas_call | solution.py:231
  2.7 2.5 %collective-permute-start = (bf16[32,2176]{1,0:T(8,128)(2,1)S(1)}, bf16[32,2176]{1,0:T(8,128)(2,1)S(1)}, u32[]{:S(2)}, u32[]{:S(2)}) collective-permute-start(bf16[32,2176]{1,0:T(8,128)(2,1)S(1)} %get-tuple-element.26.refs_0_), channel_id=1, source_target_pairs={{0,2},{2,0},{4,6},{6,4},{8,10},{10,8},{12,14},{14,12},{1,3},{3,1},... | collective-permute-start | bytes 417800 | tf_op jit(solution)/shard_map/ppermute | solution.py:272
  5.2 1.6 %collective-permute-start.1 = (bf16[32,2176]{1,0:T(8,128)(2,1)S(1)}, bf16[32,2176]{1,0:T(8,128)(2,1)S(1)}, u32[]{:S(2)}, u32[]{:S(2)}) collective-permute-start(bf16[32,2176]{1,0:T(8,128)(2,1)S(1)} %get-tuple-element.27), channel_id=1, source_target_pairs={{0,4},{2,6},{4,8},{6,10},{8,12},{10,14},{12,0},{14,2},{1,5},{3,7},... | collective-permute-start | bytes 417800 | tf_op jit(solution)/shard_map/ppermute | solution.py:263
  6.8 2.8 %collective-permute-done.refs_1_ = bf16[32,2176]{1,0:T(8,128)(2,1)S(1)} collective-permute-done((bf16[32,2176]{1,0:T(8,128)(2,1)S(1)}, bf16[32,2176]{1,0:T(8,128)(2,1)S(1)}, u32[]{:S(2)}, u32[]{:S(2)}) %collective-permute-start) | collective-permute-done | bytes 139296 | tf_op jit(solution)/shard_map/ppermute | solution.py:272
  9.6 2.8 %collective-permute-start.11 = (bf16[32,2176]{1,0:T(8,128)(2,1)S(1)}, bf16[32,2176]{1,0:T(8,128)(2,1)S(1)}, u32[]{:S(2)}, u32[]{:S(2)}) collective-permute-start(bf16[32,2176]{1,0:T(8,128)(2,1)S(1)} %get-tuple-element.35), channel_id=1, source_target_pairs={{0,8},{2,10},{4,12},{6,14},{8,0},{10,2},{12,4},{14,6},{1,9},{3,11}... | collective-permute-start | bytes 417800 | tf_op jit(solution)/shard_map/ppermute | solution.py:263
  12.4 0.5 collective-permute-done.1.refs_2_
  12.9 1.0 %collective-permute-start.2 = (bf16[32,2176]{1,0:T(8,128)(2,1)S(1)}, bf16[32,2176]{1,0:T(8,128)(2,1)S(1)}, u32[]{:S(2)}, u32[]{:S(2)}) collective-permute-start(bf16[32,2176]{1,0:T(8,128)(2,1)S(1)} %collective-permute-done.1.refs_2_), channel_id=1, source_target_pairs={{0,2},{2,0},{4,6},{6,4},{8,10},{10,8},{12,14},{14,12},{1,3},{3,1},... | collective-permute-start | bytes 417800 | tf_op jit(solution)/shard_map/ppermute | solution.py:272
  13.9 5.1 %collective-permute-done.11.refs_0_ = bf16[32,2176]{1,0:T(8,128)(2,1)S(1)} collective-permute-done((bf16[32,2176]{1,0:T(8,128)(2,1)S(1)}, bf16[32,2176]{1,0:T(8,128)(2,1)S(1)}, u32[]{:S(2)}, u32[]{:S(2)}) %collective-permute-start.11) | collective-permute-done | bytes 139296 | tf_op jit(solution)/shard_map/ppermute | solution.py:263
  19.0 1.5 %collective-permute-start.12 = (bf16[32,2176]{1,0:T(8,128)(2,1)S(1)}, bf16[32,2176]{1,0:T(8,128)(2,1)S(1)}, u32[]{:S(2)}, u32[]{:S(2)}) collective-permute-start(bf16[32,2176]{1,0:T(8,128)(2,1)S(1)} %collective-permute-done.11.refs_0_), channel_id=1, source_target_pairs={{0,2},{2,0},{4,6},{6,4},{8,10},{10,8},{12,14},{14,12},{1,3},{3,1},... | collective-permute-start | bytes 417800 | tf_op jit(solution)/shard_map/ppermute | solution.py:272
  20.4 0.0 collective-permute-done.2.refs_3_
  20.4 3.5 %collective-permute-start.16 = (bf16[32,2176]{1,0:T(8,128)(2,1)S(1)}, bf16[32,2176]{1,0:T(8,128)(2,1)S(1)}, u32[]{:S(2)}, u32[]{:S(2)}) collective-permute-start(bf16[32,2176]{1,0:T(8,128)(2,1)S(1)} %get-tuple-element.38), channel_id=1, source_target_pairs={{0,12},{2,14},{4,0},{6,2},{8,4},{10,6},{12,8},{14,10},{1,13},{3,15... | collective-permute-start | bytes 417800 | tf_op jit(solution)/shard_map/ppermute | solution.py:263
  23.9 2.9 %shard_map.83 = (bf16[2,2048,256]{2,1,0:T(8,128)(2,1)S(1)}, bf16[2,2048,256]{2,1,0:T(8,128)(2,1)S(1)}, bf16[2,256,2048]{2,1,0:T(8,128)(2,1)S(1)}, bf16[128,256]{1,0:T(8,128)(2,1)S(1)}) custom-call(bf16[2,2048,256]{2,1,0:T(8,128)(2,1)} %wg_ref.1, bf16[2,2048,256]{2,1,0:T(8,128)(2,1)} %wu_ref.1, bf16[2,256,2048]{2,1,0:T(8,128)(2,1)} %wd_ref.1, ...), custom_call_target="tpu_custom_call" | custom-call | tf_op jit(solution)/shard_map/pallas_call | solution.py:231
  26.8 0.0 collective-permute-done.3.refs_7_.refs_5_
  26.8 0.0 collective-permute-done.4.refs_8_.refs_6_
  26.8 0.0 collective-permute-done.5.refs_9_.refs_7_
  26.8 1.9 %shard_map.84 = (f32[32,2048]{1,0:T(8,128)S(1)}, bf16[32,2048]{1,0:T(8,128)(2,1)S(1)}, f32[32,2048]{1,0:T(8,128)S(1)}, bf16[32,2048]{1,0:T(8,128)(2,1)S(1)}) custom-call(bf16[32,2176]{1,0:T(8,128)(2,1)S(1)} %get-tuple-element.26.refs_0_, bf16[32,2176]{1,0:T(8,128)(2,1)S(1)} %collective-permute-done.refs_1_, ...), custom_call_target="tpu_custom_call" | custom-call | tf_op jit(solution)/shard_map/pallas_call | solution.py:231
  28.7 0.6 %collective-permute-start.8 = (bf16[32,2048]{1,0:T(8,128)(2,1)S(1)}, bf16[32,2048]{1,0:T(8,128)(2,1)S(1)}, u32[]{:S(2)}, u32[]{:S(2)}) collective-permute-start(bf16[32,2048]{1,0:T(8,128)(2,1)S(1)} %get-tuple-element.34), channel_id=1, source_target_pairs={{0,2},{2,0},{4,6},{6,4},{8,10},{10,8},{12,14},{14,12},{1,3},{3,1},... | collective-permute-start | bytes 393224 | tf_op jit(solution)/shard_map/ppermute | solution.py:272
  29.3 0.0 collective-permute-done.12.refs_1_
  29.3 1.8 %shard_map.87 = (f32[32,2048]{1,0:T(8,128)S(1)}, bf16[32,2048]{1,0:T(8,128)(2,1)S(1)}) custom-call(bf16[32,2176]{1,0:T(8,128)(2,1)S(1)} %collective-permute-done.11.refs_0_, bf16[32,2176]{1,0:T(8,128)(2,1)S(1)} %collective-permute-done.12.refs_1_, bf16[2,2048,256]{2,1,0:T(8,128)(2,1)S(1)} %get-tuple-element.28.refs_4_.refs_2_, ...), custom_call_target="tpu_custom_call" | custom-call | tf_op jit(solution)/shard_map/pallas_call | solution.py:231
  31.1 1.6 %collective-permute-start.13 = (bf16[32,2048]{1,0:T(8,128)(2,1)S(1)}, bf16[32,2048]{1,0:T(8,128)(2,1)S(1)}, u32[]{:S(2)}, u32[]{:S(2)}) collective-permute-start(bf16[32,2048]{1,0:T(8,128)(2,1)S(1)} %get-tuple-element.37), channel_id=1, source_target_pairs={{0,2},{2,0},{4,6},{6,4},{8,10},{10,8},{12,14},{14,12},{1,3},{3,1},... | collective-permute-start | bytes 393224 | tf_op jit(solution)/shard_map/ppermute | solution.py:272
  32.7 0.0 collective-permute-done.16.refs_0_
  32.7 0.5 collective-permute-start.17
  33.2 1.5 %collective-permute-start.6 = (bf16[32,2048]{1,0:T(8,128)(2,1)S(1)}, bf16[32,2048]{1,0:T(8,128)(2,1)S(1)}, u32[]{:S(2)}, u32[]{:S(2)}) collective-permute-start(bf16[32,2048]{1,0:T(8,128)(2,1)S(1)} %get-tuple-element.32), channel_id=1, source_target_pairs={{0,2},{2,0},{4,6},{6,4},{8,10},{10,8},{12,14},{14,12},{1,3},{3,1},... | collective-permute-start | bytes 393224 | tf_op jit(solution)/shard_map/ppermute | solution.py:272
  34.7 0.1 shard_map.86
  34.8 0.1 collective-permute-start.9
  34.9 2.6 %collective-permute-done.13.recv_ref = bf16[32,2048]{1,0:T(8,128)(2,1)S(1)} collective-permute-done((bf16[32,2048]{1,0:T(8,128)(2,1)S(1)}, bf16[32,2048]{1,0:T(8,128)(2,1)S(1)}, u32[]{:S(2)}, u32[]{:S(2)}) %collective-permute-start.13) | collective-permute-done | bytes 131104 | tf_op jit(solution)/shard_map/ppermute | solution.py:272
  37.5 0.1 shard_map.88
  37.7 0.0 copy-start
  37.7 0.1 collective-permute-start.14
  37.8 2.8 %collective-permute-done.17.refs_1_ = bf16[32,2176]{1,0:T(8,128)(2,1)S(1)} collective-permute-done((bf16[32,2176]{1,0:T(8,128)(2,1)S(1)}, bf16[32,2176]{1,0:T(8,128)(2,1)S(1)}, u32[]{:S(2)}, u32[]{:S(2)}) %collective-permute-start.17) | collective-permute-done | bytes 139296 | tf_op jit(solution)/shard_map/ppermute | solution.py:272
  40.5 1.8 %shard_map.89 = (f32[32,2048]{1,0:T(8,128)S(1)}, bf16[32,2048]{1,0:T(8,128)(2,1)S(1)}) custom-call(bf16[32,2176]{1,0:T(8,128)(2,1)S(1)} %collective-permute-done.16.refs_0_, bf16[32,2176]{1,0:T(8,128)(2,1)S(1)} %collective-permute-done.17.refs_1_, bf16[2,2048,256]{2,1,0:T(8,128)(2,1)S(1)} %get-tuple-element.28.refs_4_.refs_2_, ...), custom_call_target="tpu_custom_call" | custom-call | tf_op jit(solution)/shard_map/pallas_call | solution.py:231
  42.3 1.2 %collective-permute-start.18 = (bf16[32,2048]{1,0:T(8,128)(2,1)S(1)}, bf16[32,2048]{1,0:T(8,128)(2,1)S(1)}, u32[]{:S(2)}, u32[]{:S(2)}) collective-permute-start(bf16[32,2048]{1,0:T(8,128)(2,1)S(1)} %get-tuple-element.40), channel_id=1, source_target_pairs={{0,2},{2,0},{4,6},{6,4},{8,10},{10,8},{12,14},{14,12},{1,3},{3,1},... | collective-permute-start | bytes 393224 | tf_op jit(solution)/shard_map/ppermute | solution.py:272
  43.5 0.0 collective-permute-done.6.recv_ref
  43.5 0.1 shard_map.85.refs_0_
  43.7 0.1 collective-permute-start.7
  43.7 0.0 collective-permute-done.9.refs_2_
  43.7 0.5 collective-permute-start.10
  44.2 0.1 collective-permute-start.15
  44.3 3.1 %collective-permute-done.18.recv_ref = bf16[32,2048]{1,0:T(8,128)(2,1)S(1)} collective-permute-done((bf16[32,2048]{1,0:T(8,128)(2,1)S(1)}, bf16[32,2048]{1,0:T(8,128)(2,1)S(1)}, u32[]{:S(2)}, u32[]{:S(2)}) %collective-permute-start.18) | collective-permute-done | bytes 131104 | tf_op jit(solution)/shard_map/ppermute | solution.py:272
  47.4 0.1 shard_map.90
  47.5 0.1 collective-permute-start.19
  47.6 0.1 collective-permute-start.20
  47.7 6.2 %collective-permute-done.19.refs_6_ = bf16[32,1024]{1,0:T(8,128)(2,1)S(1)} collective-permute-done((bf16[32,1024]{1,0:T(8,128)(2,1)S(1)}, bf16[32,1024]{1,0:T(8,128)(2,1)S(1)}, u32[]{:S(2)}, u32[]{:S(2)}) %collective-permute-start.19) | collective-permute-done | bytes 65568 | tf_op jit(solution)/shard_map/ppermute | solution.py:263
  53.8 0.0 collective-permute-done.15.refs_5_
  53.9 1.0 %shard_map.91 = bf16[128,1024]{1,0:T(8,128)(2,1)} custom-call(bf16[128,256]{1,0:T(8,128)(2,1)S(1)} %get-tuple-element.25.map_ref, f32[1,1024]{1,0:T(1,128)S(1)} %bitcast.4, bf16[32,2048]{1,0:T(8,128)(2,1)S(1)} %shard_map.85.refs_0_, bf16[32,2048]{1,0:T(8,128)(2,1)S(1)} %collective-permute-done.7.refs_1_, ...), custom_call_target="tpu_custom_call" | custom-call | tf_op jit(solution)/shard_map/pallas_call | solution.py:231
  (6 shorter events, 0.0 us)
Async XLA Ops:
  0.0 26.8 %collective-permute-start.3 = (bf16[2,2048,256]{2,1,0:T(8,128)(2,1)}, bf16[2,2048,256]{2,1,0:T(8,128)(2,1)S(1)}, u32[]{:S(2)}, u32[]{:S(2)}) collective-permute-start(bf16[2,2048,256]{2,1,0:T(8,128)(2,1)} %wg_ref.1), channel_id=1, source_target_pairs={{0,1},{1,0},{2,3},{3,2},{4,5},{5,4},{6,7},{7,6},{8,9},{9,8},{10,11... | collective-permute-start | bytes 6291464 | tf_op jit(solution)/shard_map/ppermute | solution.py:275
  0.5 26.3 %collective-permute-start.4 = (bf16[2,2048,256]{2,1,0:T(8,128)(2,1)}, bf16[2,2048,256]{2,1,0:T(8,128)(2,1)S(1)}, u32[]{:S(2)}, u32[]{:S(2)}) collective-permute-start(bf16[2,2048,256]{2,1,0:T(8,128)(2,1)} %wu_ref.1), channel_id=1, source_target_pairs={{0,1},{1,0},{2,3},{3,2},{4,5},{5,4},{6,7},{7,6},{8,9},{9,8},{10,11... | collective-permute-start | bytes 6291464 | tf_op jit(solution)/shard_map/ppermute | solution.py:275
  0.5 26.3 %collective-permute-start.5 = (bf16[2,256,2048]{2,1,0:T(8,128)(2,1)}, bf16[2,256,2048]{2,1,0:T(8,128)(2,1)S(1)}, u32[]{:S(2)}, u32[]{:S(2)}) collective-permute-start(bf16[2,256,2048]{2,1,0:T(8,128)(2,1)} %wd_ref.1), channel_id=1, source_target_pairs={{0,1},{1,0},{2,3},{3,2},{4,5},{5,4},{6,7},{7,6},{8,9},{9,8},{10,11... | collective-permute-start | bytes 6291464 | tf_op jit(solution)/shard_map/ppermute | solution.py:275
  2.7 6.9 %collective-permute-start = (bf16[32,2176]{1,0:T(8,128)(2,1)S(1)}, bf16[32,2176]{1,0:T(8,128)(2,1)S(1)}, u32[]{:S(2)}, u32[]{:S(2)}) collective-permute-start(bf16[32,2176]{1,0:T(8,128)(2,1)S(1)} %get-tuple-element.26.refs_0_), channel_id=1, source_target_pairs={{0,2},{2,0},{4,6},{6,4},{8,10},{10,8},{12,14},{14,12},{1,3},{3,1},... | collective-permute-start | bytes 417800 | tf_op jit(solution)/shard_map/ppermute | solution.py:272
  5.2 7.7 %collective-permute-start.1 = (bf16[32,2176]{1,0:T(8,128)(2,1)S(1)}, bf16[32,2176]{1,0:T(8,128)(2,1)S(1)}, u32[]{:S(2)}, u32[]{:S(2)}) collective-permute-start(bf16[32,2176]{1,0:T(8,128)(2,1)S(1)} %get-tuple-element.27), channel_id=1, source_target_pairs={{0,4},{2,6},{4,8},{6,10},{8,12},{10,14},{12,0},{14,2},{1,5},{3,7},... | collective-permute-start | bytes 417800 | tf_op jit(solution)/shard_map/ppermute | solution.py:263
  9.6 9.4 %collective-permute-start.11 = (bf16[32,2176]{1,0:T(8,128)(2,1)S(1)}, bf16[32,2176]{1,0:T(8,128)(2,1)S(1)}, u32[]{:S(2)}, u32[]{:S(2)}) collective-permute-start(bf16[32,2176]{1,0:T(8,128)(2,1)S(1)} %get-tuple-element.35), channel_id=1, source_target_pairs={{0,8},{2,10},{4,12},{6,14},{8,0},{10,2},{12,4},{14,6},{1,9},{3,11}... | collective-permute-start | bytes 417800 | tf_op jit(solution)/shard_map/ppermute | solution.py:263
  12.9 7.5 %collective-permute-start.2 = (bf16[32,2176]{1,0:T(8,128)(2,1)S(1)}, bf16[32,2176]{1,0:T(8,128)(2,1)S(1)}, u32[]{:S(2)}, u32[]{:S(2)}) collective-permute-start(bf16[32,2176]{1,0:T(8,128)(2,1)S(1)} %collective-permute-done.1.refs_2_), channel_id=1, source_target_pairs={{0,2},{2,0},{4,6},{6,4},{8,10},{10,8},{12,14},{14,12},{1,3},{3,1},... | collective-permute-start | bytes 417800 | tf_op jit(solution)/shard_map/ppermute | solution.py:272
  19.0 10.3 %collective-permute-start.12 = (bf16[32,2176]{1,0:T(8,128)(2,1)S(1)}, bf16[32,2176]{1,0:T(8,128)(2,1)S(1)}, u32[]{:S(2)}, u32[]{:S(2)}) collective-permute-start(bf16[32,2176]{1,0:T(8,128)(2,1)S(1)} %collective-permute-done.11.refs_0_), channel_id=1, source_target_pairs={{0,2},{2,0},{4,6},{6,4},{8,10},{10,8},{12,14},{14,12},{1,3},{3,1},... | collective-permute-start | bytes 417800 | tf_op jit(solution)/shard_map/ppermute | solution.py:272
  20.4 12.2 %collective-permute-start.16 = (bf16[32,2176]{1,0:T(8,128)(2,1)S(1)}, bf16[32,2176]{1,0:T(8,128)(2,1)S(1)}, u32[]{:S(2)}, u32[]{:S(2)}) collective-permute-start(bf16[32,2176]{1,0:T(8,128)(2,1)S(1)} %get-tuple-element.38), channel_id=1, source_target_pairs={{0,12},{2,14},{4,0},{6,2},{8,4},{10,6},{12,8},{14,10},{1,13},{3,15... | collective-permute-start | bytes 417800 | tf_op jit(solution)/shard_map/ppermute | solution.py:263
  28.7 6.0 %collective-permute-start.8 = (bf16[32,2048]{1,0:T(8,128)(2,1)S(1)}, bf16[32,2048]{1,0:T(8,128)(2,1)S(1)}, u32[]{:S(2)}, u32[]{:S(2)}) collective-permute-start(bf16[32,2048]{1,0:T(8,128)(2,1)S(1)} %get-tuple-element.34), channel_id=1, source_target_pairs={{0,2},{2,0},{4,6},{6,4},{8,10},{10,8},{12,14},{14,12},{1,3},{3,1},... | collective-permute-start | bytes 393224 | tf_op jit(solution)/shard_map/ppermute | solution.py:272
  31.1 6.4 %collective-permute-start.13 = (bf16[32,2048]{1,0:T(8,128)(2,1)S(1)}, bf16[32,2048]{1,0:T(8,128)(2,1)S(1)}, u32[]{:S(2)}, u32[]{:S(2)}) collective-permute-start(bf16[32,2048]{1,0:T(8,128)(2,1)S(1)} %get-tuple-element.37), channel_id=1, source_target_pairs={{0,2},{2,0},{4,6},{6,4},{8,10},{10,8},{12,14},{14,12},{1,3},{3,1},... | collective-permute-start | bytes 393224 | tf_op jit(solution)/shard_map/ppermute | solution.py:272
  32.7 7.9 %collective-permute-start.17 = (bf16[32,2176]{1,0:T(8,128)(2,1)S(1)}, bf16[32,2176]{1,0:T(8,128)(2,1)S(1)}, u32[]{:S(2)}, u32[]{:S(2)}) collective-permute-start(bf16[32,2176]{1,0:T(8,128)(2,1)S(1)} %collective-permute-done.16.refs_0_), channel_id=1, source_target_pairs={{0,2},{2,0},{4,6},{6,4},{8,10},{10,8},{12,14},{14,12},{1,3},{3,1},... | collective-permute-start | bytes 417800 | tf_op jit(solution)/shard_map/ppermute | solution.py:272
  33.2 10.3 %collective-permute-start.6 = (bf16[32,2048]{1,0:T(8,128)(2,1)S(1)}, bf16[32,2048]{1,0:T(8,128)(2,1)S(1)}, u32[]{:S(2)}, u32[]{:S(2)}) collective-permute-start(bf16[32,2048]{1,0:T(8,128)(2,1)S(1)} %get-tuple-element.32), channel_id=1, source_target_pairs={{0,2},{2,0},{4,6},{6,4},{8,10},{10,8},{12,14},{14,12},{1,3},{3,1},... | collective-permute-start | bytes 393224 | tf_op jit(solution)/shard_map/ppermute | solution.py:272
  34.8 8.9 %collective-permute-start.9 = (bf16[32,2048]{1,0:T(8,128)(2,1)S(1)}, bf16[32,2048]{1,0:T(8,128)(2,1)S(1)}, u32[]{:S(2)}, u32[]{:S(2)}) collective-permute-start(bf16[32,2048]{1,0:T(8,128)(2,1)S(1)} %shard_map.86), channel_id=1, source_target_pairs={{0,12},{2,14},{4,0},{6,2},{8,4},{10,6},{12,8},{14,10},{1,13},{3,15... | collective-permute-start | bytes 393224 | tf_op jit(solution)/shard_map/ppermute | solution.py:263
  37.7 16.2 %copy-start = (f32[1024]{0:T(1024)S(1)}, f32[1024]{0:T(1024)}, u32[]{:S(2)}) copy-start(f32[1024]{0:T(1024)} %param.15) | copy-start | bytes 12292
  37.7 6.6 %collective-permute-start.14 = (bf16[32,2048]{1,0:T(8,128)(2,1)S(1)}, bf16[32,2048]{1,0:T(8,128)(2,1)S(1)}, u32[]{:S(2)}, u32[]{:S(2)}) collective-permute-start(bf16[32,2048]{1,0:T(8,128)(2,1)S(1)} %shard_map.88), channel_id=1, source_target_pairs={{0,8},{2,10},{4,12},{6,14},{8,0},{10,2},{12,4},{14,6},{1,9},{3,11}... | collective-permute-start | bytes 393224 | tf_op jit(solution)/shard_map/ppermute | solution.py:263
  42.3 5.0 %collective-permute-start.18 = (bf16[32,2048]{1,0:T(8,128)(2,1)S(1)}, bf16[32,2048]{1,0:T(8,128)(2,1)S(1)}, u32[]{:S(2)}, u32[]{:S(2)}) collective-permute-start(bf16[32,2048]{1,0:T(8,128)(2,1)S(1)} %get-tuple-element.40), channel_id=1, source_target_pairs={{0,2},{2,0},{4,6},{6,4},{8,10},{10,8},{12,14},{14,12},{1,3},{3,1},... | collective-permute-start | bytes 393224 | tf_op jit(solution)/shard_map/ppermute | solution.py:272
  43.7 10.2 %collective-permute-start.7 = (bf16[32,2048]{1,0:T(8,128)(2,1)S(1)}, bf16[32,2048]{1,0:T(8,128)(2,1)S(1)}, u32[]{:S(2)}, u32[]{:S(2)}) collective-permute-start(bf16[32,2048]{1,0:T(8,128)(2,1)S(1)} %shard_map.85.refs_0_), channel_id=1, source_target_pairs={{0,1},{1,0},{2,3},{3,2},{4,5},{5,4},{6,7},{7,6},{8,9},{9,8},{10,11... | collective-permute-start | bytes 393224 | tf_op jit(solution)/shard_map/ppermute | solution.py:275
  43.7 10.1 %collective-permute-start.10 = (bf16[32,2048]{1,0:T(8,128)(2,1)S(1)}, bf16[32,2048]{1,0:T(8,128)(2,1)S(1)}, u32[]{:S(2)}, u32[]{:S(2)}) collective-permute-start(bf16[32,2048]{1,0:T(8,128)(2,1)S(1)} %collective-permute-done.9.refs_2_), channel_id=1, source_target_pairs={{0,1},{1,0},{2,3},{3,2},{4,5},{5,4},{6,7},{7,6},{8,9},{9,8},{10,11... | collective-permute-start | bytes 393224 | tf_op jit(solution)/shard_map/ppermute | solution.py:275
  44.2 9.6 %collective-permute-start.15 = (bf16[32,2048]{1,0:T(8,128)(2,1)S(1)}, bf16[32,2048]{1,0:T(8,128)(2,1)S(1)}, u32[]{:S(2)}, u32[]{:S(2)}) collective-permute-start(bf16[32,2048]{1,0:T(8,128)(2,1)S(1)} %collective-permute-done.14.refs_4_), channel_id=1, source_target_pairs={{0,1},{1,0},{2,3},{3,2},{4,5},{5,4},{6,7},{7,6},{8,9},{9,8},{10,11... | collective-permute-start | bytes 393224 | tf_op jit(solution)/shard_map/ppermute | solution.py:275
  47.5 6.3 %collective-permute-start.19 = (bf16[32,1024]{1,0:T(8,128)(2,1)S(1)}, bf16[32,1024]{1,0:T(8,128)(2,1)S(1)}, u32[]{:S(2)}, u32[]{:S(2)}) collective-permute-start(bf16[32,1024]{1,0:T(8,128)(2,1)S(1)} %get-tuple-element.41), channel_id=1, source_target_pairs={{0,4},{2,6},{4,8},{6,10},{8,12},{10,14},{12,0},{14,2},{1,5},{3,7},... | collective-permute-start | bytes 196616 | tf_op jit(solution)/shard_map/ppermute | solution.py:263
  47.6 6.2 %collective-permute-start.20 = (bf16[32,1024]{1,0:T(8,128)(2,1)S(1)}, bf16[32,1024]{1,0:T(8,128)(2,1)S(1)}, u32[]{:S(2)}, u32[]{:S(2)}) collective-permute-start(bf16[32,1024]{1,0:T(8,128)(2,1)S(1)} %get-tuple-element.42), channel_id=1, source_target_pairs={{0,5},{1,4},{2,7},{3,6},{4,9},{5,8},{6,11},{7,10},{8,13},{9,12},{1... | collective-permute-start | bytes 196616 | tf_op jit(solution)/shard_map/ppermute | solution.py:269

commit v5 on v4

--- a/solution.py
+++ b/solution.py
@@ -181,9 +181,10 @@
             up_act = dot(rows, wu_ref[e])
             act = gate_act / (1.0 + jnp.exp(-gate_act)) * up_act
             hidden.append((act * weight).astype(jnp.bfloat16))
-    hidden = jnp.concatenate(hidden, axis=1)
     down = [ref[e] for e in range(local_experts) for ref in (weights[2], weights[5])]
-    total = dot(hidden, jnp.concatenate(down, axis=0))
+    total = dot(hidden[0], down[0])
+    for h, w in zip(hidden[1:], down[1:]):
+        total += dot(h, w)
     for c in range(chunks):
         outs[2 * c][...] = total[2 * c * half : (2 * c + 1) * half]
         outs[2 * c + 1][...] = total[(2 * c + 1) * half : (2 * c + 2) * half].astype(jnp.bfloat16)
@@ -209,7 +210,7 @@
 
 
 def close_kernel(cap, map_ref, gain_ref, *refs):
-    parts, out_ref, rows_ref = refs[: 2 * GROUPS], refs[-2], refs[-1]
+    parts, (out_ref, rows_ref, done_ref, sems) = refs[: 2 * GROUPS], refs[2 * GROUPS :]
     half = cap // 2
     half_width = out_ref.shape[1]
     my_half = lax.axis_index("tp")
@@ -224,20 +225,31 @@
         other = pl.multiple_of(k * cap + (1 - my_half) * half, half)
         rows_ref[pl.ds(same, half), :] = features(parts[2 * k])
         rows_ref[pl.ds(other, half), :] = features(parts[2 * k + 1])
-    out_ref[...] = (dot(map_ref[...], rows_ref[...]) * gain_ref[...]).astype(jnp.bfloat16)
-
-
-def call(kernel, outs, args, limit, scratch=(), in_specs=None):
+    copies = []
+    block = done_ref.shape[1] // 2
+    for i in range(2):
+        at = slice(i * block, (i + 1) * block)
+        done_ref[:, at] = (dot(map_ref[...], rows_ref[:, at]) * gain_ref[:, at]).astype(
+            jnp.bfloat16
+        )
+        copies.append(pltpu.make_async_copy(done_ref.at[:, at], out_ref.at[:, at], sems.at[i]))
+        copies[-1].start()
+    for copy in copies:
+        copy.wait()
+
+
+def call(kernel, outs, args, limit, scratch=(), in_specs=None, **specs):
     return pl.pallas_call(
         kernel,
         out_shape=outs,
         in_specs=in_specs or [pl.BlockSpec(memory_space=pltpu.VMEM)] * len(args),
         scratch_shapes=scratch,
+        **specs,
         compiler_params=pltpu.CompilerParams(vmem_limit_bytes=limit * MIB),
     )(*args)
 
 
-STAGES = ((0, 1), (2,), (3,))
+STAGES = ((1,), (2,), (0, 3))
 SPLIT = (3,)
 
 
@@ -345,7 +357,12 @@
         sds((tok_dev, half_width), bf16),
         (token_map, out_gain.reshape(1, -1), *back),
         8,
-        (pltpu.VMEM((GROUPS * cap, half_width), bf16),),
+        (
+            pltpu.VMEM((GROUPS * cap, half_width), bf16),
+            pltpu.VMEM((tok_dev, half_width), bf16),
+            pltpu.SemaphoreType.DMA((2,)),
+        ),
+        out_specs=anywhere,
     )
 
 

time: 55.1 us -> 56 us (1.016)
  waiting for transfers between devices: 23 us -> 23.6 us
    ppermute x6, waiting for transfers between devices: 11.7 us -> 23.1 us  [hop(): lax.ppermute(value, 'ep', [(i, far_ep(i, k)) for i in range(ep_count)])]
    ppermute x8, waiting for transfers between devices: 11.2 us -> 0.02 us  [cross(): return lax.ppermute(value, 'ep', [(i, i ^ 1) for i in range(ep_count)])]
    ppermute x6, starting transfers between devices: 8.09 us -> 9.47 us  [hop(): lax.ppermute(value, 'ep', [(i, far_ep(i, k)) for i in range(ep_count)])]
    ppermute x6, starting transfers between devices: 1.65 us -> 1.08 us  [swap(): return lax.ppermute(value, 'tp', [(0, 1), (1, 0)])]
where the time goes in v5:
time: 56 us; the launch traced here: 55.8 us
  waiting for transfers between devices  23.6 us (42%)
  starting transfers between devices  20.5 us (37%)
  Pallas kernels  11.6 us (21%)
    ppermute x6, waiting for transfers between devices, hop(): lax.ppermute(value, 'ep', [(i, far_ep(i, k)) for i in range(ep_count)])  23.1 us
    pallas_call x10, Pallas kernels, call(): pl.pallas_call(kernel, out_shape=outs, in_specs=in_specs or [pl.BlockSpec...  11.6 us
    ppermute x8, starting transfers between devices, cross(): return lax.ppermute(value, 'ep', [(i, i ^ 1) for i in range(ep_count)])  9.92 us
    ppermute x6, starting transfers between devices, hop(): lax.ppermute(value, 'ep', [(i, far_ep(i, k)) for i in range(ep_count)])  9.47 us
  transfers between devices with their start and end apart: 21, of which 7 were waited for; matrix products, arithmetic and copies ran while one was open for 0% of the time, Pallas kernels for 19%

profile of v5, /device:TPU:0, one launch (start us, length us, event | category | flops | bytes accessed | tf_op | source)
XLA Modules:
  0.0 55.8 jit_solution(6193533316324015491)
XLA Ops:
  0.0 0.5 collective-permute-start.3
  0.5 0.0 collective-permute-start.4
  0.5 0.5 collective-permute-start.5
  1.0 1.7 %shard_map.82 = (bf16[32,2176]{1,0:T(8,128)(2,1)S(1)}, bf16[32,2176]{1,0:T(8,128)(2,1)S(1)}, bf16[32,2176]{1,0:T(8,128)(2,1)S(1)}, bf16[32,2176]{1,0:T(8,128)(2,1)S(1)}, bf16[256,128]{1,0:T(8,128)(2,1)S(1)}) custom-call(bf16[128,2048]{1,0:T(8,128)(2,1)} %refs_0_.1, f32[1,2048]{1,0:T(1,128)} %bitcast.5, s32[4,128]{1,0:T(4,128)} %bitcast.6, f32[4,128]{1,0:T(4,128)} %bitcast.7), custom_call_target="tpu_custom_call" | custom-call | tf_op jit(solution)/shard_map/pallas_call | solution.py:242
  2.7 4.6 %collective-permute-start.1 = (bf16[32,2176]{1,0:T(8,128)(2,1)S(1)}, bf16[32,2176]{1,0:T(8,128)(2,1)S(1)}, u32[]{:S(2)}, u32[]{:S(2)}) collective-permute-start(bf16[32,2176]{1,0:T(8,128)(2,1)S(1)} %get-tuple-element.27), channel_id=1, source_target_pairs={{0,12},{2,14},{4,0},{6,2},{8,4},{10,6},{12,8},{14,10},{1,13},{3,15... | collective-permute-start | bytes 417800 | tf_op jit(solution)/shard_map/ppermute | solution.py:275
  7.3 4.1 %collective-permute-done.1.refs_2_ = bf16[32,2176]{1,0:T(8,128)(2,1)S(1)} collective-permute-done((bf16[32,2176]{1,0:T(8,128)(2,1)S(1)}, bf16[32,2176]{1,0:T(8,128)(2,1)S(1)}, u32[]{:S(2)}, u32[]{:S(2)}) %collective-permute-start.1) | collective-permute-done | bytes 139296 | tf_op jit(solution)/shard_map/ppermute | solution.py:275
  11.4 1.0 %collective-permute-start.13 = (bf16[32,2176]{1,0:T(8,128)(2,1)S(1)}, bf16[32,2176]{1,0:T(8,128)(2,1)S(1)}, u32[]{:S(2)}, u32[]{:S(2)}) collective-permute-start(bf16[32,2176]{1,0:T(8,128)(2,1)S(1)} %get-tuple-element.36), channel_id=1, source_target_pairs={{0,8},{2,10},{4,12},{6,14},{8,0},{10,2},{12,4},{14,6},{1,9},{3,11}... | collective-permute-start | bytes 417800 | tf_op jit(solution)/shard_map/ppermute | solution.py:275
  12.4 2.6 %collective-permute-done.8.refs_0_ = bf16[32,2176]{1,0:T(8,128)(2,1)S(1)} collective-permute-done((bf16[32,2176]{1,0:T(8,128)(2,1)S(1)}, bf16[32,2176]{1,0:T(8,128)(2,1)S(1)}, u32[]{:S(2)}, u32[]{:S(2)}) %collective-permute-start.8) | collective-permute-done | bytes 139296 | tf_op jit(solution)/shard_map/ppermute | solution.py:275
  15.0 1.5 %collective-permute-start.9 = (bf16[32,2176]{1,0:T(8,128)(2,1)S(1)}, bf16[32,2176]{1,0:T(8,128)(2,1)S(1)}, u32[]{:S(2)}, u32[]{:S(2)}) collective-permute-start(bf16[32,2176]{1,0:T(8,128)(2,1)S(1)} %collective-permute-done.8.refs_0_), channel_id=1, source_target_pairs={{0,2},{2,0},{4,6},{6,4},{8,10},{10,8},{12,14},{14,12},{1,3},{3,1},... | collective-permute-start | bytes 417800 | tf_op jit(solution)/shard_map/ppermute | solution.py:284
  16.5 4.4 %collective-permute-done.13.refs_0_ = bf16[32,2176]{1,0:T(8,128)(2,1)S(1)} collective-permute-done((bf16[32,2176]{1,0:T(8,128)(2,1)S(1)}, bf16[32,2176]{1,0:T(8,128)(2,1)S(1)}, u32[]{:S(2)}, u32[]{:S(2)}) %collective-permute-start.13) | collective-permute-done | bytes 139296 | tf_op jit(solution)/shard_map/ppermute | solution.py:275
  20.9 1.5 %collective-permute-start.14 = (bf16[32,2176]{1,0:T(8,128)(2,1)S(1)}, bf16[32,2176]{1,0:T(8,128)(2,1)S(1)}, u32[]{:S(2)}, u32[]{:S(2)}) collective-permute-start(bf16[32,2176]{1,0:T(8,128)(2,1)S(1)} %collective-permute-done.13.refs_0_), channel_id=1, source_target_pairs={{0,2},{2,0},{4,6},{6,4},{8,10},{10,8},{12,14},{14,12},{1,3},{3,1},... | collective-permute-start | bytes 417800 | tf_op jit(solution)/shard_map/ppermute | solution.py:284
  22.4 0.0 collective-permute-done.9.refs_1_
  22.4 0.5 collective-permute-start
  22.9 0.0 collective-permute-done.3.refs_7_.refs_5_
  22.9 1.5 %collective-permute-start.2 = (bf16[32,2176]{1,0:T(8,128)(2,1)S(1)}, bf16[32,2176]{1,0:T(8,128)(2,1)S(1)}, u32[]{:S(2)}, u32[]{:S(2)}) collective-permute-start(bf16[32,2176]{1,0:T(8,128)(2,1)S(1)} %collective-permute-done.1.refs_2_), channel_id=1, source_target_pairs={{0,2},{2,0},{4,6},{6,4},{8,10},{10,8},{12,14},{14,12},{1,3},{3,1},... | collective-permute-start | bytes 417800 | tf_op jit(solution)/shard_map/ppermute | solution.py:284
  24.4 2.9 %shard_map.83 = (bf16[2,2048,256]{2,1,0:T(8,128)(2,1)S(1)}, bf16[2,2048,256]{2,1,0:T(8,128)(2,1)S(1)}, bf16[2,256,2048]{2,1,0:T(8,128)(2,1)S(1)}, bf16[128,256]{1,0:T(8,128)(2,1)S(1)}) custom-call(bf16[2,2048,256]{2,1,0:T(8,128)(2,1)} %wg_ref.1, bf16[2,2048,256]{2,1,0:T(8,128)(2,1)} %wu_ref.1, bf16[2,256,2048]{2,1,0:T(8,128)(2,1)} %wd_ref.1, ...), custom_call_target="tpu_custom_call" | custom-call | tf_op jit(solution)/shard_map/pallas_call | solution.py:242
  27.3 0.0 collective-permute-done.4.refs_8_.refs_6_
  27.3 1.8 %shard_map.86 = (f32[32,2048]{1,0:T(8,128)S(1)}, bf16[32,2048]{1,0:T(8,128)(2,1)S(1)}) custom-call(bf16[32,2176]{1,0:T(8,128)(2,1)S(1)} %collective-permute-done.8.refs_0_, bf16[32,2176]{1,0:T(8,128)(2,1)S(1)} %collective-permute-done.9.refs_1_, bf16[2,2048,256]{2,1,0:T(8,128)(2,1)S(1)} %get-tuple-element.28.refs_4_.refs_2_, ...), custom_call_target="tpu_custom_call" | custom-call | tf_op jit(solution)/shard_map/pallas_call | solution.py:242
  29.1 0.6 %collective-permute-start.10 = (bf16[32,2048]{1,0:T(8,128)(2,1)S(1)}, bf16[32,2048]{1,0:T(8,128)(2,1)S(1)}, u32[]{:S(2)}, u32[]{:S(2)}) collective-permute-start(bf16[32,2048]{1,0:T(8,128)(2,1)S(1)} %get-tuple-element.35), channel_id=1, source_target_pairs={{0,2},{2,0},{4,6},{6,4},{8,10},{10,8},{12,14},{14,12},{1,3},{3,1},... | collective-permute-start | bytes 393224 | tf_op jit(solution)/shard_map/ppermute | solution.py:284
  29.7 0.0 collective-permute-done.14.refs_1_
  29.7 1.8 %shard_map.88 = (f32[32,2048]{1,0:T(8,128)S(1)}, bf16[32,2048]{1,0:T(8,128)(2,1)S(1)}) custom-call(bf16[32,2176]{1,0:T(8,128)(2,1)S(1)} %collective-permute-done.13.refs_0_, bf16[32,2176]{1,0:T(8,128)(2,1)S(1)} %collective-permute-done.14.refs_1_, bf16[2,2048,256]{2,1,0:T(8,128)(2,1)S(1)} %get-tuple-element.28.refs_4_.refs_2_, ...), custom_call_target="tpu_custom_call" | custom-call | tf_op jit(solution)/shard_map/pallas_call | solution.py:242
  31.6 0.0 copy-start
  31.6 1.6 %collective-permute-start.15 = (bf16[32,2048]{1,0:T(8,128)(2,1)S(1)}, bf16[32,2048]{1,0:T(8,128)(2,1)S(1)}, u32[]{:S(2)}, u32[]{:S(2)}) collective-permute-start(bf16[32,2048]{1,0:T(8,128)(2,1)S(1)} %get-tuple-element.38), channel_id=1, source_target_pairs={{0,2},{2,0},{4,6},{6,4},{8,10},{10,8},{12,14},{14,12},{1,3},{3,1},... | collective-permute-start | bytes 393224 | tf_op jit(solution)/shard_map/ppermute | solution.py:284
  33.2 0.0 collective-permute-done.2.refs_3_
  33.2 1.8 %shard_map.84 = (f32[32,2048]{1,0:T(8,128)S(1)}, bf16[32,2048]{1,0:T(8,128)(2,1)S(1)}, f32[32,2048]{1,0:T(8,128)S(1)}, bf16[32,2048]{1,0:T(8,128)(2,1)S(1)}) custom-call(bf16[32,2176]{1,0:T(8,128)(2,1)S(1)} %get-tuple-element.26.refs_0_, bf16[32,2176]{1,0:T(8,128)(2,1)S(1)} %collective-permute-done.refs_1_, ...), custom_call_target="tpu_custom_call" | custom-call | tf_op jit(solution)/shard_map/pallas_call | solution.py:242
  35.0 1.8 %collective-permute-start.6 = (bf16[32,2048]{1,0:T(8,128)(2,1)S(1)}, bf16[32,2048]{1,0:T(8,128)(2,1)S(1)}, u32[]{:S(2)}, u32[]{:S(2)}) collective-permute-start(bf16[32,2048]{1,0:T(8,128)(2,1)S(1)} %get-tuple-element.32), channel_id=1, source_target_pairs={{0,2},{2,0},{4,6},{6,4},{8,10},{10,8},{12,14},{14,12},{1,3},{3,1},... | collective-permute-start | bytes 393224 | tf_op jit(solution)/shard_map/ppermute | solution.py:284
  36.8 0.1 shard_map.87
  37.0 3.2 %collective-permute-start.11 = (bf16[32,2048]{1,0:T(8,128)(2,1)S(1)}, bf16[32,2048]{1,0:T(8,128)(2,1)S(1)}, u32[]{:S(2)}, u32[]{:S(2)}) collective-permute-start(bf16[32,2048]{1,0:T(8,128)(2,1)S(1)} %shard_map.87), channel_id=1, source_target_pairs={{0,12},{2,14},{4,0},{6,2},{8,4},{10,6},{12,8},{14,10},{1,13},{3,15... | collective-permute-start | bytes 393224 | tf_op jit(solution)/shard_map/ppermute | solution.py:275
  40.2 0.1 shard_map.89
  40.3 0.1 collective-permute-start.16
  40.4 1.0 %collective-permute-start.18 = (bf16[32,2048]{1,0:T(8,128)(2,1)S(1)}, bf16[32,2048]{1,0:T(8,128)(2,1)S(1)}, u32[]{:S(2)}, u32[]{:S(2)}) collective-permute-start(bf16[32,2048]{1,0:T(8,128)(2,1)S(1)} %get-tuple-element.40), channel_id=1, source_target_pairs={{0,2},{2,0},{4,6},{6,4},{8,10},{10,8},{12,14},{14,12},{1,3},{3,1},... | collective-permute-start | bytes 393224 | tf_op jit(solution)/shard_map/ppermute | solution.py:284
  41.3 0.0 collective-permute-done.6.recv_ref
  41.3 0.1 shard_map.85.refs_0_
  41.5 0.1 collective-permute-start.7
  41.5 1.1 %collective-permute-done.11.refs_2_ = bf16[32,2048]{1,0:T(8,128)(2,1)S(1)} collective-permute-done((bf16[32,2048]{1,0:T(8,128)(2,1)S(1)}, bf16[32,2048]{1,0:T(8,128)(2,1)S(1)}, u32[]{:S(2)}, u32[]{:S(2)}) %collective-permute-start.11) | collective-permute-done | bytes 131104 | tf_op jit(solution)/shard_map/ppermute | solution.py:275
  42.7 0.0 collective-permute-start.12
  42.7 4.7 %collective-permute-done.16.refs_4_ = bf16[32,2048]{1,0:T(8,128)(2,1)S(1)} collective-permute-done((bf16[32,2048]{1,0:T(8,128)(2,1)S(1)}, bf16[32,2048]{1,0:T(8,128)(2,1)S(1)}, u32[]{:S(2)}, u32[]{:S(2)}) %collective-permute-start.16) | collective-permute-done | bytes 131104 | tf_op jit(solution)/shard_map/ppermute | solution.py:275
  47.4 0.0 collective-permute-start.17
  47.4 0.0 collective-permute-done.18.recv_ref
  47.4 0.1 shard_map.90
  47.5 0.6 %collective-permute-start.19 = (bf16[32,1024]{1,0:T(8,128)(2,1)S(1)}, bf16[32,1024]{1,0:T(8,128)(2,1)S(1)}, u32[]{:S(2)}, u32[]{:S(2)}) collective-permute-start(bf16[32,1024]{1,0:T(8,128)(2,1)S(1)} %get-tuple-element.41), channel_id=1, source_target_pairs={{0,4},{2,6},{4,8},{6,10},{8,12},{10,14},{12,0},{14,2},{1,5},{3,7},... | collective-permute-start | bytes 196616 | tf_op jit(solution)/shard_map/ppermute | solution.py:275
  48.1 0.1 collective-permute-start.20
  48.2 6.2 %collective-permute-done.19.refs_6_ = bf16[32,1024]{1,0:T(8,128)(2,1)S(1)} collective-permute-done((bf16[32,1024]{1,0:T(8,128)(2,1)S(1)}, bf16[32,1024]{1,0:T(8,128)(2,1)S(1)}, u32[]{:S(2)}, u32[]{:S(2)}) %collective-permute-start.19) | collective-permute-done | bytes 65568 | tf_op jit(solution)/shard_map/ppermute | solution.py:275
  54.3 0.5 collective-permute-done.20.refs_7_
  54.8 0.0 collective-permute-done.7.refs_1_
  54.8 0.0 collective-permute-done.12.refs_3_
  54.8 0.0 collective-permute-done.17.refs_5_
  54.8 1.0 %shard_map.91 = bf16[128,1024]{1,0:T(8,128)(2,1)} custom-call(bf16[128,256]{1,0:T(8,128)(2,1)S(1)} %get-tuple-element.25.map_ref, f32[1,1024]{1,0:T(1,128)S(1)} %bitcast.4, bf16[32,2048]{1,0:T(8,128)(2,1)S(1)} %shard_map.85.refs_0_, bf16[32,2048]{1,0:T(8,128)(2,1)S(1)} %collective-permute-done.7.refs_1_, ...), custom_call_target="tpu_custom_call" | custom-call | tf_op jit(solution)/shard_map/pallas_call | solution.py:242
  (6 shorter events, 0.0 us)
Async XLA Ops:
  0.0 22.9 %collective-permute-start.3 = (bf16[2,2048,256]{2,1,0:T(8,128)(2,1)}, bf16[2,2048,256]{2,1,0:T(8,128)(2,1)S(1)}, u32[]{:S(2)}, u32[]{:S(2)}) collective-permute-start(bf16[2,2048,256]{2,1,0:T(8,128)(2,1)} %wg_ref.1), channel_id=1, source_target_pairs={{0,1},{1,0},{2,3},{3,2},{4,5},{5,4},{6,7},{7,6},{8,9},{9,8},{10,11... | collective-permute-start | bytes 6291464 | tf_op jit(solution)/shard_map/ppermute | solution.py:287
  0.5 26.8 %collective-permute-start.4 = (bf16[2,2048,256]{2,1,0:T(8,128)(2,1)}, bf16[2,2048,256]{2,1,0:T(8,128)(2,1)S(1)}, u32[]{:S(2)}, u32[]{:S(2)}) collective-permute-start(bf16[2,2048,256]{2,1,0:T(8,128)(2,1)} %wu_ref.1), channel_id=1, source_target_pairs={{0,1},{1,0},{2,3},{3,2},{4,5},{5,4},{6,7},{7,6},{8,9},{9,8},{10,11... | collective-permute-start | bytes 6291464 | tf_op jit(solution)/shard_map/ppermute | solution.py:287
  0.5 26.8 %collective-permute-start.5 = (bf16[2,256,2048]{2,1,0:T(8,128)(2,1)}, bf16[2,256,2048]{2,1,0:T(8,128)(2,1)S(1)}, u32[]{:S(2)}, u32[]{:S(2)}) collective-permute-start(bf16[2,256,2048]{2,1,0:T(8,128)(2,1)} %wd_ref.1), channel_id=1, source_target_pairs={{0,1},{1,0},{2,3},{3,2},{4,5},{5,4},{6,7},{7,6},{8,9},{9,8},{10,11... | collective-permute-start | bytes 6291464 | tf_op jit(solution)/shard_map/ppermute | solution.py:287
  2.7 8.8 %collective-permute-start.1 = (bf16[32,2176]{1,0:T(8,128)(2,1)S(1)}, bf16[32,2176]{1,0:T(8,128)(2,1)S(1)}, u32[]{:S(2)}, u32[]{:S(2)}) collective-permute-start(bf16[32,2176]{1,0:T(8,128)(2,1)S(1)} %get-tuple-element.27), channel_id=1, source_target_pairs={{0,12},{2,14},{4,0},{6,2},{8,4},{10,6},{12,8},{14,10},{1,13},{3,15... | collective-permute-start | bytes 417800 | tf_op jit(solution)/shard_map/ppermute | solution.py:275
  7.3 7.7 %collective-permute-start.8 = (bf16[32,2176]{1,0:T(8,128)(2,1)S(1)}, bf16[32,2176]{1,0:T(8,128)(2,1)S(1)}, u32[]{:S(2)}, u32[]{:S(2)}) collective-permute-start(bf16[32,2176]{1,0:T(8,128)(2,1)S(1)} %get-tuple-element.33), channel_id=1, source_target_pairs={{0,4},{2,6},{4,8},{6,10},{8,12},{10,14},{12,0},{14,2},{1,5},{3,7},... | collective-permute-start | bytes 417800 | tf_op jit(solution)/shard_map/ppermute | solution.py:275
  11.4 9.5 %collective-permute-start.13 = (bf16[32,2176]{1,0:T(8,128)(2,1)S(1)}, bf16[32,2176]{1,0:T(8,128)(2,1)S(1)}, u32[]{:S(2)}, u32[]{:S(2)}) collective-permute-start(bf16[32,2176]{1,0:T(8,128)(2,1)S(1)} %get-tuple-element.36), channel_id=1, source_target_pairs={{0,8},{2,10},{4,12},{6,14},{8,0},{10,2},{12,4},{14,6},{1,9},{3,11}... | collective-permute-start | bytes 417800 | tf_op jit(solution)/shard_map/ppermute | solution.py:275
  15.0 7.4 %collective-permute-start.9 = (bf16[32,2176]{1,0:T(8,128)(2,1)S(1)}, bf16[32,2176]{1,0:T(8,128)(2,1)S(1)}, u32[]{:S(2)}, u32[]{:S(2)}) collective-permute-start(bf16[32,2176]{1,0:T(8,128)(2,1)S(1)} %collective-permute-done.8.refs_0_), channel_id=1, source_target_pairs={{0,2},{2,0},{4,6},{6,4},{8,10},{10,8},{12,14},{14,12},{1,3},{3,1},... | collective-permute-start | bytes 417800 | tf_op jit(solution)/shard_map/ppermute | solution.py:284
  20.9 8.9 %collective-permute-start.14 = (bf16[32,2176]{1,0:T(8,128)(2,1)S(1)}, bf16[32,2176]{1,0:T(8,128)(2,1)S(1)}, u32[]{:S(2)}, u32[]{:S(2)}) collective-permute-start(bf16[32,2176]{1,0:T(8,128)(2,1)S(1)} %collective-permute-done.13.refs_0_), channel_id=1, source_target_pairs={{0,2},{2,0},{4,6},{6,4},{8,10},{10,8},{12,14},{14,12},{1,3},{3,1},... | collective-permute-start | bytes 417800 | tf_op jit(solution)/shard_map/ppermute | solution.py:284
  22.4 10.8 %collective-permute-start = (bf16[32,2176]{1,0:T(8,128)(2,1)S(1)}, bf16[32,2176]{1,0:T(8,128)(2,1)S(1)}, u32[]{:S(2)}, u32[]{:S(2)}) collective-permute-start(bf16[32,2176]{1,0:T(8,128)(2,1)S(1)} %get-tuple-element.26.refs_0_), channel_id=1, source_target_pairs={{0,2},{2,0},{4,6},{6,4},{8,10},{10,8},{12,14},{14,12},{1,3},{3,1},... | collective-permute-start | bytes 417800 | tf_op jit(solution)/shard_map/ppermute | solution.py:284
  22.9 10.2 %collective-permute-start.2 = (bf16[32,2176]{1,0:T(8,128)(2,1)S(1)}, bf16[32,2176]{1,0:T(8,128)(2,1)S(1)}, u32[]{:S(2)}, u32[]{:S(2)}) collective-permute-start(bf16[32,2176]{1,0:T(8,128)(2,1)S(1)} %collective-permute-done.1.refs_2_), channel_id=1, source_target_pairs={{0,2},{2,0},{4,6},{6,4},{8,10},{10,8},{12,14},{14,12},{1,3},{3,1},... | collective-permute-start | bytes 417800 | tf_op jit(solution)/shard_map/ppermute | solution.py:284
  29.1 7.7 %collective-permute-start.10 = (bf16[32,2048]{1,0:T(8,128)(2,1)S(1)}, bf16[32,2048]{1,0:T(8,128)(2,1)S(1)}, u32[]{:S(2)}, u32[]{:S(2)}) collective-permute-start(bf16[32,2048]{1,0:T(8,128)(2,1)S(1)} %get-tuple-element.35), channel_id=1, source_target_pairs={{0,2},{2,0},{4,6},{6,4},{8,10},{10,8},{12,14},{14,12},{1,3},{3,1},... | collective-permute-start | bytes 393224 | tf_op jit(solution)/shard_map/ppermute | solution.py:284
  31.6 23.2 %copy-start = (f32[1024]{0:T(1024)S(1)}, f32[1024]{0:T(1024)}, u32[]{:S(2)}) copy-start(f32[1024]{0:T(1024)} %param.15) | copy-start | bytes 12292
  31.6 8.6 %collective-permute-start.15 = (bf16[32,2048]{1,0:T(8,128)(2,1)S(1)}, bf16[32,2048]{1,0:T(8,128)(2,1)S(1)}, u32[]{:S(2)}, u32[]{:S(2)}) collective-permute-start(bf16[32,2048]{1,0:T(8,128)(2,1)S(1)} %get-tuple-element.38), channel_id=1, source_target_pairs={{0,2},{2,0},{4,6},{6,4},{8,10},{10,8},{12,14},{14,12},{1,3},{3,1},... | collective-permute-start | bytes 393224 | tf_op jit(solution)/shard_map/ppermute | solution.py:284
  35.0 6.3 %collective-permute-start.6 = (bf16[32,2048]{1,0:T(8,128)(2,1)S(1)}, bf16[32,2048]{1,0:T(8,128)(2,1)S(1)}, u32[]{:S(2)}, u32[]{:S(2)}) collective-permute-start(bf16[32,2048]{1,0:T(8,128)(2,1)S(1)} %get-tuple-element.32), channel_id=1, source_target_pairs={{0,2},{2,0},{4,6},{6,4},{8,10},{10,8},{12,14},{14,12},{1,3},{3,1},... | collective-permute-start | bytes 393224 | tf_op jit(solution)/shard_map/ppermute | solution.py:284
  37.0 5.7 %collective-permute-start.11 = (bf16[32,2048]{1,0:T(8,128)(2,1)S(1)}, bf16[32,2048]{1,0:T(8,128)(2,1)S(1)}, u32[]{:S(2)}, u32[]{:S(2)}) collective-permute-start(bf16[32,2048]{1,0:T(8,128)(2,1)S(1)} %shard_map.87), channel_id=1, source_target_pairs={{0,12},{2,14},{4,0},{6,2},{8,4},{10,6},{12,8},{14,10},{1,13},{3,15... | collective-permute-start | bytes 393224 | tf_op jit(solution)/shard_map/ppermute | solution.py:275
  40.3 7.1 %collective-permute-start.16 = (bf16[32,2048]{1,0:T(8,128)(2,1)S(1)}, bf16[32,2048]{1,0:T(8,128)(2,1)S(1)}, u32[]{:S(2)}, u32[]{:S(2)}) collective-permute-start(bf16[32,2048]{1,0:T(8,128)(2,1)S(1)} %shard_map.89), channel_id=1, source_target_pairs={{0,8},{2,10},{4,12},{6,14},{8,0},{10,2},{12,4},{14,6},{1,9},{3,11}... | collective-permute-start | bytes 393224 | tf_op jit(solution)/shard_map/ppermute | solution.py:275
  40.4 7.0 %collective-permute-start.18 = (bf16[32,2048]{1,0:T(8,128)(2,1)S(1)}, bf16[32,2048]{1,0:T(8,128)(2,1)S(1)}, u32[]{:S(2)}, u32[]{:S(2)}) collective-permute-start(bf16[32,2048]{1,0:T(8,128)(2,1)S(1)} %get-tuple-element.40), channel_id=1, source_target_pairs={{0,2},{2,0},{4,6},{6,4},{8,10},{10,8},{12,14},{14,12},{1,3},{3,1},... | collective-permute-start | bytes 393224 | tf_op jit(solution)/shard_map/ppermute | solution.py:284
  41.5 13.3 %collective-permute-start.7 = (bf16[32,2048]{1,0:T(8,128)(2,1)S(1)}, bf16[32,2048]{1,0:T(8,128)(2,1)S(1)}, u32[]{:S(2)}, u32[]{:S(2)}) collective-permute-start(bf16[32,2048]{1,0:T(8,128)(2,1)S(1)} %shard_map.85.refs_0_), channel_id=1, source_target_pairs={{0,1},{1,0},{2,3},{3,2},{4,5},{5,4},{6,7},{7,6},{8,9},{9,8},{10,11... | collective-permute-start | bytes 393224 | tf_op jit(solution)/shard_map/ppermute | solution.py:287
  42.7 12.1 %collective-permute-start.12 = (bf16[32,2048]{1,0:T(8,128)(2,1)S(1)}, bf16[32,2048]{1,0:T(8,128)(2,1)S(1)}, u32[]{:S(2)}, u32[]{:S(2)}) collective-permute-start(bf16[32,2048]{1,0:T(8,128)(2,1)S(1)} %collective-permute-done.11.refs_2_), channel_id=1, source_target_pairs={{0,1},{1,0},{2,3},{3,2},{4,5},{5,4},{6,7},{7,6},{8,9},{9,8},{10,11... | collective-permute-start | bytes 393224 | tf_op jit(solution)/shard_map/ppermute | solution.py:287
  47.4 7.5 %collective-permute-start.17 = (bf16[32,2048]{1,0:T(8,128)(2,1)S(1)}, bf16[32,2048]{1,0:T(8,128)(2,1)S(1)}, u32[]{:S(2)}, u32[]{:S(2)}) collective-permute-start(bf16[32,2048]{1,0:T(8,128)(2,1)S(1)} %collective-permute-done.16.refs_4_), channel_id=1, source_target_pairs={{0,1},{1,0},{2,3},{3,2},{4,5},{5,4},{6,7},{7,6},{8,9},{9,8},{10,11... | collective-permute-start | bytes 393224 | tf_op jit(solution)/shard_map/ppermute | solution.py:287
  47.5 6.8 %collective-permute-start.19 = (bf16[32,1024]{1,0:T(8,128)(2,1)S(1)}, bf16[32,1024]{1,0:T(8,128)(2,1)S(1)}, u32[]{:S(2)}, u32[]{:S(2)}) collective-permute-start(bf16[32,1024]{1,0:T(8,128)(2,1)S(1)} %get-tuple-element.41), channel_id=1, source_target_pairs={{0,4},{2,6},{4,8},{6,10},{8,12},{10,14},{12,0},{14,2},{1,5},{3,7},... | collective-permute-start | bytes 196616 | tf_op jit(solution)/shard_map/ppermute | solution.py:275
  48.1 6.7 %collective-permute-start.20 = (bf16[32,1024]{1,0:T(8,128)(2,1)S(1)}, bf16[32,1024]{1,0:T(8,128)(2,1)S(1)}, u32[]{:S(2)}, u32[]{:S(2)}) collective-permute-start(bf16[32,1024]{1,0:T(8,128)(2,1)S(1)} %get-tuple-element.42), channel_id=1, source_target_pairs={{0,5},{1,4},{2,7},{3,6},{4,9},{5,8},{6,11},{7,10},{8,13},{9,12},{1... | collective-permute-start | bytes 196616 | tf_op jit(solution)/shard_map/ppermute | solution.py:281
